TPU v7x, 512 devices: a whole 4x4x16 slice. The times are simulated.
512 devices in a mesh: gr: 2 (over z_hi), fs: 32 (over z_lo, y), tp: 8 (over x, core).
Axes of the slice: x: 4, y: 4, z: 16 (z_hi: 2, z_lo: 8; z = z_hi * 8 + z_lo), core: 2. Of those that a mesh axis runs over, the one named last changes fastest.
Arguments:
- tokens: bfloat16 [8192, 2048], P(('gr', 'fs')), may hold values from -6 to 6
- norm_gain: float32 [2048], P(('gr', 'fs')), may hold values from 0.1 to 1.9
- gate_train: float32 [32, 2048, 1024], P(None, ('gr', 'fs'), 'tp'), may hold values from -0.3125 to 0.3125
- up_train: float32 [32, 2048, 1024], P(None, ('gr', 'fs'), 'tp'), may hold values from -0.3125 to 0.3125
- down_train: float32 [32, 1024, 2048], P(None, ('gr', 'fs'), 'tp'), may hold values from -0.09375 to 0.09375
- routes: int32 [8192, 4], P(('gr', 'fs')), may hold values from 0 to 31, all different within a row; in each aligned block of 128 rows (0 to 127, 128 to 255, ...) at most 32 rows name the same one
- route_weight: float32 [8192, 4], P(('gr', 'fs')), may hold values from 0.05 to 1
Outputs:
- mixed: bfloat16 [8192, 2048], P(('gr', 'fs'), 'tp')
- gate_packed: bfloat16 [32, 2048, 1024], P('fs', None, 'tp')
- up_packed: bfloat16 [32, 2048, 1024], P('fs', None, 'tp')
- down_packed: bfloat16 [32, 1024, 2048], P('fs', 'tp')
Inputs may be any that keep to these rules, and one draw needn't show every extreme that they name: `routes`: each row names 4 different experts. Among the rows of one device no expert is named more than 32 times, and in every draw some expert is named exactly 32 times by the rows of some device.
All inputs are finite; a program needn't handle non-finite values.
Results may differ from a plain program's by a relative error of at most 0.015.
Values may be sent and summed in bfloat16 or wider, within the bound.
No kernel may reach another device: no remote copies, remote signals or barrier semaphores. Data moves between devices by JAX's collectives and lax.ppermute only.
A program may use at most 64 MiB of HBM per device.

v0:
```python
import jax
import jax.numpy as jnp
from jax import lax
from jax.sharding import Mesh
from jax.sharding import PartitionSpec as P

CAP = 32
CLAMP_LIMIT = 7.0
SLOPE_ALPHA = 1.702
NORM_EPSILON = 1e-06

GR, ZL, Y, X, C = 2, 8, 4, 4, 2
FS = ("zl", "y")

BF = jnp.bfloat16
F32 = jnp.float32


def ring(n, k):
    return [(i, (i + k) % n) for i in range(n)]


def exchange(a, axis):
    return lax.all_to_all(a, axis, split_axis=0, concat_axis=0, tiled=True)


def gather_tp(own):
    mine = [own] + [lax.ppermute(own, "x", ring(X, k)) for k in (1, 3, 2)]
    mine = [mine[0], mine[1], mine[3], mine[2]]
    other = [lax.ppermute(a, "c", ring(C, 1)) for a in mine]
    return [(mine[k], other[k]) for k in range(X)]


def relative(blocks, ix, ic):
    found = []
    for k in range(X):
        row = lax.dynamic_index_in_dim(blocks, (ix + X - k) % X, 0, keepdims=False)
        for s in range(C):
            found.append(lax.dynamic_index_in_dim(row, (ic + s) % C, 0, keepdims=False))
    return jnp.concatenate(found, axis=0)


def layer(tokens, norm_gain, gate_train, up_train, down_train, routes, route_weight):
    ix, iy, ic = lax.axis_index("x"), lax.axis_index("y"), lax.axis_index("c")
    n_tok, width = tokens.shape
    part = width // (X * C)
    n_exp = ZL * Y
    n_up, ff = gate_train.shape[1], gate_train.shape[2]

    hit = routes.T[None, :, :] == jnp.arange(n_exp, dtype=jnp.int32)[:, None, None]
    member = jnp.any(hit, axis=1)
    weight = jnp.sum(jnp.where(hit, route_weight.T[None, :, :], 0.0), axis=1)
    earlier = (jnp.arange(n_tok)[:, None] < jnp.arange(n_tok)[None, :]).astype(BF)
    rank = jnp.dot(member.astype(BF), earlier, preferred_element_type=F32).astype(jnp.int32)
    place = jnp.where(member, rank, -1)
    at_slot = place[:, None, :] == jnp.arange(CAP, dtype=jnp.int32)[None, :, None]
    pick = at_slot.astype(BF).reshape(n_exp * CAP, n_tok)

    wide = tokens.astype(F32)
    scale = lax.rsqrt(jnp.mean(wide * wide, axis=1, keepdims=True) + NORM_EPSILON)
    own = lax.dynamic_slice_in_dim(tokens, (ix * C + ic) * part, part, 1).astype(F32)
    normed = (own * scale).astype(BF)
    slots = jnp.dot(pick, normed, preferred_element_type=F32).astype(BF)
    arrived = exchange(slots.reshape(n_exp, CAP, part), FS)
    arrived = arrived.reshape(n_exp * CAP, part)

    gain = norm_gain[None, :, None]

    def column(j):
        at = (iy + j) % Y

        def take(a):
            cut = a.reshape(ZL, Y, a.shape[1], a.shape[2])
            return lax.dynamic_index_in_dim(cut, at, 1, keepdims=False)

        return jnp.concatenate(
            [(gain * take(gate_train)).astype(BF), (gain * take(up_train)).astype(BF)], axis=2
        )

    got = [column(0)] + [lax.ppermute(column(j), "y", ring(Y, j)) for j in range(1, Y)]
    by_offset = jnp.stack([got[(-j) % Y] for j in range(Y)], axis=1)
    by_source = lax.dynamic_slice_in_dim(
        jnp.concatenate([by_offset, by_offset], axis=1), (Y - iy) % Y, Y, 1
    ).reshape(ZL, Y * n_up, 2 * ff)
    by_source, arrived = lax.optimization_barrier((by_source, arrived))
    served = exchange(jnp.concatenate([by_source] * GR, axis=0), ("gr", "zl"))
    pieces = gather_tp(arrived)
    rows = jnp.concatenate([a for pair in pieces for a in pair], axis=1)

    down_local = down_train.astype(BF)
    down_local, served = lax.optimization_barrier((down_local, served))
    down_cols = exchange(jnp.concatenate([down_local] * GR, axis=0), ("gr",) + FS)
    served = served.reshape(width, 2 * ff)
    gate_weight = served[None, :, :ff]
    up_weight = served[None, :, ff:]

    pre = jnp.dot(
        rows, relative(served.reshape(X, C, part, 2 * ff), ix, ic), preferred_element_type=F32
    )
    clipped = jnp.minimum(pre[:, :ff], CLAMP_LIMIT)
    hidden = (
        (jnp.clip(pre[:, ff:], -CLAMP_LIMIT, CLAMP_LIMIT) + 1.0)
        * clipped
        * jax.nn.sigmoid(SLOPE_ALPHA * clipped)
    ).astype(BF)
    pieces = gather_tp(hidden)
    hidden_all = jnp.concatenate([a for pair in pieces for a in pair], axis=1)

    down_blocks = down_cols.reshape(X, C, ff, part)
    total = jnp.dot(hidden_all, relative(down_blocks, ix, ic), preferred_element_type=F32).astype(BF)
    result = exchange(total.reshape(n_exp, CAP, part), FS)

    kept = lax.dynamic_index_in_dim(down_blocks, ic, 1, keepdims=False)
    given = lax.dynamic_index_in_dim(down_blocks, 1 - ic, 1, keepdims=False)
    taken = lax.ppermute(given, "c", ring(C, 1))
    first = jnp.where(ic == 0, kept, taken)
    second = jnp.where(ic == 0, taken, kept)
    wide_rows = jnp.concatenate([first, second], axis=2)
    cols = []
    for k in range(X):
        block = lax.dynamic_index_in_dim(wide_rows, (ix + k) % X, 0, keepdims=False)
        cols.append(block if k == 0 else lax.ppermute(block, "x", ring(X, k)))
    around = jnp.stack([cols[(-j) % X] for j in range(X)] * 2, axis=0)
    ordered = lax.dynamic_slice_in_dim(around, (X - ix) % X, X, 0)
    down_weight = ordered.transpose(1, 0, 2).reshape(1, ff, width)

    spread = jnp.where(at_slot, weight[:, None, :], 0.0).reshape(n_exp * CAP, n_tok)
    high = lax.reduce_precision(spread, 8, 7)
    contract = (((0,), (0,)), ((), ()))
    result = result.reshape(n_exp * CAP, part)
    mixed = lax.dot_general(
        high.astype(BF), result, contract, preferred_element_type=F32
    ) + lax.dot_general((spread - high).astype(BF), result, contract, preferred_element_type=F32)
    return (mixed.astype(BF), gate_weight, up_weight, down_weight)


def solution(mesh):
    fine = Mesh(mesh.devices.reshape(GR, ZL, Y, X, C), ("gr", "zl", "y", "x", "c"))
    rows, tp = ("gr", "zl", "y"), ("x", "c")
    placed = (
        P(rows, None),
        P(rows),
        P(None, rows, tp),
        P(None, rows, tp),
        P(None, rows, tp),
        P(rows, None),
        P(rows, None),
    )
    return jax.shard_map(
        layer,
        mesh=fine,
        in_specs=placed,
        out_specs=(
            P(rows, tp),
            P(FS, None, tp),
            P(FS, None, tp),
            P(FS, tp, None),
        ),
        check_vma=False,
    )
```

profile of v0, /device:TPU:6, one launch (start us, length us, event | category | flops | bytes accessed | tf_op | source)
XLA Modules:
  0.0 197.3 jit_solution(11319108976307794598)
XLA Ops:
  1.6 1.2 multiply_reduce_fusion
  3.0 2.0 %convolution_convert_fusion.1 = bf16[1024,256]{1,0:T(8,128)(2,1)} fusion(pred[1024,128]{1,0:T(32,128)(4,1)S(1)} %bitcast_compare_fusion, f32[128]{0:T(128)S(1)} %add_rsqrt_fusion, bf16[128,2048]{1,0:T(8,128)(2,1)} %param.7, s32[]{:T(128)S(6)} %select_n.229), kind=kOutput, calls=%fused_computation.1 | convolution fusion | flops 67469312 | bytes 721412 | tf_op jit(solution)/shard_map/dot_general | solution.py:63
  5.0 15.5 %all-to-all-start = ((bf16[32,32,256]{2,1,0:T(8,128)(2,1)}), bf16[32,32,256]{2,1,0:T(8,128)(2,1)S(1)}, u32[]{:S(2)}, u32[]{:S(2)}) async-start(bf16[32,32,256]{2,1,0:T(8,128)(2,1)} %bitcast.24), calls=%async_computation | async-start | bytes 1048576 | tf_op jit(solution)/shard_map/all_to_all | solution.py:24
  20.6 1.5 fusion.23
  22.2 5.0 %collective-permute-start = (bf16[8,32,256]{2,1,0:T(8,128)(2,1)S(1)}, bf16[8,32,256]{2,1,0:T(8,128)(2,1)S(1)}, u32[]{:S(2)}, u32[]{:S(2)}) collective-permute-start(bf16[8,32,256]{2,1,0:T(8,128)(2,1)S(1)} %pad_maximum_fusion.2), channel_id=1, source_target_pairs={{0,24},{8,0},{16,8},{24,16},{1,25},{9,1},{17,9},{25,17},{2,26},{10... | collective-permute-start | bytes 393224 | tf_op jit(solution)/shard_map/ppermute | solution.py:80
  27.3 2.8 %collective-permute-start.1 = (bf16[8,32,256]{2,1,0:T(8,128)(2,1)S(1)}, bf16[8,32,256]{2,1,0:T(8,128)(2,1)S(1)}, u32[]{:S(2)}, u32[]{:S(2)}) collective-permute-start(bf16[8,32,256]{2,1,0:T(8,128)(2,1)S(1)} %pad_maximum_fusion.3), channel_id=1, source_target_pairs={{0,16},{8,24},{16,0},{24,8},{1,17},{9,25},{17,1},{25,9},{2,18},{10... | collective-permute-start | bytes 393224 | tf_op jit(solution)/shard_map/ppermute | solution.py:80
  30.0 2.8 %collective-permute-start.2 = (bf16[8,32,256]{2,1,0:T(8,128)(2,1)S(1)}, bf16[8,32,256]{2,1,0:T(8,128)(2,1)S(1)}, u32[]{:S(2)}, u32[]{:S(2)}) collective-permute-start(bf16[8,32,256]{2,1,0:T(8,128)(2,1)S(1)} %pad_maximum_fusion.4), channel_id=1, source_target_pairs={{0,8},{8,16},{16,24},{24,0},{1,9},{9,17},{17,25},{25,1},{2,10},{10... | collective-permute-start | bytes 393224 | tf_op jit(solution)/shard_map/ppermute | solution.py:80
  32.9 1.1 collective-permute-done
  33.9 3.9 %collective-permute-done.1 = bf16[8,32,256]{2,1,0:T(8,128)(2,1)S(1)} collective-permute-done((bf16[8,32,256]{2,1,0:T(8,128)(2,1)S(1)}, bf16[8,32,256]{2,1,0:T(8,128)(2,1)S(1)}, u32[]{:S(2)}, u32[]{:S(2)}) %collective-permute-start.1) | collective-permute-done | bytes 131104 | tf_op jit(solution)/shard_map/ppermute | solution.py:80
  37.8 1.5 collective-permute-done.2
  39.5 10.7 %all-to-all-done = bf16[32,32,256]{2,1,0:T(8,128)(2,1)S(1)} async-done(((bf16[32,32,256]{2,1,0:T(8,128)(2,1)}), bf16[32,32,256]{2,1,0:T(8,128)(2,1)S(1)}, u32[]{:S(2)}, u32[]{:S(2)}) %all-to-all-start) | async-done | bytes 524320 | tf_op jit(solution)/shard_map/all_to_all | solution.py:24
  50.2 1.1 pad_maximum_fusion
  51.3 7.7 %all-to-all-start.1 = ((bf16[16,128,256]{2,1,0:T(8,128)(2,1)}), bf16[16,128,256]{2,1,0:T(8,128)(2,1)S(1)}, u32[]{:S(2)}, u32[]{:S(2)}) async-start(bf16[16,128,256]{2,1,0:T(8,128)(2,1)} %pad_maximum_fusion), calls=%async_computation.1 | async-start | bytes 2097152 | tf_op jit(solution)/shard_map/all_to_all | solution.py:24
  59.0 2.4 %collective-permute-start.4 = (bf16[1024,256]{1,0:T(8,128)(2,1)S(1)}, bf16[1024,256]{1,0:T(8,128)(2,1)}, u32[]{:S(2)}, u32[]{:S(2)}) collective-permute-start(bf16[1024,256]{1,0:T(8,128)(2,1)S(1)} %bitcast.168), channel_id=1, source_target_pairs={{0,2},{2,4},{4,6},{6,0},{1,3},{3,5},{5,7},{7,1},{8,10},{10,12},{12... | collective-permute-start | bytes 1572872 | tf_op jit(solution)/shard_map/ppermute | solution.py:28
  61.4 4.3 %collective-permute-start.6 = (bf16[1024,256]{1,0:T(8,128)(2,1)S(1)}, bf16[1024,256]{1,0:T(8,128)(2,1)S(1)}, u32[]{:S(2)}, u32[]{:S(2)}) collective-permute-start(bf16[1024,256]{1,0:T(8,128)(2,1)S(1)} %bitcast.169), channel_id=1, source_target_pairs={{0,4},{2,6},{4,0},{6,2},{1,5},{3,7},{5,1},{7,3},{8,12},{10,14},{12... | collective-permute-start | bytes 1572872 | tf_op jit(solution)/shard_map/ppermute | solution.py:28
  65.7 1.9 collective-permute-start.8
  67.7 1.9 collective-permute-start.3
  69.6 6.2 %collective-permute-done.4 = bf16[1024,256]{1,0:T(8,128)(2,1)} collective-permute-done((bf16[1024,256]{1,0:T(8,128)(2,1)S(1)}, bf16[1024,256]{1,0:T(8,128)(2,1)}, u32[]{:S(2)}, u32[]{:S(2)}) %collective-permute-start.4) | collective-permute-done | bytes 524320 | tf_op jit(solution)/shard_map/ppermute | solution.py:28
  75.8 1.9 collective-permute-start.5
  77.9 1.7 collective-permute-done.6
  79.6 1.9 collective-permute-start.7
  82.4 4.1 %collective-permute-done.8 = bf16[1024,256]{1,0:T(8,128)(2,1)S(1)} collective-permute-done((bf16[1024,256]{1,0:T(8,128)(2,1)S(1)}, bf16[1024,256]{1,0:T(8,128)(2,1)S(1)}, u32[]{:S(2)}, u32[]{:S(2)}) %collective-permute-start.8) | collective-permute-done | bytes 524320 | tf_op jit(solution)/shard_map/ppermute | solution.py:28
  86.6 1.9 collective-permute-start.9
  88.5 1.9 constant_dynamic-update-slice_fusion.8
  90.4 1.9 constant_dynamic-update-slice_fusion.7
  92.3 1.9 constant_dynamic-update-slice_fusion.6
  97.7 7.6 %all-to-all-done.1 = bf16[16,128,256]{2,1,0:T(8,128)(2,1)S(1)} async-done(((bf16[16,128,256]{2,1,0:T(8,128)(2,1)}), bf16[16,128,256]{2,1,0:T(8,128)(2,1)S(1)}, u32[]{:S(2)}, u32[]{:S(2)}) %all-to-all-start.1) | async-done | bytes 1048608 | tf_op jit(solution)/shard_map/all_to_all | solution.py:24
  106.3 11.4 %all-to-all-start.2 = ((bf16[64,16,256]{2,1,0:T(8,128)(2,1)}), bf16[64,16,256]{2,1,0:T(8,128)(2,1)S(1)}, u32[]{:S(2)}, u32[]{:S(2)}) async-start(bf16[64,16,256]{2,1,0:T(8,128)(2,1)} %pad_maximum_fusion.1), calls=%async_computation.2 | async-start | bytes 1048576 | tf_op jit(solution)/shard_map/all_to_all | solution.py:24
  117.7 3.5 %fusion.37 = f32[1024,256]{0,1:T(8,128)S(1)} fusion(bf16[1024,2048]{1,0:T(8,128)(2,1)} %constant_dynamic-update-slice_fusion.2, bf16[2048,256]{1,0:T(8,128)(2,1)S(1)} %bitcast_dynamic-update-slice_fusion.10), kind=kOutput, calls=%fused_computation.129 | convolution fusion | flops 1073741824 | bytes 6291456 | tf_op jit(solution)/shard_map/dot_general | solution.py:97
  122.1 2.4 %collective-permute-start.11 = (bf16[1024,128]{0,1:T(8,128)(2,1)S(1)}, bf16[1024,128]{0,1:T(8,128)(2,1)S(1)}, u32[]{:S(2)}, u32[]{:S(2)}) collective-permute-start(bf16[1024,128]{0,1:T(8,128)(2,1)S(1)} %get-tuple-element.21), channel_id=1, source_target_pairs={{0,2},{2,4},{4,6},{6,0},{1,3},{3,5},{5,7},{7,1},{8,10},{10,12},{12... | collective-permute-start | bytes 786440 | tf_op jit(solution)/shard_map/ppermute | solution.py:28
  124.5 4.3 %collective-permute-start.13 = (bf16[1024,128]{0,1:T(8,128)(2,1)S(1)}, bf16[1024,128]{0,1:T(8,128)(2,1)S(1)}, u32[]{:S(2)}, u32[]{:S(2)}) collective-permute-start(bf16[1024,128]{0,1:T(8,128)(2,1)S(1)} %get-tuple-element.21), channel_id=1, source_target_pairs={{0,4},{2,6},{4,0},{6,2},{1,5},{3,7},{5,1},{7,3},{8,12},{10,14},{12... | collective-permute-start | bytes 786440 | tf_op jit(solution)/shard_map/ppermute | solution.py:28
  128.8 1.9 collective-permute-start.10
  130.8 1.9 collective-permute-start.15
  133.2 1.9 collective-permute-start.12
  135.2 2.4 %collective-permute-start.14 = (bf16[1024,128]{0,1:T(8,128)(2,1)S(1)}, bf16[1024,128]{0,1:T(8,128)(2,1)S(1)}, u32[]{:S(2)}, u32[]{:S(2)}) collective-permute-start(bf16[1024,128]{0,1:T(8,128)(2,1)S(1)} %collective-permute-done.13), channel_id=1, source_target_pairs={{0,1},{1,0},{2,3},{3,2},{4,5},{5,4},{6,7},{7,6},{8,9},{9,8},{10,11... | collective-permute-start | bytes 786440 | tf_op jit(solution)/shard_map/ppermute | solution.py:30
  139.0 3.5 %collective-permute-done.15 = bf16[1024,128]{0,1:T(8,128)(2,1)S(1)} collective-permute-done((bf16[1024,128]{0,1:T(8,128)(2,1)S(1)}, bf16[1024,128]{0,1:T(8,128)(2,1)S(1)}, u32[]{:S(2)}, u32[]{:S(2)}) %collective-permute-start.15) | collective-permute-done | bytes 262176 | tf_op jit(solution)/shard_map/ppermute | solution.py:28
  142.6 1.9 collective-permute-start.16
  148.2 1.7 all-to-all-done.2
  150.1 1.9 collective-permute-start.17
  152.0 3.2 %convolution_convert_fusion = bf16[1024,256]{1,0:T(8,128)(2,1)} fusion(bf16[1024,1024]{0,1:T(8,128)(2,1)} %constant_dynamic-update-slice_fusion.10, bf16[1024,256]{1,0:T(8,128)(2,1)S(1)} %constant_dynamic-update-slice_fusion.18), kind=kOutput, calls=%fused_computation | convolution fusion | flops 537133056 | bytes 3145728 | tf_op jit(solution)/shard_map/dot_general | solution.py:110
  155.2 11.1 %all-to-all-start.3 = ((bf16[32,32,256]{2,1,0:T(8,128)(2,1)}), bf16[32,32,256]{2,1,0:T(8,128)(2,1)S(1)}, u32[]{:S(2)}, u32[]{:S(2)}) async-start(bf16[32,32,256]{2,1,0:T(8,128)(2,1)} %bitcast.44), calls=%async_computation.3 | async-start | bytes 1048576 | tf_op jit(solution)/shard_map/all_to_all | solution.py:24
  166.4 1.9 collective-permute-start.18
  168.3 1.0 slice_bitcast_fusion
  169.4 3.9 %collective-permute-start.19 = (bf16[128,512]{1,0:T(8,128)(2,1)S(1)}, bf16[128,512]{1,0:T(8,128)(2,1)S(1)}, u32[]{:S(2)}, u32[]{:S(2)}) collective-permute-start(bf16[128,512]{1,0:T(8,128)(2,1)S(1)} %get-tuple-element.37), channel_id=1, source_target_pairs={{0,4},{2,6},{4,0},{6,2},{1,5},{3,7},{5,1},{7,3},{8,12},{10,14},{12... | collective-permute-start | bytes 393224 | tf_op jit(solution)/shard_map/ppermute | solution.py:122
  173.3 3.1 %collective-permute-start.20 = (bf16[128,512]{1,0:T(8,128)(2,1)S(1)}, bf16[128,512]{1,0:T(8,128)(2,1)S(1)}, u32[]{:S(2)}, u32[]{:S(2)}) collective-permute-start(bf16[128,512]{1,0:T(8,128)(2,1)S(1)} %get-tuple-element.34), channel_id=1, source_target_pairs={{0,2},{2,4},{4,6},{6,0},{1,3},{3,5},{5,7},{7,1},{8,10},{10,12},{12... | collective-permute-start | bytes 393224 | tf_op jit(solution)/shard_map/ppermute | solution.py:122
  176.4 1.4 collective-permute-done.19
  177.9 3.2 %collective-permute-done.20 = bf16[128,512]{1,0:T(8,128)(2,1)S(1)} collective-permute-done((bf16[128,512]{1,0:T(8,128)(2,1)S(1)}, bf16[128,512]{1,0:T(8,128)(2,1)S(1)}, u32[]{:S(2)}, u32[]{:S(2)}) %collective-permute-start.20) | collective-permute-done | bytes 131104 | tf_op jit(solution)/shard_map/ppermute | solution.py:122
  182.5 13.6 %all-to-all-done.3 = bf16[32,32,256]{2,1,0:T(8,128)(2,1)S(1)} async-done(((bf16[32,32,256]{2,1,0:T(8,128)(2,1)}), bf16[32,32,256]{2,1,0:T(8,128)(2,1)S(1)}, u32[]{:S(2)}, u32[]{:S(2)}) %all-to-all-start.3) | async-done | bytes 524320 | tf_op jit(solution)/shard_map/all_to_all | solution.py:24
  (83 shorter events, 16.1 us)
Async XLA Ops:
  5.0 45.2 %all-to-all-start = ((bf16[32,32,256]{2,1,0:T(8,128)(2,1)}), bf16[32,32,256]{2,1,0:T(8,128)(2,1)S(1)}, u32[]{:S(2)}, u32[]{:S(2)}) async-start(bf16[32,32,256]{2,1,0:T(8,128)(2,1)} %bitcast.24), calls=%async_computation | async-start | bytes 1048576 | tf_op jit(solution)/shard_map/all_to_all | solution.py:24
  22.1 55.7 %copy-start = (f32[32,16,256]{2,1,0:T(8,128)S(1)}, f32[32,16,256]{2,1,0:T(8,128)}, u32[]{:S(2)}) copy-start(f32[32,16,256]{2,1,0:T(8,128)} %param.11) | copy-start | bytes 1572868
  22.2 11.8 %collective-permute-start = (bf16[8,32,256]{2,1,0:T(8,128)(2,1)S(1)}, bf16[8,32,256]{2,1,0:T(8,128)(2,1)S(1)}, u32[]{:S(2)}, u32[]{:S(2)}) collective-permute-start(bf16[8,32,256]{2,1,0:T(8,128)(2,1)S(1)} %pad_maximum_fusion.2), channel_id=1, source_target_pairs={{0,24},{8,0},{16,8},{24,16},{1,25},{9,1},{17,9},{25,17},{2,26},{10... | collective-permute-start | bytes 393224 | tf_op jit(solution)/shard_map/ppermute | solution.py:80
  27.3 10.6 %collective-permute-start.1 = (bf16[8,32,256]{2,1,0:T(8,128)(2,1)S(1)}, bf16[8,32,256]{2,1,0:T(8,128)(2,1)S(1)}, u32[]{:S(2)}, u32[]{:S(2)}) collective-permute-start(bf16[8,32,256]{2,1,0:T(8,128)(2,1)S(1)} %pad_maximum_fusion.3), channel_id=1, source_target_pairs={{0,16},{8,24},{16,0},{24,8},{1,17},{9,25},{17,1},{25,9},{2,18},{10... | collective-permute-start | bytes 393224 | tf_op jit(solution)/shard_map/ppermute | solution.py:80
  30.0 9.3 %collective-permute-start.2 = (bf16[8,32,256]{2,1,0:T(8,128)(2,1)S(1)}, bf16[8,32,256]{2,1,0:T(8,128)(2,1)S(1)}, u32[]{:S(2)}, u32[]{:S(2)}) collective-permute-start(bf16[8,32,256]{2,1,0:T(8,128)(2,1)S(1)} %pad_maximum_fusion.4), channel_id=1, source_target_pairs={{0,8},{8,16},{16,24},{24,0},{1,9},{9,17},{17,25},{25,1},{2,10},{10... | collective-permute-start | bytes 393224 | tf_op jit(solution)/shard_map/ppermute | solution.py:80
  51.3 54.0 %all-to-all-start.1 = ((bf16[16,128,256]{2,1,0:T(8,128)(2,1)}), bf16[16,128,256]{2,1,0:T(8,128)(2,1)S(1)}, u32[]{:S(2)}, u32[]{:S(2)}) async-start(bf16[16,128,256]{2,1,0:T(8,128)(2,1)} %pad_maximum_fusion), calls=%async_computation.1 | async-start | bytes 2097152 | tf_op jit(solution)/shard_map/all_to_all | solution.py:24
  59.0 16.8 %collective-permute-start.4 = (bf16[1024,256]{1,0:T(8,128)(2,1)S(1)}, bf16[1024,256]{1,0:T(8,128)(2,1)}, u32[]{:S(2)}, u32[]{:S(2)}) collective-permute-start(bf16[1024,256]{1,0:T(8,128)(2,1)S(1)} %bitcast.168), channel_id=1, source_target_pairs={{0,2},{2,4},{4,6},{6,0},{1,3},{3,5},{5,7},{7,1},{8,10},{10,12},{12... | collective-permute-start | bytes 1572872 | tf_op jit(solution)/shard_map/ppermute | solution.py:28
  61.4 18.2 %collective-permute-start.6 = (bf16[1024,256]{1,0:T(8,128)(2,1)S(1)}, bf16[1024,256]{1,0:T(8,128)(2,1)S(1)}, u32[]{:S(2)}, u32[]{:S(2)}) collective-permute-start(bf16[1024,256]{1,0:T(8,128)(2,1)S(1)} %bitcast.169), channel_id=1, source_target_pairs={{0,4},{2,6},{4,0},{6,2},{1,5},{3,7},{5,1},{7,3},{8,12},{10,14},{12... | collective-permute-start | bytes 1572872 | tf_op jit(solution)/shard_map/ppermute | solution.py:28
  65.7 20.8 %collective-permute-start.8 = (bf16[1024,256]{1,0:T(8,128)(2,1)S(1)}, bf16[1024,256]{1,0:T(8,128)(2,1)S(1)}, u32[]{:S(2)}, u32[]{:S(2)}) collective-permute-start(bf16[1024,256]{1,0:T(8,128)(2,1)S(1)} %bitcast.170), channel_id=1, source_target_pairs={{0,6},{2,0},{4,2},{6,4},{1,7},{3,1},{5,3},{7,5},{8,14},{10,8},{12,... | collective-permute-start | bytes 1572872 | tf_op jit(solution)/shard_map/ppermute | solution.py:28
  67.7 20.8 %collective-permute-start.3 = (bf16[1024,256]{1,0:T(8,128)(2,1)S(1)}, bf16[1024,256]{1,0:T(8,128)(2,1)}, u32[]{:S(2)}, u32[]{:S(2)}) collective-permute-start(bf16[1024,256]{1,0:T(8,128)(2,1)S(1)} %bitcast.171), channel_id=1, source_target_pairs={{0,1},{1,0},{2,3},{3,2},{4,5},{5,4},{6,7},{7,6},{8,9},{9,8},{10,11... | collective-permute-start | bytes 1572872 | tf_op jit(solution)/shard_map/ppermute | solution.py:30
  75.8 16.5 %collective-permute-start.5 = (bf16[1024,256]{1,0:T(8,128)(2,1)}, bf16[1024,256]{1,0:T(8,128)(2,1)}, u32[]{:S(2)}, u32[]{:S(2)}) collective-permute-start(bf16[1024,256]{1,0:T(8,128)(2,1)} %collective-permute-done.4), channel_id=1, source_target_pairs={{0,1},{1,0},{2,3},{3,2},{4,5},{5,4},{6,7},{7,6},{8,9},{9,8},{10,11... | collective-permute-start | bytes 1572872 | tf_op jit(solution)/shard_map/ppermute | solution.py:30
  79.6 15.5 %collective-permute-start.7 = (bf16[1024,256]{1,0:T(8,128)(2,1)S(1)}, bf16[1024,256]{1,0:T(8,128)(2,1)S(1)}, u32[]{:S(2)}, u32[]{:S(2)}) collective-permute-start(bf16[1024,256]{1,0:T(8,128)(2,1)S(1)} %collective-permute-done.6), channel_id=1, source_target_pairs={{0,1},{1,0},{2,3},{3,2},{4,5},{5,4},{6,7},{7,6},{8,9},{9,8},{10,11... | collective-permute-start | bytes 1572872 | tf_op jit(solution)/shard_map/ppermute | solution.py:30
  86.6 10.3 %collective-permute-start.9 = (bf16[1024,256]{1,0:T(8,128)(2,1)S(1)}, bf16[1024,256]{1,0:T(8,128)(2,1)S(1)}, u32[]{:S(2)}, u32[]{:S(2)}) collective-permute-start(bf16[1024,256]{1,0:T(8,128)(2,1)S(1)} %collective-permute-done.8), channel_id=1, source_target_pairs={{0,1},{1,0},{2,3},{3,2},{4,5},{5,4},{6,7},{7,6},{8,9},{9,8},{10,11... | collective-permute-start | bytes 1572872 | tf_op jit(solution)/shard_map/ppermute | solution.py:30
  106.3 43.6 %all-to-all-start.2 = ((bf16[64,16,256]{2,1,0:T(8,128)(2,1)}), bf16[64,16,256]{2,1,0:T(8,128)(2,1)S(1)}, u32[]{:S(2)}, u32[]{:S(2)}) async-start(bf16[64,16,256]{2,1,0:T(8,128)(2,1)} %pad_maximum_fusion.1), calls=%async_computation.2 | async-start | bytes 1048576 | tf_op jit(solution)/shard_map/all_to_all | solution.py:24
  117.7 17.4 %copy-start.1 = (s32[128,4]{0,1:T(4,128)S(1)}, s32[128,4]{0,1:T(4,128)}, u32[]{:S(2)}) copy-start(s32[128,4]{0,1:T(4,128)} %param.12) | copy-start | bytes 6148
  117.7 17.4 %copy-start.2 = (f32[128,4]{0,1:T(4,128)S(1)}, f32[128,4]{0,1:T(4,128)}, u32[]{:S(2)}) copy-start(f32[128,4]{0,1:T(4,128)} %param.13) | copy-start | bytes 6148
  122.1 11.1 %collective-permute-start.11 = (bf16[1024,128]{0,1:T(8,128)(2,1)S(1)}, bf16[1024,128]{0,1:T(8,128)(2,1)S(1)}, u32[]{:S(2)}, u32[]{:S(2)}) collective-permute-start(bf16[1024,128]{0,1:T(8,128)(2,1)S(1)} %get-tuple-element.21), channel_id=1, source_target_pairs={{0,2},{2,4},{4,6},{6,0},{1,3},{3,5},{5,7},{7,1},{8,10},{10,12},{12... | collective-permute-start | bytes 786440 | tf_op jit(solution)/shard_map/ppermute | solution.py:28
  124.5 10.7 %collective-permute-start.13 = (bf16[1024,128]{0,1:T(8,128)(2,1)S(1)}, bf16[1024,128]{0,1:T(8,128)(2,1)S(1)}, u32[]{:S(2)}, u32[]{:S(2)}) collective-permute-start(bf16[1024,128]{0,1:T(8,128)(2,1)S(1)} %get-tuple-element.21), channel_id=1, source_target_pairs={{0,4},{2,6},{4,0},{6,2},{1,5},{3,7},{5,1},{7,3},{8,12},{10,14},{12... | collective-permute-start | bytes 786440 | tf_op jit(solution)/shard_map/ppermute | solution.py:28
  128.8 8.8 %collective-permute-start.10 = (bf16[1024,128]{0,1:T(8,128)(2,1)S(1)}, bf16[1024,128]{0,1:T(8,128)(2,1)S(1)}, u32[]{:S(2)}, u32[]{:S(2)}) collective-permute-start(bf16[1024,128]{0,1:T(8,128)(2,1)S(1)} %get-tuple-element.21), channel_id=1, source_target_pairs={{0,1},{1,0},{2,3},{3,2},{4,5},{5,4},{6,7},{7,6},{8,9},{9,8},{10,11... | collective-permute-start | bytes 786440 | tf_op jit(solution)/shard_map/ppermute | solution.py:30
  130.8 11.8 %collective-permute-start.15 = (bf16[1024,128]{0,1:T(8,128)(2,1)S(1)}, bf16[1024,128]{0,1:T(8,128)(2,1)S(1)}, u32[]{:S(2)}, u32[]{:S(2)}) collective-permute-start(bf16[1024,128]{0,1:T(8,128)(2,1)S(1)} %get-tuple-element.21), channel_id=1, source_target_pairs={{0,6},{2,0},{4,2},{6,4},{1,7},{3,1},{5,3},{7,5},{8,14},{10,8},{12,... | collective-permute-start | bytes 786440 | tf_op jit(solution)/shard_map/ppermute | solution.py:28
  133.2 11.3 %collective-permute-start.12 = (bf16[1024,128]{0,1:T(8,128)(2,1)S(1)}, bf16[1024,128]{0,1:T(8,128)(2,1)S(1)}, u32[]{:S(2)}, u32[]{:S(2)}) collective-permute-start(bf16[1024,128]{0,1:T(8,128)(2,1)S(1)} %collective-permute-done.11), channel_id=1, source_target_pairs={{0,1},{1,0},{2,3},{3,2},{4,5},{5,4},{6,7},{7,6},{8,9},{9,8},{10,11... | collective-permute-start | bytes 786440 | tf_op jit(solution)/shard_map/ppermute | solution.py:30
  135.2 10.8 %collective-permute-start.14 = (bf16[1024,128]{0,1:T(8,128)(2,1)S(1)}, bf16[1024,128]{0,1:T(8,128)(2,1)S(1)}, u32[]{:S(2)}, u32[]{:S(2)}) collective-permute-start(bf16[1024,128]{0,1:T(8,128)(2,1)S(1)} %collective-permute-done.13), channel_id=1, source_target_pairs={{0,1},{1,0},{2,3},{3,2},{4,5},{5,4},{6,7},{7,6},{8,9},{9,8},{10,11... | collective-permute-start | bytes 786440 | tf_op jit(solution)/shard_map/ppermute | solution.py:30
  142.6 4.9 %collective-permute-start.16 = (bf16[1024,128]{0,1:T(8,128)(2,1)S(1)}, bf16[1024,128]{0,1:T(8,128)(2,1)S(1)}, u32[]{:S(2)}, u32[]{:S(2)}) collective-permute-start(bf16[1024,128]{0,1:T(8,128)(2,1)S(1)} %collective-permute-done.15), channel_id=1, source_target_pairs={{0,1},{1,0},{2,3},{3,2},{4,5},{5,4},{6,7},{7,6},{8,9},{9,8},{10,11... | collective-permute-start | bytes 786440 | tf_op jit(solution)/shard_map/ppermute | solution.py:30
  150.1 16.2 %collective-permute-start.17 = (bf16[4,128,256]{2,1,0:T(8,128)(2,1)S(1)}, bf16[4,128,256]{2,1,0:T(8,128)(2,1)S(1)}, u32[]{:S(2)}, u32[]{:S(2)}) collective-permute-start(bf16[4,128,256]{2,1,0:T(8,128)(2,1)S(1)} %dynamic-slice_bitcast_fusion.1), channel_id=1, source_target_pairs={{0,1},{1,0},{2,3},{3,2},{4,5},{5,4},{6,7},{7,6},{8,9},{9,8},{10,11... | collective-permute-start | bytes 786440 | tf_op jit(solution)/shard_map/ppermute | solution.py:115
  155.2 40.9 %all-to-all-start.3 = ((bf16[32,32,256]{2,1,0:T(8,128)(2,1)}), bf16[32,32,256]{2,1,0:T(8,128)(2,1)S(1)}, u32[]{:S(2)}, u32[]{:S(2)}) async-start(bf16[32,32,256]{2,1,0:T(8,128)(2,1)} %bitcast.44), calls=%async_computation.3 | async-start | bytes 1048576 | tf_op jit(solution)/shard_map/all_to_all | solution.py:24
  166.4 10.0 %collective-permute-start.18 = (bf16[128,512]{1,0:T(8,128)(2,1)S(1)}, bf16[128,512]{1,0:T(8,128)(2,1)S(1)}, u32[]{:S(2)}, u32[]{:S(2)}) collective-permute-start(bf16[128,512]{1,0:T(8,128)(2,1)S(1)} %get-tuple-element.36), channel_id=1, source_target_pairs={{0,6},{2,0},{4,2},{6,4},{1,7},{3,1},{5,3},{7,5},{8,14},{10,8},{12,... | collective-permute-start | bytes 393224 | tf_op jit(solution)/shard_map/ppermute | solution.py:122
  169.4 8.5 %collective-permute-start.19 = (bf16[128,512]{1,0:T(8,128)(2,1)S(1)}, bf16[128,512]{1,0:T(8,128)(2,1)S(1)}, u32[]{:S(2)}, u32[]{:S(2)}) collective-permute-start(bf16[128,512]{1,0:T(8,128)(2,1)S(1)} %get-tuple-element.37), channel_id=1, source_target_pairs={{0,4},{2,6},{4,0},{6,2},{1,5},{3,7},{5,1},{7,3},{8,12},{10,14},{12... | collective-permute-start | bytes 393224 | tf_op jit(solution)/shard_map/ppermute | solution.py:122
  173.3 7.8 %collective-permute-start.20 = (bf16[128,512]{1,0:T(8,128)(2,1)S(1)}, bf16[128,512]{1,0:T(8,128)(2,1)S(1)}, u32[]{:S(2)}, u32[]{:S(2)}) collective-permute-start(bf16[128,512]{1,0:T(8,128)(2,1)S(1)} %get-tuple-element.34), channel_id=1, source_target_pairs={{0,2},{2,4},{4,6},{6,0},{1,3},{3,5},{5,7},{7,1},{8,10},{10,12},{12... | collective-permute-start | bytes 393224 | tf_op jit(solution)/shard_map/ppermute | solution.py:122
where the time goes:
time: 199 us; the launch traced here: 197 us
  starting transfers between devices  100 us (50%)
  waiting for transfers between devices  60.7 us (31%)
  local copies, waits for them, and re-layouts  18.1 us (9%)
  matrix products  9.97 us (5%)
  other arithmetic  6.73 us (3%)
    all_to_all x4, starting transfers between devices, exchange(): return lax.all_to_all(a, axis, split_axis=0, concat_axis=0, tiled=True)  45.7 us
    all_to_all x4, waiting for transfers between devices, exchange(): return lax.all_to_all(a, axis, split_axis=0, concat_axis=0, tiled=True)  33.6 us
    ppermute x6, starting transfers between devices, gather_tp(): mine = [own] + [lax.ppermute(own, 'x', ring(X, k)) for k in (1, 3, 2)]  17.3 us
    ppermute x6, waiting for transfers between devices, gather_tp(): mine = [own] + [lax.ppermute(own, 'x', ring(X, k)) for k in (1, 3, 2)]  16.1 us
    ppermute x8, starting transfers between devices, gather_tp(): other = [lax.ppermute(a, 'c', ring(C, 1)) for a in mine]  15.8 us
    unnamed x44, local copies, waits for them, and re-layouts  14.9 us
    ppermute x3, starting transfers between devices, layer(): lax.ppermute(column(j), 'y', ring(Y, j))  10.6 us
    ppermute x3, starting transfers between devices, layer(): cols.append(block if k == 0 else lax.ppermute(block, 'x', ring(X, k)))  8.96 us
  transfers between devices with their start and end apart: 25, of which 14 were waited for; matrix products, arithmetic and copies ran while one was open for 14% of the time, Pallas kernels for 0%

commit v1 on v0

--- a/solution.py
+++ b/solution.py
@@ -3,6 +3,7 @@
 from jax import lax
 from jax.sharding import Mesh
 from jax.sharding import PartitionSpec as P
+
 
 CAP = 32
 CLAMP_LIMIT = 7.0
@@ -24,11 +25,13 @@
     return lax.all_to_all(a, axis, split_axis=0, concat_axis=0, tiled=True)
 
 
-def gather_tp(own):
-    mine = [own] + [lax.ppermute(own, "x", ring(X, k)) for k in (1, 3, 2)]
-    mine = [mine[0], mine[1], mine[3], mine[2]]
-    other = [lax.ppermute(a, "c", ring(C, 1)) for a in mine]
-    return [(mine[k], other[k]) for k in range(X)]
+def along_x(own):
+    sent = {k: lax.ppermute(own, "x", ring(X, k)) for k in (1, 3, 2)}
+    return [own, sent[1], sent[2], sent[3]]
+
+
+def other_core(a):
+    return lax.ppermute(a, "c", ring(C, 1))
 
 
 def relative(blocks, ix, ic):
@@ -45,7 +48,7 @@
     n_tok, width = tokens.shape
     part = width // (X * C)
     n_exp = ZL * Y
-    n_up, ff = gate_train.shape[1], gate_train.shape[2]
+    n_up, ff, n_down = gate_train.shape[1], gate_train.shape[2], down_train.shape[1]
 
     hit = routes.T[None, :, :] == jnp.arange(n_exp, dtype=jnp.int32)[:, None, None]
     member = jnp.any(hit, axis=1)
@@ -61,8 +64,10 @@
     own = lax.dynamic_slice_in_dim(tokens, (ix * C + ic) * part, part, 1).astype(F32)
     normed = (own * scale).astype(BF)
     slots = jnp.dot(pick, normed, preferred_element_type=F32).astype(BF)
-    arrived = exchange(slots.reshape(n_exp, CAP, part), FS)
-    arrived = arrived.reshape(n_exp * CAP, part)
+    slots = slots.reshape(n_exp, CAP, part)
+    mixed_in = exchange(jnp.concatenate([slots, down_train.astype(BF)], axis=1), FS)
+    arrived = mixed_in[:, :CAP].reshape(n_exp * CAP, part)
+    down_half = mixed_in[:, CAP:].reshape(n_exp * n_down, part)
 
     gain = norm_gain[None, :, None]
 
@@ -82,14 +87,16 @@
     by_source = lax.dynamic_slice_in_dim(
         jnp.concatenate([by_offset, by_offset], axis=1), (Y - iy) % Y, Y, 1
     ).reshape(ZL, Y * n_up, 2 * ff)
-    by_source, arrived = lax.optimization_barrier((by_source, arrived))
-    served = exchange(jnp.concatenate([by_source] * GR, axis=0), ("gr", "zl"))
-    pieces = gather_tp(arrived)
-    rows = jnp.concatenate([a for pair in pieces for a in pair], axis=1)
+    twice = jnp.concatenate([by_source] * GR, axis=0)
+    twice, arrived = lax.optimization_barrier((twice, arrived))
+    served = exchange(twice, ("gr", "zl"))
+    near = along_x(arrived)
+    far = {k: other_core(near[k]) for k in (0, 1, 3)}
+    down_half, near[2] = lax.optimization_barrier((down_half, near[2]))
+    down_other = lax.ppermute(down_half, "gr", ring(GR, 1))
+    far[2] = other_core(near[2])
+    rows = jnp.concatenate([a for k in range(X) for a in (near[k], far[k])], axis=1)
 
-    down_local = down_train.astype(BF)
-    down_local, served = lax.optimization_barrier((down_local, served))
-    down_cols = exchange(jnp.concatenate([down_local] * GR, axis=0), ("gr",) + FS)
     served = served.reshape(width, 2 * ff)
     gate_weight = served[None, :, :ff]
     up_weight = served[None, :, ff:]
@@ -103,11 +110,25 @@
         * clipped
         * jax.nn.sigmoid(SLOPE_ALPHA * clipped)
     ).astype(BF)
-    pieces = gather_tp(hidden)
-    hidden_all = jnp.concatenate([a for pair in pieces for a in pair], axis=1)
+    own_core = exchange(jnp.broadcast_to(hidden[None], (X,) + hidden.shape), "x")
+    their_core = other_core(own_core)
 
-    down_blocks = down_cols.reshape(X, C, ff, part)
-    total = jnp.dot(hidden_all, relative(down_blocks, ix, ic), preferred_element_type=F32).astype(BF)
+    ig = lax.axis_index("gr")
+    down_blocks = jnp.concatenate(
+        [jnp.where(ig == 0, down_half, down_other), jnp.where(ig == 0, down_other, down_half)], axis=0
+    ).reshape(X, C, ff, part)
+
+    def down_of(core):
+        return lax.dynamic_index_in_dim(down_blocks, core, 1, keepdims=False).reshape(X * ff, part)
+
+    def flat(a):
+        return jnp.concatenate([a[x] for x in range(X)], axis=1)
+
+    total = (
+        jnp.dot(flat(own_core), down_of(ic), preferred_element_type=F32)
+        + jnp.dot(flat(their_core), down_of(1 - ic), preferred_element_type=F32)
+    ).astype(BF)
+    total, down_blocks = lax.optimization_barrier((total, down_blocks))
     result = exchange(total.reshape(n_exp, CAP, part), FS)
 
     kept = lax.dynamic_index_in_dim(down_blocks, ic, 1, keepdims=False)

time: 199 us -> 211 us (1.060)
  the two profiles are of different devices: /device:TPU:6 before, /device:TPU:2 now
where the time goes in v1:
time: 211 us; the launch traced here: 210 us
  starting transfers between devices  105 us (50%)
  waiting for transfers between devices  72.7 us (34%)
  local copies, waits for them, and re-layouts  16.5 us (8%)
  matrix products  7.66 us (4%)
  other arithmetic  6.01 us (3%)
    all_to_all x4, starting transfers between devices, exchange(): return lax.all_to_all(a, axis, split_axis=0, concat_axis=0, tiled=True)  53 us
    all_to_all x4, waiting for transfers between devices, exchange(): return lax.all_to_all(a, axis, split_axis=0, concat_axis=0, tiled=True)  40.5 us
    unnamed x35, local copies, waits for them, and re-layouts  11.5 us
    ppermute x1, waiting for transfers between devices, layer(): down_other = lax.ppermute(down_half, 'gr', ring(GR, 1))  10.6 us
    ppermute x3, waiting for transfers between devices, along_x(): sent = {k: lax.ppermute(own, 'x', ring(X, k)) for k in (1, 3, 2)}  10.5 us
    ppermute x3, starting transfers between devices, along_x(): sent = {k: lax.ppermute(own, 'x', ring(X, k)) for k in (1, 3, 2)}  10.5 us
    ppermute x3, starting transfers between devices, layer(): lax.ppermute(column(j), 'y', ring(Y, j))  10.4 us
    ppermute x3, starting transfers between devices, layer(): cols.append(block if k == 0 else lax.ppermute(block, 'x', ring(X, k)))  10.4 us
  transfers between devices with their start and end apart: 20, of which 12 were waited for; matrix products, arithmetic and copies ran while one was open for 8% of the time, Pallas kernels for 0%

profile of v1, /device:TPU:2, one launch (start us, length us, event | category | flops | bytes accessed | tf_op | source)
XLA Modules:
  0.0 209.7 jit_solution(12785516966168526763)
XLA Ops:
  0.7 1.2 convert_element_type.76
  2.7 1.2 multiply_reduce_fusion
  4.2 1.2 convolution_convert_fusion
  5.4 0.9 pad_maximum_fusion.1
  6.4 15.5 %all-to-all-start = ((bf16[32,48,256]{2,1,0:T(8,128)(2,1)}), bf16[32,48,256]{2,1,0:T(8,128)(2,1)S(1)}, u32[]{:S(2)}, u32[]{:S(2)}) async-start(bf16[32,48,256]{2,1,0:T(8,128)(2,1)} %pad_maximum_fusion.1), calls=%async_computation | async-start | bytes 1572864 | tf_op jit(solution)/shard_map/all_to_all | solution.py:25
  22.2 4.9 %collective-permute-start = (bf16[8,32,256]{2,1,0:T(8,128)(2,1)S(1)}, bf16[8,32,256]{2,1,0:T(8,128)(2,1)S(1)}, u32[]{:S(2)}, u32[]{:S(2)}) collective-permute-start(bf16[8,32,256]{2,1,0:T(8,128)(2,1)S(1)} %pad_maximum_fusion.3), channel_id=1, source_target_pairs={{0,24},{8,0},{16,8},{24,16},{1,25},{9,1},{17,9},{25,17},{2,26},{10... | collective-permute-start | bytes 393224 | tf_op jit(solution)/shard_map/ppermute | solution.py:85
  27.2 2.8 %collective-permute-start.1 = (bf16[8,32,256]{2,1,0:T(8,128)(2,1)S(1)}, bf16[8,32,256]{2,1,0:T(8,128)(2,1)S(1)}, u32[]{:S(2)}, u32[]{:S(2)}) collective-permute-start(bf16[8,32,256]{2,1,0:T(8,128)(2,1)S(1)} %pad_maximum_fusion.4), channel_id=1, source_target_pairs={{0,16},{8,24},{16,0},{24,8},{1,17},{9,25},{17,1},{25,9},{2,18},{10... | collective-permute-start | bytes 393224 | tf_op jit(solution)/shard_map/ppermute | solution.py:85
  30.0 2.8 %collective-permute-start.2 = (bf16[8,32,256]{2,1,0:T(8,128)(2,1)S(1)}, bf16[8,32,256]{2,1,0:T(8,128)(2,1)S(1)}, u32[]{:S(2)}, u32[]{:S(2)}) collective-permute-start(bf16[8,32,256]{2,1,0:T(8,128)(2,1)S(1)} %pad_maximum_fusion.5), channel_id=1, source_target_pairs={{0,8},{8,16},{16,24},{24,0},{1,9},{9,17},{17,25},{25,1},{2,10},{10... | collective-permute-start | bytes 393224 | tf_op jit(solution)/shard_map/ppermute | solution.py:85
  32.8 0.9 collective-permute-done
  33.7 4.2 %collective-permute-done.1 = bf16[8,32,256]{2,1,0:T(8,128)(2,1)S(1)} collective-permute-done((bf16[8,32,256]{2,1,0:T(8,128)(2,1)S(1)}, bf16[8,32,256]{2,1,0:T(8,128)(2,1)S(1)}, u32[]{:S(2)}, u32[]{:S(2)}) %collective-permute-start.1) | collective-permute-done | bytes 131104 | tf_op jit(solution)/shard_map/ppermute | solution.py:85
  37.9 2.5 %collective-permute-done.2 = bf16[8,32,256]{2,1,0:T(8,128)(2,1)S(1)} collective-permute-done((bf16[8,32,256]{2,1,0:T(8,128)(2,1)S(1)}, bf16[8,32,256]{2,1,0:T(8,128)(2,1)S(1)}, u32[]{:S(2)}, u32[]{:S(2)}) %collective-permute-start.2) | collective-permute-done | bytes 131104 | tf_op jit(solution)/shard_map/ppermute | solution.py:85
  40.5 1.1 pad_maximum_fusion
  41.6 21.2 %all-to-all-done = bf16[32,48,256]{2,1,0:T(8,128)(2,1)S(1)} async-done(((bf16[32,48,256]{2,1,0:T(8,128)(2,1)}), bf16[32,48,256]{2,1,0:T(8,128)(2,1)S(1)}, u32[]{:S(2)}, u32[]{:S(2)}) %all-to-all-start) | async-done | bytes 786464 | tf_op jit(solution)/shard_map/all_to_all | solution.py:25
  62.9 7.7 %all-to-all-start.1 = ((bf16[16,128,256]{2,1,0:T(8,128)(2,1)}), bf16[16,128,256]{2,1,0:T(8,128)(2,1)S(1)}, u32[]{:S(2)}, u32[]{:S(2)}) async-start(bf16[16,128,256]{2,1,0:T(8,128)(2,1)} %pad_maximum_fusion), calls=%async_computation.1 | async-start | bytes 2097152 | tf_op jit(solution)/shard_map/all_to_all | solution.py:25
  70.7 3.4 %collective-permute-start.4 = (bf16[1024,256]{1,0:T(8,128)(2,1)S(1)}, bf16[1024,256]{1,0:T(8,128)(2,1)}, u32[]{:S(2)}, u32[]{:S(2)}) collective-permute-start(bf16[1024,256]{1,0:T(8,128)(2,1)S(1)} %bitcast.161), channel_id=1, source_target_pairs={{0,2},{2,4},{4,6},{6,0},{1,3},{3,5},{5,7},{7,1},{8,10},{10,12},{12... | collective-permute-start | bytes 1572872 | tf_op jit(solution)/shard_map/ppermute | solution.py:29
  74.1 3.0 %collective-permute-start.6 = (bf16[1024,256]{1,0:T(8,128)(2,1)S(1)}, bf16[1024,256]{1,0:T(8,128)(2,1)}, u32[]{:S(2)}, u32[]{:S(2)}) collective-permute-start(bf16[1024,256]{1,0:T(8,128)(2,1)S(1)} %bitcast.162), channel_id=1, source_target_pairs={{0,4},{2,6},{4,0},{6,2},{1,5},{3,7},{5,1},{7,3},{8,12},{10,14},{12... | collective-permute-start | bytes 1572872 | tf_op jit(solution)/shard_map/ppermute | solution.py:29
  77.1 4.1 %collective-permute-start.8 = (bf16[1024,256]{1,0:T(8,128)(2,1)S(1)}, bf16[1024,256]{1,0:T(8,128)(2,1)S(1)}, u32[]{:S(2)}, u32[]{:S(2)}) collective-permute-start(bf16[1024,256]{1,0:T(8,128)(2,1)S(1)} %bitcast.163), channel_id=1, source_target_pairs={{0,6},{2,0},{4,2},{6,4},{1,7},{3,1},{5,3},{7,5},{8,14},{10,8},{12,... | collective-permute-start | bytes 1572872 | tf_op jit(solution)/shard_map/ppermute | solution.py:29
  81.2 1.9 collective-permute-start.3
  83.1 4.4 %collective-permute-done.4 = bf16[1024,256]{1,0:T(8,128)(2,1)} collective-permute-done((bf16[1024,256]{1,0:T(8,128)(2,1)S(1)}, bf16[1024,256]{1,0:T(8,128)(2,1)}, u32[]{:S(2)}, u32[]{:S(2)}) %collective-permute-start.4) | collective-permute-done | bytes 524320 | tf_op jit(solution)/shard_map/ppermute | solution.py:29
  87.5 1.9 collective-permute-start.5
  89.5 2.9 %collective-permute-done.6 = bf16[1024,256]{1,0:T(8,128)(2,1)} collective-permute-done((bf16[1024,256]{1,0:T(8,128)(2,1)S(1)}, bf16[1024,256]{1,0:T(8,128)(2,1)}, u32[]{:S(2)}, u32[]{:S(2)}) %collective-permute-start.6) | collective-permute-done | bytes 524320 | tf_op jit(solution)/shard_map/ppermute | solution.py:29
  92.4 1.9 collective-permute-start.7
  95.1 3.3 %collective-permute-done.8 = bf16[1024,256]{1,0:T(8,128)(2,1)S(1)} collective-permute-done((bf16[1024,256]{1,0:T(8,128)(2,1)S(1)}, bf16[1024,256]{1,0:T(8,128)(2,1)S(1)}, u32[]{:S(2)}, u32[]{:S(2)}) %collective-permute-start.8) | collective-permute-done | bytes 524320 | tf_op jit(solution)/shard_map/ppermute | solution.py:29
  98.4 1.9 collective-permute-start.9
  100.4 1.9 constant_dynamic-update-slice_fusion.6
  102.3 1.9 constant_dynamic-update-slice_fusion.5
  104.2 1.9 constant_dynamic-update-slice_fusion.4
  106.1 1.9 constant_dynamic-update-slice_fusion.3
  109.8 0.9 constant_dynamic-update-slice_fusion
  110.6 5.6 %all-to-all-done.1 = bf16[16,128,256]{2,1,0:T(8,128)(2,1)S(1)} async-done(((bf16[16,128,256]{2,1,0:T(8,128)(2,1)}), bf16[16,128,256]{2,1,0:T(8,128)(2,1)S(1)}, u32[]{:S(2)}, u32[]{:S(2)}) %all-to-all-start.1) | async-done | bytes 1048608 | tf_op jit(solution)/shard_map/all_to_all | solution.py:25
  116.4 3.4 %fusion.56 = f32[1024,256]{1,0:T(8,128)S(1)} fusion(bf16[1024,2048]{1,0:T(8,128)(2,1)} %constant_dynamic-update-slice_fusion, bf16[2048,256]{1,0:T(8,128)(2,1)S(1)} %bitcast_dynamic-update-slice_fusion.10), kind=kOutput, calls=%fused_computation.144 | convolution fusion | flops 1073741824 | bytes 6291456 | tf_op jit(solution)/shard_map/dot_general | solution.py:104
  120.1 1.1 broadcast_in_dim.55
  121.2 4.8 %all-to-all-start.2 = ((bf16[4,1024,128]{2,1,0:T(8,128)(2,1)}), bf16[4,1024,128]{2,1,0:T(8,128)(2,1)S(1)}, u32[]{:S(2)}, u32[]{:S(2)}) async-start(bf16[4,1024,128]{2,1,0:T(8,128)(2,1)} %broadcast_in_dim.55), calls=%async_computation.2 | async-start | bytes 2097152 | tf_op jit(solution)/shard_map/all_to_all | solution.py:25
  126.0 9.5 %collective-permute-start.10 = (bf16[512,256]{1,0:T(8,128)(2,1)S(1)}, bf16[512,256]{1,0:T(8,128)(2,1)S(1)}, u32[]{:S(2)}, u32[]{:S(2)}) collective-permute-start(bf16[512,256]{1,0:T(8,128)(2,1)S(1)} %bitcast.167), channel_id=1, source_target_pairs={{0,256},{256,0},{1,257},{257,1},{2,258},{258,2},{3,259},{259,3},{4... | collective-permute-start | bytes 786440 | tf_op jit(solution)/shard_map/ppermute | solution.py:96
  135.5 1.9 collective-permute-start.11
  137.4 10.6 %collective-permute-done.10 = bf16[512,256]{1,0:T(8,128)(2,1)S(1)} collective-permute-done((bf16[512,256]{1,0:T(8,128)(2,1)S(1)}, bf16[512,256]{1,0:T(8,128)(2,1)S(1)}, u32[]{:S(2)}, u32[]{:S(2)}) %collective-permute-start.10) | collective-permute-done | bytes 262176 | tf_op jit(solution)/shard_map/ppermute | solution.py:96
  148.7 1.3 slice_bitcast_fusion.5
  150.0 1.2 fusion
  151.3 1.9 collective-permute-start.12
  153.3 24.9 %all-to-all-start.3 = ((bf16[32,32,256]{2,1,0:T(8,128)(2,1)}), bf16[32,32,256]{2,1,0:T(8,128)(2,1)S(1)}, u32[]{:S(2)}, u32[]{:S(2)}) async-start(bf16[32,32,256]{2,1,0:T(8,128)(2,1)} %bitcast.47), calls=%async_computation.3 | async-start | bytes 1048576 | tf_op jit(solution)/shard_map/all_to_all | solution.py:25
  178.3 2.2 %collective-permute-start.13 = (bf16[128,512]{1,0:T(8,128)(2,1)S(1)}, bf16[128,512]{1,0:T(8,128)(2,1)S(1)}, u32[]{:S(2)}, u32[]{:S(2)}) collective-permute-start(bf16[128,512]{1,0:T(8,128)(2,1)S(1)} %get-tuple-element.46), channel_id=1, source_target_pairs={{0,6},{2,0},{4,2},{6,4},{1,7},{3,1},{5,3},{7,5},{8,14},{10,8},{12,... | collective-permute-start | bytes 393224 | tf_op jit(solution)/shard_map/ppermute | solution.py:143
  180.5 1.0 slice_bitcast_fusion
  181.6 4.5 %collective-permute-start.14 = (bf16[128,512]{1,0:T(8,128)(2,1)S(1)}, bf16[128,512]{1,0:T(8,128)(2,1)S(1)}, u32[]{:S(2)}, u32[]{:S(2)}) collective-permute-start(bf16[128,512]{1,0:T(8,128)(2,1)S(1)} %get-tuple-element.47), channel_id=1, source_target_pairs={{0,4},{2,6},{4,0},{6,2},{1,5},{3,7},{5,1},{7,3},{8,12},{10,14},{12... | collective-permute-start | bytes 393224 | tf_op jit(solution)/shard_map/ppermute | solution.py:143
  186.1 3.7 %collective-permute-start.15 = (bf16[128,512]{1,0:T(8,128)(2,1)S(1)}, bf16[128,512]{1,0:T(8,128)(2,1)S(1)}, u32[]{:S(2)}, u32[]{:S(2)}) collective-permute-start(bf16[128,512]{1,0:T(8,128)(2,1)S(1)} %get-tuple-element.44), channel_id=1, source_target_pairs={{0,2},{2,4},{4,6},{6,0},{1,3},{3,5},{5,7},{7,1},{8,10},{10,12},{12... | collective-permute-start | bytes 393224 | tf_op jit(solution)/shard_map/ppermute | solution.py:143
  190.3 3.1 %collective-permute-done.15 = bf16[128,512]{1,0:T(8,128)(2,1)S(1)} collective-permute-done((bf16[128,512]{1,0:T(8,128)(2,1)S(1)}, bf16[128,512]{1,0:T(8,128)(2,1)S(1)}, u32[]{:S(2)}, u32[]{:S(2)}) %collective-permute-start.15) | collective-permute-done | bytes 131104 | tf_op jit(solution)/shard_map/ppermute | solution.py:143
  193.8 1.0 copy.40
  194.8 13.7 %all-to-all-done.3 = bf16[32,32,256]{2,1,0:T(8,128)(2,1)S(1)} async-done(((bf16[32,32,256]{2,1,0:T(8,128)(2,1)}), bf16[32,32,256]{2,1,0:T(8,128)(2,1)S(1)}, u32[]{:S(2)}, u32[]{:S(2)}) %all-to-all-start.3) | async-done | bytes 524320 | tf_op jit(solution)/shard_map/all_to_all | solution.py:25
  208.8 0.9 fusion.2
  (71 shorter events, 6.4 us)
Async XLA Ops:
  0.6 21.4 %copy-start = (f32[32,32,128]{2,1,0:T(8,128)S(1)}, f32[32,32,128]{2,1,0:T(8,128)}, u32[]{:S(2)}) copy-start(f32[32,32,128]{2,1,0:T(8,128)} %param.9) | copy-start | bytes 1572868
  0.6 21.4 %copy-start.4 = (f32[32]{0:T(128)S(1)}, f32[32]{0:T(128)}, u32[]{:S(2)}) copy-start(f32[32]{0:T(128)} %param.8) | copy-start | bytes 388
  0.7 21.4 %copy-start.1 = (f32[32,32,128]{2,1,0:T(8,128)S(1)}, f32[32,32,128]{2,1,0:T(8,128)}, u32[]{:S(2)}) copy-start(f32[32,32,128]{2,1,0:T(8,128)} %param.10) | copy-start | bytes 1572868
  6.4 56.5 %all-to-all-start = ((bf16[32,48,256]{2,1,0:T(8,128)(2,1)}), bf16[32,48,256]{2,1,0:T(8,128)(2,1)S(1)}, u32[]{:S(2)}, u32[]{:S(2)}) async-start(bf16[32,48,256]{2,1,0:T(8,128)(2,1)} %pad_maximum_fusion.1), calls=%async_computation | async-start | bytes 1572864 | tf_op jit(solution)/shard_map/all_to_all | solution.py:25
  22.2 11.4 %collective-permute-start = (bf16[8,32,256]{2,1,0:T(8,128)(2,1)S(1)}, bf16[8,32,256]{2,1,0:T(8,128)(2,1)S(1)}, u32[]{:S(2)}, u32[]{:S(2)}) collective-permute-start(bf16[8,32,256]{2,1,0:T(8,128)(2,1)S(1)} %pad_maximum_fusion.3), channel_id=1, source_target_pairs={{0,24},{8,0},{16,8},{24,16},{1,25},{9,1},{17,9},{25,17},{2,26},{10... | collective-permute-start | bytes 393224 | tf_op jit(solution)/shard_map/ppermute | solution.py:85
  27.2 10.7 %collective-permute-start.1 = (bf16[8,32,256]{2,1,0:T(8,128)(2,1)S(1)}, bf16[8,32,256]{2,1,0:T(8,128)(2,1)S(1)}, u32[]{:S(2)}, u32[]{:S(2)}) collective-permute-start(bf16[8,32,256]{2,1,0:T(8,128)(2,1)S(1)} %pad_maximum_fusion.4), channel_id=1, source_target_pairs={{0,16},{8,24},{16,0},{24,8},{1,17},{9,25},{17,1},{25,9},{2,18},{10... | collective-permute-start | bytes 393224 | tf_op jit(solution)/shard_map/ppermute | solution.py:85
  30.0 10.4 %collective-permute-start.2 = (bf16[8,32,256]{2,1,0:T(8,128)(2,1)S(1)}, bf16[8,32,256]{2,1,0:T(8,128)(2,1)S(1)}, u32[]{:S(2)}, u32[]{:S(2)}) collective-permute-start(bf16[8,32,256]{2,1,0:T(8,128)(2,1)S(1)} %pad_maximum_fusion.5), channel_id=1, source_target_pairs={{0,8},{8,16},{16,24},{24,0},{1,9},{9,17},{17,25},{25,1},{2,10},{10... | collective-permute-start | bytes 393224 | tf_op jit(solution)/shard_map/ppermute | solution.py:85
  62.9 53.3 %all-to-all-start.1 = ((bf16[16,128,256]{2,1,0:T(8,128)(2,1)}), bf16[16,128,256]{2,1,0:T(8,128)(2,1)S(1)}, u32[]{:S(2)}, u32[]{:S(2)}) async-start(bf16[16,128,256]{2,1,0:T(8,128)(2,1)} %pad_maximum_fusion), calls=%async_computation.1 | async-start | bytes 2097152 | tf_op jit(solution)/shard_map/all_to_all | solution.py:25
  70.7 16.8 %collective-permute-start.4 = (bf16[1024,256]{1,0:T(8,128)(2,1)S(1)}, bf16[1024,256]{1,0:T(8,128)(2,1)}, u32[]{:S(2)}, u32[]{:S(2)}) collective-permute-start(bf16[1024,256]{1,0:T(8,128)(2,1)S(1)} %bitcast.161), channel_id=1, source_target_pairs={{0,2},{2,4},{4,6},{6,0},{1,3},{3,5},{5,7},{7,1},{8,10},{10,12},{12... | collective-permute-start | bytes 1572872 | tf_op jit(solution)/shard_map/ppermute | solution.py:29
  74.1 18.3 %collective-permute-start.6 = (bf16[1024,256]{1,0:T(8,128)(2,1)S(1)}, bf16[1024,256]{1,0:T(8,128)(2,1)}, u32[]{:S(2)}, u32[]{:S(2)}) collective-permute-start(bf16[1024,256]{1,0:T(8,128)(2,1)S(1)} %bitcast.162), channel_id=1, source_target_pairs={{0,4},{2,6},{4,0},{6,2},{1,5},{3,7},{5,1},{7,3},{8,12},{10,14},{12... | collective-permute-start | bytes 1572872 | tf_op jit(solution)/shard_map/ppermute | solution.py:29
  77.1 21.3 %collective-permute-start.8 = (bf16[1024,256]{1,0:T(8,128)(2,1)S(1)}, bf16[1024,256]{1,0:T(8,128)(2,1)S(1)}, u32[]{:S(2)}, u32[]{:S(2)}) collective-permute-start(bf16[1024,256]{1,0:T(8,128)(2,1)S(1)} %bitcast.163), channel_id=1, source_target_pairs={{0,6},{2,0},{4,2},{6,4},{1,7},{3,1},{5,3},{7,5},{8,14},{10,8},{12,... | collective-permute-start | bytes 1572872 | tf_op jit(solution)/shard_map/ppermute | solution.py:29
  81.2 19.2 %collective-permute-start.3 = (bf16[1024,256]{1,0:T(8,128)(2,1)S(1)}, bf16[1024,256]{1,0:T(8,128)(2,1)}, u32[]{:S(2)}, u32[]{:S(2)}) collective-permute-start(bf16[1024,256]{1,0:T(8,128)(2,1)S(1)} %bitcast.164), channel_id=1, source_target_pairs={{0,1},{1,0},{2,3},{3,2},{4,5},{5,4},{6,7},{7,6},{8,9},{9,8},{10,11... | collective-permute-start | bytes 1572872 | tf_op jit(solution)/shard_map/ppermute | solution.py:34
  87.5 16.7 %collective-permute-start.5 = (bf16[1024,256]{1,0:T(8,128)(2,1)}, bf16[1024,256]{1,0:T(8,128)(2,1)}, u32[]{:S(2)}, u32[]{:S(2)}) collective-permute-start(bf16[1024,256]{1,0:T(8,128)(2,1)} %collective-permute-done.4), channel_id=1, source_target_pairs={{0,1},{1,0},{2,3},{3,2},{4,5},{5,4},{6,7},{7,6},{8,9},{9,8},{10,11... | collective-permute-start | bytes 1572872 | tf_op jit(solution)/shard_map/ppermute | solution.py:34
  92.4 15.7 %collective-permute-start.7 = (bf16[1024,256]{1,0:T(8,128)(2,1)}, bf16[1024,256]{1,0:T(8,128)(2,1)S(1)}, u32[]{:S(2)}, u32[]{:S(2)}) collective-permute-start(bf16[1024,256]{1,0:T(8,128)(2,1)} %collective-permute-done.6), channel_id=1, source_target_pairs={{0,1},{1,0},{2,3},{3,2},{4,5},{5,4},{6,7},{7,6},{8,9},{9,8},{10,11... | collective-permute-start | bytes 1572872 | tf_op jit(solution)/shard_map/ppermute | solution.py:34
  98.4 11.3 %collective-permute-start.9 = (bf16[1024,256]{1,0:T(8,128)(2,1)S(1)}, bf16[1024,256]{1,0:T(8,128)(2,1)S(1)}, u32[]{:S(2)}, u32[]{:S(2)}) collective-permute-start(bf16[1024,256]{1,0:T(8,128)(2,1)S(1)} %collective-permute-done.8), channel_id=1, source_target_pairs={{0,1},{1,0},{2,3},{3,2},{4,5},{5,4},{6,7},{7,6},{8,9},{9,8},{10,11... | collective-permute-start | bytes 1572872 | tf_op jit(solution)/shard_map/ppermute | solution.py:34
  121.2 14.3 %all-to-all-start.2 = ((bf16[4,1024,128]{2,1,0:T(8,128)(2,1)}), bf16[4,1024,128]{2,1,0:T(8,128)(2,1)S(1)}, u32[]{:S(2)}, u32[]{:S(2)}) async-start(bf16[4,1024,128]{2,1,0:T(8,128)(2,1)} %broadcast_in_dim.55), calls=%async_computation.2 | async-start | bytes 2097152 | tf_op jit(solution)/shard_map/all_to_all | solution.py:25
  126.0 22.0 %collective-permute-start.10 = (bf16[512,256]{1,0:T(8,128)(2,1)S(1)}, bf16[512,256]{1,0:T(8,128)(2,1)S(1)}, u32[]{:S(2)}, u32[]{:S(2)}) collective-permute-start(bf16[512,256]{1,0:T(8,128)(2,1)S(1)} %bitcast.167), channel_id=1, source_target_pairs={{0,256},{256,0},{1,257},{257,1},{2,258},{258,2},{3,259},{259,3},{4... | collective-permute-start | bytes 786440 | tf_op jit(solution)/shard_map/ppermute | solution.py:96
  135.5 13.2 %collective-permute-start.11 = (bf16[4,1024,128]{2,1,0:T(8,128)(2,1)S(1)}, bf16[4,1024,128]{2,1,0:T(8,128)(2,1)}, u32[]{:S(2)}, u32[]{:S(2)}) collective-permute-start(bf16[4,1024,128]{2,1,0:T(8,128)(2,1)S(1)} %all-to-all-done.2), channel_id=1, source_target_pairs={{0,1},{1,0},{2,3},{3,2},{4,5},{5,4},{6,7},{7,6},{8,9},{9,8},{10,11... | collective-permute-start | bytes 3145736 | tf_op jit(solution)/shard_map/ppermute | solution.py:34
  148.7 4.5 %copy-start.2 = (s32[128,4]{0,1:T(4,128)S(1)}, s32[128,4]{0,1:T(4,128)}, u32[]{:S(2)}) copy-start(s32[128,4]{0,1:T(4,128)} %param.12) | copy-start | bytes 6148
  148.7 4.5 %copy-start.3 = (f32[128,4]{0,1:T(4,128)S(1)}, f32[128,4]{0,1:T(4,128)}, u32[]{:S(2)}) copy-start(f32[128,4]{0,1:T(4,128)} %param.13) | copy-start | bytes 6148
  151.3 26.9 %collective-permute-start.12 = (bf16[4,128,256]{2,1,0:T(8,128)(2,1)S(1)}, bf16[4,128,256]{2,1,0:T(8,128)(2,1)S(1)}, u32[]{:S(2)}, u32[]{:S(2)}) collective-permute-start(bf16[4,128,256]{2,1,0:T(8,128)(2,1)S(1)} %dynamic-slice_bitcast_fusion.1), channel_id=1, source_target_pairs={{0,1},{1,0},{2,3},{3,2},{4,5},{5,4},{6,7},{7,6},{8,9},{9,8},{10,11... | collective-permute-start | bytes 786440 | tf_op jit(solution)/shard_map/ppermute | solution.py:136
  153.3 55.2 %all-to-all-start.3 = ((bf16[32,32,256]{2,1,0:T(8,128)(2,1)}), bf16[32,32,256]{2,1,0:T(8,128)(2,1)S(1)}, u32[]{:S(2)}, u32[]{:S(2)}) async-start(bf16[32,32,256]{2,1,0:T(8,128)(2,1)} %bitcast.47), calls=%async_computation.3 | async-start | bytes 1048576 | tf_op jit(solution)/shard_map/all_to_all | solution.py:25
  178.3 11.5 %collective-permute-start.13 = (bf16[128,512]{1,0:T(8,128)(2,1)S(1)}, bf16[128,512]{1,0:T(8,128)(2,1)S(1)}, u32[]{:S(2)}, u32[]{:S(2)}) collective-permute-start(bf16[128,512]{1,0:T(8,128)(2,1)S(1)} %get-tuple-element.46), channel_id=1, source_target_pairs={{0,6},{2,0},{4,2},{6,4},{1,7},{3,1},{5,3},{7,5},{8,14},{10,8},{12,... | collective-permute-start | bytes 393224 | tf_op jit(solution)/shard_map/ppermute | solution.py:143
  181.6 8.7 %collective-permute-start.14 = (bf16[128,512]{1,0:T(8,128)(2,1)S(1)}, bf16[128,512]{1,0:T(8,128)(2,1)S(1)}, u32[]{:S(2)}, u32[]{:S(2)}) collective-permute-start(bf16[128,512]{1,0:T(8,128)(2,1)S(1)} %get-tuple-element.47), channel_id=1, source_target_pairs={{0,4},{2,6},{4,0},{6,2},{1,5},{3,7},{5,1},{7,3},{8,12},{10,14},{12... | collective-permute-start | bytes 393224 | tf_op jit(solution)/shard_map/ppermute | solution.py:143
  186.1 7.3 %collective-permute-start.15 = (bf16[128,512]{1,0:T(8,128)(2,1)S(1)}, bf16[128,512]{1,0:T(8,128)(2,1)S(1)}, u32[]{:S(2)}, u32[]{:S(2)}) collective-permute-start(bf16[128,512]{1,0:T(8,128)(2,1)S(1)} %get-tuple-element.44), channel_id=1, source_target_pairs={{0,2},{2,4},{4,6},{6,0},{1,3},{3,5},{5,7},{7,1},{8,10},{10,12},{12... | collective-permute-start | bytes 393224 | tf_op jit(solution)/shard_map/ppermute | solution.py:143

commit v2 on v0

--- a/solution.py
+++ b/solution.py
@@ -3,6 +3,7 @@
 from jax import lax
 from jax.sharding import Mesh
 from jax.sharding import PartitionSpec as P
+
 
 CAP = 32
 CLAMP_LIMIT = 7.0
@@ -45,7 +46,7 @@
     n_tok, width = tokens.shape
     part = width // (X * C)
     n_exp = ZL * Y
-    n_up, ff = gate_train.shape[1], gate_train.shape[2]
+    n_up, ff, n_down = gate_train.shape[1], gate_train.shape[2], down_train.shape[1]
 
     hit = routes.T[None, :, :] == jnp.arange(n_exp, dtype=jnp.int32)[:, None, None]
     member = jnp.any(hit, axis=1)
@@ -73,23 +74,24 @@
             cut = a.reshape(ZL, Y, a.shape[1], a.shape[2])
             return lax.dynamic_index_in_dim(cut, at, 1, keepdims=False)
 
-        return jnp.concatenate(
+        both = jnp.concatenate(
             [(gain * take(gate_train)).astype(BF), (gain * take(up_train)).astype(BF)], axis=2
         )
+        return jnp.concatenate([both, take(down_train).astype(BF)], axis=1)
 
     got = [column(0)] + [lax.ppermute(column(j), "y", ring(Y, j)) for j in range(1, Y)]
     by_offset = jnp.stack([got[(-j) % Y] for j in range(Y)], axis=1)
     by_source = lax.dynamic_slice_in_dim(
         jnp.concatenate([by_offset, by_offset], axis=1), (Y - iy) % Y, Y, 1
-    ).reshape(ZL, Y * n_up, 2 * ff)
-    by_source, arrived = lax.optimization_barrier((by_source, arrived))
-    served = exchange(jnp.concatenate([by_source] * GR, axis=0), ("gr", "zl"))
+    )
+    down_part = by_source[:, :, n_up:].reshape(ZL, Y * n_down, part)
+    down_twice = jnp.concatenate([down_part] * GR, axis=0)
+    by_source = by_source[:, :, :n_up].reshape(ZL, Y * n_up, 2 * ff)
+    twice, arrived = lax.optimization_barrier((jnp.concatenate([by_source] * GR, axis=0), arrived))
+    served = exchange(twice, ("gr", "zl"))
     pieces = gather_tp(arrived)
     rows = jnp.concatenate([a for pair in pieces for a in pair], axis=1)
 
-    down_local = down_train.astype(BF)
-    down_local, served = lax.optimization_barrier((down_local, served))
-    down_cols = exchange(jnp.concatenate([down_local] * GR, axis=0), ("gr",) + FS)
     served = served.reshape(width, 2 * ff)
     gate_weight = served[None, :, :ff]
     up_weight = served[None, :, ff:]
@@ -103,11 +105,14 @@
         * clipped
         * jax.nn.sigmoid(SLOPE_ALPHA * clipped)
     ).astype(BF)
+    down_twice, hidden = lax.optimization_barrier((down_twice, hidden))
+    down_cols = exchange(down_twice, ("gr", "zl"))
     pieces = gather_tp(hidden)
     hidden_all = jnp.concatenate([a for pair in pieces for a in pair], axis=1)
 
     down_blocks = down_cols.reshape(X, C, ff, part)
     total = jnp.dot(hidden_all, relative(down_blocks, ix, ic), preferred_element_type=F32).astype(BF)
+    total, down_blocks = lax.optimization_barrier((total, down_blocks))
     result = exchange(total.reshape(n_exp, CAP, part), FS)
 
     kept = lax.dynamic_index_in_dim(down_blocks, ic, 1, keepdims=False)

time: 199 us -> 196 us (0.985)
  starting transfers between devices: 100 us -> 96.3 us
  local copies, waits for them, and re-layouts: 18.1 us -> 21.3 us
    all_to_all x4, starting transfers between devices: 45.7 us -> 39.8 us  [exchange(): return lax.all_to_all(a, axis, split_axis=0, concat_axis=0, tiled=True)]
    ppermute x3, waiting for transfers between devices: 6.42 us -> 8.59 us  [layer(): lax.ppermute(column(j), 'y', ring(Y, j))]
    ppermute x3, starting transfers between devices: 10.6 us -> 12.6 us  [layer(): lax.ppermute(column(j), 'y', ring(Y, j))]
    unnamed x44 -> x47, local copies, waits for them, and re-layouts: 14.9 us -> 16.9 us
  transfers between devices with their start and end apart: 25 -> 25, of which waited for: 14 -> 13; matrix products, arithmetic and copies ran while one was open for 14% -> 13% of each run, Pallas kernels for 0% -> 0%
where the time goes in v2:
time: 196 us; the launch traced here: 194 us
  starting transfers between devices  96.3 us (49%)
  waiting for transfers between devices  61.1 us (31%)
  local copies, waits for them, and re-layouts  21.3 us (11%)
  matrix products  9.05 us (5%)
  other arithmetic  4.94 us (3%)
    all_to_all x4, starting transfers between devices, exchange(): return lax.all_to_all(a, axis, split_axis=0, concat_axis=0, tiled=True)  39.8 us
    all_to_all x4, waiting for transfers between devices, exchange(): return lax.all_to_all(a, axis, split_axis=0, concat_axis=0, tiled=True)  33.1 us
    ppermute x6, starting transfers between devices, gather_tp(): mine = [own] + [lax.ppermute(own, 'x', ring(X, k)) for k in (1, 3, 2)]  17.3 us
    unnamed x47, local copies, waits for them, and re-layouts  16.9 us
    ppermute x8, starting transfers between devices, gather_tp(): other = [lax.ppermute(a, 'c', ring(C, 1)) for a in mine]  15.8 us
    ppermute x6, waiting for transfers between devices, gather_tp(): mine = [own] + [lax.ppermute(own, 'x', ring(X, k)) for k in (1, 3, 2)]  14.7 us
    ppermute x3, starting transfers between devices, layer(): lax.ppermute(column(j), 'y', ring(Y, j))  12.6 us
    ppermute x3, starting transfers between devices, layer(): cols.append(block if k == 0 else lax.ppermute(block, 'x', ring(X, k)))  8.96 us
  transfers between devices with their start and end apart: 25, of which 13 were waited for; matrix products, arithmetic and copies ran while one was open for 13% of the time, Pallas kernels for 0%

profile of v2, /device:TPU:6, one launch (start us, length us, event | category | flops | bytes accessed | tf_op | source)
XLA Modules:
  0.0 194.2 jit_solution(10717942434853500557)
XLA Ops:
  0.7 1.2 fusion.35
  1.9 1.5 fusion.23
  3.4 4.9 %collective-permute-start = (bf16[8,48,256]{2,1,0:T(8,128)(2,1)S(1)}, bf16[8,48,256]{2,1,0:T(8,128)(2,1)S(1)}, u32[]{:S(2)}, u32[]{:S(2)}) collective-permute-start(bf16[8,48,256]{2,1,0:T(8,128)(2,1)S(1)} %pad_maximum_fusion.2), channel_id=1, source_target_pairs={{0,24},{8,0},{16,8},{24,16},{1,25},{9,1},{17,9},{25,17},{2,26},{10... | collective-permute-start | bytes 589832 | tf_op jit(solution)/shard_map/ppermute | solution.py:82
  9.0 1.2 convolution_convert_fusion.1
  10.2 13.1 %all-to-all-start = ((bf16[32,32,256]{2,1,0:T(8,128)(2,1)}), bf16[32,32,256]{2,1,0:T(8,128)(2,1)S(1)}, u32[]{:S(2)}, u32[]{:S(2)}) async-start(bf16[32,32,256]{2,1,0:T(8,128)(2,1)} %bitcast.30), calls=%async_computation | async-start | bytes 1048576 | tf_op jit(solution)/shard_map/all_to_all | solution.py:25
  23.3 5.2 %collective-permute-start.1 = (bf16[8,48,256]{2,1,0:T(8,128)(2,1)S(1)}, bf16[8,48,256]{2,1,0:T(8,128)(2,1)S(1)}, u32[]{:S(2)}, u32[]{:S(2)}) collective-permute-start(bf16[8,48,256]{2,1,0:T(8,128)(2,1)S(1)} %pad_maximum_fusion.3), channel_id=1, source_target_pairs={{0,16},{8,24},{16,0},{24,8},{1,17},{9,25},{17,1},{25,9},{2,18},{10... | collective-permute-start | bytes 589832 | tf_op jit(solution)/shard_map/ppermute | solution.py:82
  29.2 2.5 %collective-permute-start.2 = (bf16[8,48,256]{2,1,0:T(8,128)(2,1)}, bf16[8,48,256]{2,1,0:T(8,128)(2,1)S(1)}, u32[]{:S(2)}, u32[]{:S(2)}) collective-permute-start(bf16[8,48,256]{2,1,0:T(8,128)(2,1)} %pad_maximum_fusion.4), channel_id=1, source_target_pairs={{0,8},{8,16},{16,24},{24,0},{1,9},{9,17},{17,25},{25,1},{2,10},{10... | collective-permute-start | bytes 589832 | tf_op jit(solution)/shard_map/ppermute | solution.py:82
  31.8 4.3 %collective-permute-done.1 = bf16[8,48,256]{2,1,0:T(8,128)(2,1)S(1)} collective-permute-done((bf16[8,48,256]{2,1,0:T(8,128)(2,1)S(1)}, bf16[8,48,256]{2,1,0:T(8,128)(2,1)S(1)}, u32[]{:S(2)}, u32[]{:S(2)}) %collective-permute-start.1) | collective-permute-done | bytes 196640 | tf_op jit(solution)/shard_map/ppermute | solution.py:82
  36.1 4.3 %collective-permute-done.2 = bf16[8,48,256]{2,1,0:T(8,128)(2,1)S(1)} collective-permute-done((bf16[8,48,256]{2,1,0:T(8,128)(2,1)}, bf16[8,48,256]{2,1,0:T(8,128)(2,1)S(1)}, u32[]{:S(2)}, u32[]{:S(2)}) %collective-permute-start.2) | collective-permute-done | bytes 196640 | tf_op jit(solution)/shard_map/ppermute | solution.py:82
  40.6 1.1 pad_maximum_fusion
  41.7 11.0 %all-to-all-done = bf16[32,32,256]{2,1,0:T(8,128)(2,1)S(1)} async-done(((bf16[32,32,256]{2,1,0:T(8,128)(2,1)}), bf16[32,32,256]{2,1,0:T(8,128)(2,1)S(1)}, u32[]{:S(2)}, u32[]{:S(2)}) %all-to-all-start) | async-done | bytes 524320 | tf_op jit(solution)/shard_map/all_to_all | solution.py:25
  52.7 7.7 %all-to-all-start.1 = ((bf16[16,128,256]{2,1,0:T(8,128)(2,1)}), bf16[16,128,256]{2,1,0:T(8,128)(2,1)S(1)}, u32[]{:S(2)}, u32[]{:S(2)}) async-start(bf16[16,128,256]{2,1,0:T(8,128)(2,1)} %pad_maximum_fusion), calls=%async_computation.1 | async-start | bytes 2097152 | tf_op jit(solution)/shard_map/all_to_all | solution.py:25
  60.3 2.4 %collective-permute-start.4 = (bf16[1024,256]{1,0:T(8,128)(2,1)S(1)}, bf16[1024,256]{1,0:T(8,128)(2,1)}, u32[]{:S(2)}, u32[]{:S(2)}) collective-permute-start(bf16[1024,256]{1,0:T(8,128)(2,1)S(1)} %bitcast.190), channel_id=1, source_target_pairs={{0,2},{2,4},{4,6},{6,0},{1,3},{3,5},{5,7},{7,1},{8,10},{10,12},{12... | collective-permute-start | bytes 1572872 | tf_op jit(solution)/shard_map/ppermute | solution.py:29
  62.8 4.3 %collective-permute-start.6 = (bf16[1024,256]{1,0:T(8,128)(2,1)S(1)}, bf16[1024,256]{1,0:T(8,128)(2,1)}, u32[]{:S(2)}, u32[]{:S(2)}) collective-permute-start(bf16[1024,256]{1,0:T(8,128)(2,1)S(1)} %bitcast.191), channel_id=1, source_target_pairs={{0,4},{2,6},{4,0},{6,2},{1,5},{3,7},{5,1},{7,3},{8,12},{10,14},{12... | collective-permute-start | bytes 1572872 | tf_op jit(solution)/shard_map/ppermute | solution.py:29
  67.1 1.9 collective-permute-start.8
  69.0 1.9 collective-permute-start.3
  71.0 6.1 %collective-permute-done.4 = bf16[1024,256]{1,0:T(8,128)(2,1)} collective-permute-done((bf16[1024,256]{1,0:T(8,128)(2,1)S(1)}, bf16[1024,256]{1,0:T(8,128)(2,1)}, u32[]{:S(2)}, u32[]{:S(2)}) %collective-permute-start.4) | collective-permute-done | bytes 524320 | tf_op jit(solution)/shard_map/ppermute | solution.py:29
  77.1 1.9 collective-permute-start.5
  79.9 1.2 collective-permute-done.6
  81.1 1.9 collective-permute-start.7
  83.9 4.1 %collective-permute-done.8 = bf16[1024,256]{1,0:T(8,128)(2,1)} collective-permute-done((bf16[1024,256]{1,0:T(8,128)(2,1)S(1)}, bf16[1024,256]{1,0:T(8,128)(2,1)}, u32[]{:S(2)}, u32[]{:S(2)}) %collective-permute-start.8) | collective-permute-done | bytes 524320 | tf_op jit(solution)/shard_map/ppermute | solution.py:29
  88.0 1.9 collective-permute-start.9
  89.9 1.9 constant_dynamic-update-slice_fusion.6
  91.9 1.9 constant_dynamic-update-slice_fusion.5
  94.6 1.9 constant_dynamic-update-slice_fusion.3
  97.4 1.9 constant_dynamic-update-slice_fusion.1
  100.2 6.4 %all-to-all-done.1 = bf16[16,128,256]{2,1,0:T(8,128)(2,1)S(1)} async-done(((bf16[16,128,256]{2,1,0:T(8,128)(2,1)}), bf16[16,128,256]{2,1,0:T(8,128)(2,1)S(1)}, u32[]{:S(2)}, u32[]{:S(2)}) %all-to-all-start.1) | async-done | bytes 1048608 | tf_op jit(solution)/shard_map/all_to_all | solution.py:25
  106.8 3.4 %fusion.42 = f32[1024,256]{1,0:T(8,128)S(1)} fusion(bf16[1024,2048]{1,0:T(8,128)(2,1)} %constant_dynamic-update-slice_fusion, bf16[2048,256]{1,0:T(8,128)(2,1)S(1)} %bitcast_dynamic-update-slice_fusion.12), kind=kOutput, calls=%fused_computation.138 | convolution fusion | flops 1073741824 | bytes 6291456 | tf_op jit(solution)/shard_map/dot_general | solution.py:99
  110.5 9.0 %all-to-all-start.2 = ((bf16[16,64,256]{2,1,0:T(8,128)(2,1)}), bf16[16,64,256]{2,1,0:T(8,128)(2,1)S(1)}, u32[]{:S(2)}, u32[]{:S(2)}) async-start(bf16[16,64,256]{2,1,0:T(8,128)(2,1)} %pad_maximum_fusion.1), calls=%async_computation.2 | async-start | bytes 1048576 | tf_op jit(solution)/shard_map/all_to_all | solution.py:25
  119.5 2.4 %collective-permute-start.11 = (bf16[1024,128]{1,0:T(8,128)(2,1)S(1)}, bf16[1024,128]{1,0:T(8,128)(2,1)S(1)}, u32[]{:S(2)}, u32[]{:S(2)}) collective-permute-start(bf16[1024,128]{1,0:T(8,128)(2,1)S(1)} %fusion.7), channel_id=1, source_target_pairs={{0,2},{2,4},{4,6},{6,0},{1,3},{3,5},{5,7},{7,1},{8,10},{10,12},{12... | collective-permute-start | bytes 786440 | tf_op jit(solution)/shard_map/ppermute | solution.py:29
  121.9 4.3 %collective-permute-start.13 = (bf16[1024,128]{1,0:T(8,128)(2,1)S(1)}, bf16[1024,128]{1,0:T(8,128)(2,1)S(1)}, u32[]{:S(2)}, u32[]{:S(2)}) collective-permute-start(bf16[1024,128]{1,0:T(8,128)(2,1)S(1)} %fusion.7), channel_id=1, source_target_pairs={{0,4},{2,6},{4,0},{6,2},{1,5},{3,7},{5,1},{7,3},{8,12},{10,14},{12... | collective-permute-start | bytes 786440 | tf_op jit(solution)/shard_map/ppermute | solution.py:29
  126.2 1.9 collective-permute-start.10
  128.2 1.9 collective-permute-start.15
  130.6 1.9 %collective-permute-start.12 = (bf16[1024,128]{1,0:T(8,128)(2,1)S(1)}, bf16[1024,128]{1,0:T(8,128)(2,1)S(1)}, u32[]{:S(2)}, u32[]{:S(2)}) collective-permute-start(bf16[1024,128]{1,0:T(8,128)(2,1)S(1)} %collective-permute-done.11), channel_id=1, source_target_pairs={{0,1},{1,0},{2,3},{3,2},{4,5},{5,4},{6,7},{7,6},{8,9},{9,8},{10,11... | collective-permute-start | bytes 786440 | tf_op jit(solution)/shard_map/ppermute | solution.py:31
  133.3 2.4 %collective-permute-start.14 = (bf16[1024,128]{1,0:T(8,128)(2,1)S(1)}, bf16[1024,128]{1,0:T(8,128)(2,1)S(1)}, u32[]{:S(2)}, u32[]{:S(2)}) collective-permute-start(bf16[1024,128]{1,0:T(8,128)(2,1)S(1)} %collective-permute-done.13), channel_id=1, source_target_pairs={{0,1},{1,0},{2,3},{3,2},{4,5},{5,4},{6,7},{7,6},{8,9},{9,8},{10,11... | collective-permute-start | bytes 786440 | tf_op jit(solution)/shard_map/ppermute | solution.py:31
  137.1 2.8 %collective-permute-done.15 = bf16[1024,128]{1,0:T(8,128)(2,1)S(1)} collective-permute-done((bf16[1024,128]{1,0:T(8,128)(2,1)S(1)}, bf16[1024,128]{1,0:T(8,128)(2,1)S(1)}, u32[]{:S(2)}, u32[]{:S(2)}) %collective-permute-start.15) | collective-permute-done | bytes 262176 | tf_op jit(solution)/shard_map/ppermute | solution.py:29
  140.0 1.9 collective-permute-start.16
  145.7 2.2 %all-to-all-done.2 = bf16[16,64,256]{2,1,0:T(8,128)(2,1)S(1)} async-done(((bf16[16,64,256]{2,1,0:T(8,128)(2,1)}), bf16[16,64,256]{2,1,0:T(8,128)(2,1)S(1)}, u32[]{:S(2)}, u32[]{:S(2)}) %all-to-all-start.2) | async-done | bytes 524320 | tf_op jit(solution)/shard_map/all_to_all | solution.py:25
  148.0 3.1 %convolution_convert_fusion = bf16[1024,256]{1,0:T(8,128)(2,1)} fusion(bf16[1024,1024]{1,0:T(8,128)(2,1)} %constant_dynamic-update-slice_fusion.8, bf16[1024,256]{1,0:T(8,128)(2,1)S(1)} %constant_dynamic-update-slice_fusion.16), kind=kOutput, calls=%fused_computation | convolution fusion | flops 537133056 | bytes 3145728 | tf_op jit(solution)/shard_map/dot_general | solution.py:114
  151.2 1.9 collective-permute-start.17
  153.2 10.0 %all-to-all-start.3 = ((bf16[32,32,256]{2,1,0:T(8,128)(2,1)}), bf16[32,32,256]{2,1,0:T(8,128)(2,1)S(1)}, u32[]{:S(2)}, u32[]{:S(2)}) async-start(bf16[32,32,256]{2,1,0:T(8,128)(2,1)} %bitcast.50), calls=%async_computation.3 | async-start | bytes 1048576 | tf_op jit(solution)/shard_map/all_to_all | solution.py:25
  163.3 1.9 collective-permute-start.18
  165.2 1.0 slice_bitcast_fusion
  166.3 3.9 %collective-permute-start.19 = (bf16[128,512]{1,0:T(8,128)(2,1)S(1)}, bf16[128,512]{1,0:T(8,128)(2,1)S(1)}, u32[]{:S(2)}, u32[]{:S(2)}) collective-permute-start(bf16[128,512]{1,0:T(8,128)(2,1)S(1)} %get-tuple-element.39), channel_id=1, source_target_pairs={{0,4},{2,6},{4,0},{6,2},{1,5},{3,7},{5,1},{7,3},{8,12},{10,14},{12... | collective-permute-start | bytes 393224 | tf_op jit(solution)/shard_map/ppermute | solution.py:127
  170.2 3.1 %collective-permute-start.20 = (bf16[128,512]{1,0:T(8,128)(2,1)S(1)}, bf16[128,512]{1,0:T(8,128)(2,1)S(1)}, u32[]{:S(2)}, u32[]{:S(2)}) collective-permute-start(bf16[128,512]{1,0:T(8,128)(2,1)S(1)} %get-tuple-element.36), channel_id=1, source_target_pairs={{0,2},{2,4},{4,6},{6,0},{1,3},{3,5},{5,7},{7,1},{8,10},{10,12},{12... | collective-permute-start | bytes 393224 | tf_op jit(solution)/shard_map/ppermute | solution.py:127
  173.4 1.4 collective-permute-done.19
  174.8 3.2 %collective-permute-done.20 = bf16[128,512]{1,0:T(8,128)(2,1)S(1)} collective-permute-done((bf16[128,512]{1,0:T(8,128)(2,1)S(1)}, bf16[128,512]{1,0:T(8,128)(2,1)S(1)}, u32[]{:S(2)}, u32[]{:S(2)}) %collective-permute-start.20) | collective-permute-done | bytes 131104 | tf_op jit(solution)/shard_map/ppermute | solution.py:127
  179.4 13.6 %all-to-all-done.3 = bf16[32,32,256]{2,1,0:T(8,128)(2,1)S(1)} async-done(((bf16[32,32,256]{2,1,0:T(8,128)(2,1)}), bf16[32,32,256]{2,1,0:T(8,128)(2,1)S(1)}, u32[]{:S(2)}, u32[]{:S(2)}) %all-to-all-start.3) | async-done | bytes 524320 | tf_op jit(solution)/shard_map/all_to_all | solution.py:25
  (87 shorter events, 15.6 us)
Async XLA Ops:
  0.6 7.8 %copy-start.1 = (s32[128,4]{0,1:T(4,128)S(1)}, s32[128,4]{0,1:T(4,128)}, u32[]{:S(2)}) copy-start(s32[128,4]{0,1:T(4,128)} %param.12) | copy-start | bytes 6148
  0.6 8.0 %copy-start = (bf16[128,2048]{1,0:T(8,128)(2,1)S(1)}, bf16[128,2048]{1,0:T(8,128)(2,1)}, u32[]{:S(2)}) copy-start(bf16[128,2048]{1,0:T(8,128)(2,1)} %param.7) | copy-start | bytes 1572868
  3.4 28.3 %collective-permute-start = (bf16[8,48,256]{2,1,0:T(8,128)(2,1)S(1)}, bf16[8,48,256]{2,1,0:T(8,128)(2,1)S(1)}, u32[]{:S(2)}, u32[]{:S(2)}) collective-permute-start(bf16[8,48,256]{2,1,0:T(8,128)(2,1)S(1)} %pad_maximum_fusion.2), channel_id=1, source_target_pairs={{0,24},{8,0},{16,8},{24,16},{1,25},{9,1},{17,9},{25,17},{2,26},{10... | collective-permute-start | bytes 589832 | tf_op jit(solution)/shard_map/ppermute | solution.py:82
  10.2 42.5 %all-to-all-start = ((bf16[32,32,256]{2,1,0:T(8,128)(2,1)}), bf16[32,32,256]{2,1,0:T(8,128)(2,1)S(1)}, u32[]{:S(2)}, u32[]{:S(2)}) async-start(bf16[32,32,256]{2,1,0:T(8,128)(2,1)} %bitcast.30), calls=%async_computation | async-start | bytes 1048576 | tf_op jit(solution)/shard_map/all_to_all | solution.py:25
  23.3 12.7 %collective-permute-start.1 = (bf16[8,48,256]{2,1,0:T(8,128)(2,1)S(1)}, bf16[8,48,256]{2,1,0:T(8,128)(2,1)S(1)}, u32[]{:S(2)}, u32[]{:S(2)}) collective-permute-start(bf16[8,48,256]{2,1,0:T(8,128)(2,1)S(1)} %pad_maximum_fusion.3), channel_id=1, source_target_pairs={{0,16},{8,24},{16,0},{24,8},{1,17},{9,25},{17,1},{25,9},{2,18},{10... | collective-permute-start | bytes 589832 | tf_op jit(solution)/shard_map/ppermute | solution.py:82
  29.2 11.2 %collective-permute-start.2 = (bf16[8,48,256]{2,1,0:T(8,128)(2,1)}, bf16[8,48,256]{2,1,0:T(8,128)(2,1)S(1)}, u32[]{:S(2)}, u32[]{:S(2)}) collective-permute-start(bf16[8,48,256]{2,1,0:T(8,128)(2,1)} %pad_maximum_fusion.4), channel_id=1, source_target_pairs={{0,8},{8,16},{16,24},{24,0},{1,9},{9,17},{17,25},{25,1},{2,10},{10... | collective-permute-start | bytes 589832 | tf_op jit(solution)/shard_map/ppermute | solution.py:82
  52.7 54.0 %all-to-all-start.1 = ((bf16[16,128,256]{2,1,0:T(8,128)(2,1)}), bf16[16,128,256]{2,1,0:T(8,128)(2,1)S(1)}, u32[]{:S(2)}, u32[]{:S(2)}) async-start(bf16[16,128,256]{2,1,0:T(8,128)(2,1)} %pad_maximum_fusion), calls=%async_computation.1 | async-start | bytes 2097152 | tf_op jit(solution)/shard_map/all_to_all | solution.py:25
  60.3 16.8 %collective-permute-start.4 = (bf16[1024,256]{1,0:T(8,128)(2,1)S(1)}, bf16[1024,256]{1,0:T(8,128)(2,1)}, u32[]{:S(2)}, u32[]{:S(2)}) collective-permute-start(bf16[1024,256]{1,0:T(8,128)(2,1)S(1)} %bitcast.190), channel_id=1, source_target_pairs={{0,2},{2,4},{4,6},{6,0},{1,3},{3,5},{5,7},{7,1},{8,10},{10,12},{12... | collective-permute-start | bytes 1572872 | tf_op jit(solution)/shard_map/ppermute | solution.py:29
  62.8 18.3 %collective-permute-start.6 = (bf16[1024,256]{1,0:T(8,128)(2,1)S(1)}, bf16[1024,256]{1,0:T(8,128)(2,1)}, u32[]{:S(2)}, u32[]{:S(2)}) collective-permute-start(bf16[1024,256]{1,0:T(8,128)(2,1)S(1)} %bitcast.191), channel_id=1, source_target_pairs={{0,4},{2,6},{4,0},{6,2},{1,5},{3,7},{5,1},{7,3},{8,12},{10,14},{12... | collective-permute-start | bytes 1572872 | tf_op jit(solution)/shard_map/ppermute | solution.py:29
  67.1 20.9 %collective-permute-start.8 = (bf16[1024,256]{1,0:T(8,128)(2,1)S(1)}, bf16[1024,256]{1,0:T(8,128)(2,1)}, u32[]{:S(2)}, u32[]{:S(2)}) collective-permute-start(bf16[1024,256]{1,0:T(8,128)(2,1)S(1)} %bitcast.192), channel_id=1, source_target_pairs={{0,6},{2,0},{4,2},{6,4},{1,7},{3,1},{5,3},{7,5},{8,14},{10,8},{12,... | collective-permute-start | bytes 1572872 | tf_op jit(solution)/shard_map/ppermute | solution.py:29
  69.0 20.9 %collective-permute-start.3 = (bf16[1024,256]{1,0:T(8,128)(2,1)S(1)}, bf16[1024,256]{1,0:T(8,128)(2,1)}, u32[]{:S(2)}, u32[]{:S(2)}) collective-permute-start(bf16[1024,256]{1,0:T(8,128)(2,1)S(1)} %bitcast.193), channel_id=1, source_target_pairs={{0,1},{1,0},{2,3},{3,2},{4,5},{5,4},{6,7},{7,6},{8,9},{9,8},{10,11... | collective-permute-start | bytes 1572872 | tf_op jit(solution)/shard_map/ppermute | solution.py:31
  77.1 16.6 %collective-permute-start.5 = (bf16[1024,256]{1,0:T(8,128)(2,1)}, bf16[1024,256]{1,0:T(8,128)(2,1)S(1)}, u32[]{:S(2)}, u32[]{:S(2)}) collective-permute-start(bf16[1024,256]{1,0:T(8,128)(2,1)} %collective-permute-done.4), channel_id=1, source_target_pairs={{0,1},{1,0},{2,3},{3,2},{4,5},{5,4},{6,7},{7,6},{8,9},{9,8},{10,11... | collective-permute-start | bytes 1572872 | tf_op jit(solution)/shard_map/ppermute | solution.py:31
  81.1 15.4 %collective-permute-start.7 = (bf16[1024,256]{1,0:T(8,128)(2,1)}, bf16[1024,256]{1,0:T(8,128)(2,1)S(1)}, u32[]{:S(2)}, u32[]{:S(2)}) collective-permute-start(bf16[1024,256]{1,0:T(8,128)(2,1)} %collective-permute-done.6), channel_id=1, source_target_pairs={{0,1},{1,0},{2,3},{3,2},{4,5},{5,4},{6,7},{7,6},{8,9},{9,8},{10,11... | collective-permute-start | bytes 1572872 | tf_op jit(solution)/shard_map/ppermute | solution.py:31
  88.0 11.3 %collective-permute-start.9 = (bf16[1024,256]{1,0:T(8,128)(2,1)}, bf16[1024,256]{1,0:T(8,128)(2,1)S(1)}, u32[]{:S(2)}, u32[]{:S(2)}) collective-permute-start(bf16[1024,256]{1,0:T(8,128)(2,1)} %collective-permute-done.8), channel_id=1, source_target_pairs={{0,1},{1,0},{2,3},{3,2},{4,5},{5,4},{6,7},{7,6},{8,9},{9,8},{10,11... | collective-permute-start | bytes 1572872 | tf_op jit(solution)/shard_map/ppermute | solution.py:31
  110.5 37.4 %all-to-all-start.2 = ((bf16[16,64,256]{2,1,0:T(8,128)(2,1)}), bf16[16,64,256]{2,1,0:T(8,128)(2,1)S(1)}, u32[]{:S(2)}, u32[]{:S(2)}) async-start(bf16[16,64,256]{2,1,0:T(8,128)(2,1)} %pad_maximum_fusion.1), calls=%async_computation.2 | async-start | bytes 1048576 | tf_op jit(solution)/shard_map/all_to_all | solution.py:25
  119.5 11.1 %collective-permute-start.11 = (bf16[1024,128]{1,0:T(8,128)(2,1)S(1)}, bf16[1024,128]{1,0:T(8,128)(2,1)S(1)}, u32[]{:S(2)}, u32[]{:S(2)}) collective-permute-start(bf16[1024,128]{1,0:T(8,128)(2,1)S(1)} %fusion.7), channel_id=1, source_target_pairs={{0,2},{2,4},{4,6},{6,0},{1,3},{3,5},{5,7},{7,1},{8,10},{10,12},{12... | collective-permute-start | bytes 786440 | tf_op jit(solution)/shard_map/ppermute | solution.py:29
  121.9 11.4 %collective-permute-start.13 = (bf16[1024,128]{1,0:T(8,128)(2,1)S(1)}, bf16[1024,128]{1,0:T(8,128)(2,1)S(1)}, u32[]{:S(2)}, u32[]{:S(2)}) collective-permute-start(bf16[1024,128]{1,0:T(8,128)(2,1)S(1)} %fusion.7), channel_id=1, source_target_pairs={{0,4},{2,6},{4,0},{6,2},{1,5},{3,7},{5,1},{7,3},{8,12},{10,14},{12... | collective-permute-start | bytes 786440 | tf_op jit(solution)/shard_map/ppermute | solution.py:29
  126.2 9.4 %collective-permute-start.10 = (bf16[1024,128]{1,0:T(8,128)(2,1)S(1)}, bf16[1024,128]{1,0:T(8,128)(2,1)S(1)}, u32[]{:S(2)}, u32[]{:S(2)}) collective-permute-start(bf16[1024,128]{1,0:T(8,128)(2,1)S(1)} %fusion.7), channel_id=1, source_target_pairs={{0,1},{1,0},{2,3},{3,2},{4,5},{5,4},{6,7},{7,6},{8,9},{9,8},{10,11... | collective-permute-start | bytes 786440 | tf_op jit(solution)/shard_map/ppermute | solution.py:31
  128.2 11.8 %collective-permute-start.15 = (bf16[1024,128]{1,0:T(8,128)(2,1)S(1)}, bf16[1024,128]{1,0:T(8,128)(2,1)S(1)}, u32[]{:S(2)}, u32[]{:S(2)}) collective-permute-start(bf16[1024,128]{1,0:T(8,128)(2,1)S(1)} %fusion.7), channel_id=1, source_target_pairs={{0,6},{2,0},{4,2},{6,4},{1,7},{3,1},{5,3},{7,5},{8,14},{10,8},{12,... | collective-permute-start | bytes 786440 | tf_op jit(solution)/shard_map/ppermute | solution.py:29
  130.6 11.3 %collective-permute-start.12 = (bf16[1024,128]{1,0:T(8,128)(2,1)S(1)}, bf16[1024,128]{1,0:T(8,128)(2,1)S(1)}, u32[]{:S(2)}, u32[]{:S(2)}) collective-permute-start(bf16[1024,128]{1,0:T(8,128)(2,1)S(1)} %collective-permute-done.11), channel_id=1, source_target_pairs={{0,1},{1,0},{2,3},{3,2},{4,5},{5,4},{6,7},{7,6},{8,9},{9,8},{10,11... | collective-permute-start | bytes 786440 | tf_op jit(solution)/shard_map/ppermute | solution.py:31
  133.3 10.2 %collective-permute-start.14 = (bf16[1024,128]{1,0:T(8,128)(2,1)S(1)}, bf16[1024,128]{1,0:T(8,128)(2,1)S(1)}, u32[]{:S(2)}, u32[]{:S(2)}) collective-permute-start(bf16[1024,128]{1,0:T(8,128)(2,1)S(1)} %collective-permute-done.13), channel_id=1, source_target_pairs={{0,1},{1,0},{2,3},{3,2},{4,5},{5,4},{6,7},{7,6},{8,9},{9,8},{10,11... | collective-permute-start | bytes 786440 | tf_op jit(solution)/shard_map/ppermute | solution.py:31
  140.0 5.0 %collective-permute-start.16 = (bf16[1024,128]{1,0:T(8,128)(2,1)S(1)}, bf16[1024,128]{1,0:T(8,128)(2,1)S(1)}, u32[]{:S(2)}, u32[]{:S(2)}) collective-permute-start(bf16[1024,128]{1,0:T(8,128)(2,1)S(1)} %collective-permute-done.15), channel_id=1, source_target_pairs={{0,1},{1,0},{2,3},{3,2},{4,5},{5,4},{6,7},{7,6},{8,9},{9,8},{10,11... | collective-permute-start | bytes 786440 | tf_op jit(solution)/shard_map/ppermute | solution.py:31
  148.0 5.1 %copy-start.2 = (s32[128,4]{0,1:T(4,128)S(1)}, s32[128,4]{0,1:T(4,128)}, u32[]{:S(2)}) copy-start(s32[128,4]{0,1:T(4,128)} %param.12) | copy-start | bytes 6148
  148.0 5.1 %copy-start.3 = (f32[128,4]{0,1:T(4,128)S(1)}, f32[128,4]{0,1:T(4,128)}, u32[]{:S(2)}) copy-start(f32[128,4]{0,1:T(4,128)} %param.13) | copy-start | bytes 6148
  151.2 12.0 %collective-permute-start.17 = (bf16[4,128,256]{2,1,0:T(8,128)(2,1)S(1)}, bf16[4,128,256]{2,1,0:T(8,128)(2,1)S(1)}, u32[]{:S(2)}, u32[]{:S(2)}) collective-permute-start(bf16[4,128,256]{2,1,0:T(8,128)(2,1)S(1)} %dynamic-slice_bitcast_fusion.1), channel_id=1, source_target_pairs={{0,1},{1,0},{2,3},{3,2},{4,5},{5,4},{6,7},{7,6},{8,9},{9,8},{10,11... | collective-permute-start | bytes 786440 | tf_op jit(solution)/shard_map/ppermute | solution.py:120
  153.2 39.8 %all-to-all-start.3 = ((bf16[32,32,256]{2,1,0:T(8,128)(2,1)}), bf16[32,32,256]{2,1,0:T(8,128)(2,1)S(1)}, u32[]{:S(2)}, u32[]{:S(2)}) async-start(bf16[32,32,256]{2,1,0:T(8,128)(2,1)} %bitcast.50), calls=%async_computation.3 | async-start | bytes 1048576 | tf_op jit(solution)/shard_map/all_to_all | solution.py:25
  163.3 10.0 %collective-permute-start.18 = (bf16[128,512]{1,0:T(8,128)(2,1)S(1)}, bf16[128,512]{1,0:T(8,128)(2,1)S(1)}, u32[]{:S(2)}, u32[]{:S(2)}) collective-permute-start(bf16[128,512]{1,0:T(8,128)(2,1)S(1)} %get-tuple-element.38), channel_id=1, source_target_pairs={{0,6},{2,0},{4,2},{6,4},{1,7},{3,1},{5,3},{7,5},{8,14},{10,8},{12,... | collective-permute-start | bytes 393224 | tf_op jit(solution)/shard_map/ppermute | solution.py:127
  166.3 8.5 %collective-permute-start.19 = (bf16[128,512]{1,0:T(8,128)(2,1)S(1)}, bf16[128,512]{1,0:T(8,128)(2,1)S(1)}, u32[]{:S(2)}, u32[]{:S(2)}) collective-permute-start(bf16[128,512]{1,0:T(8,128)(2,1)S(1)} %get-tuple-element.39), channel_id=1, source_target_pairs={{0,4},{2,6},{4,0},{6,2},{1,5},{3,7},{5,1},{7,3},{8,12},{10,14},{12... | collective-permute-start | bytes 393224 | tf_op jit(solution)/shard_map/ppermute | solution.py:127
  170.2 7.8 %collective-permute-start.20 = (bf16[128,512]{1,0:T(8,128)(2,1)S(1)}, bf16[128,512]{1,0:T(8,128)(2,1)S(1)}, u32[]{:S(2)}, u32[]{:S(2)}) collective-permute-start(bf16[128,512]{1,0:T(8,128)(2,1)S(1)} %get-tuple-element.36), channel_id=1, source_target_pairs={{0,2},{2,4},{4,6},{6,0},{1,3},{3,5},{5,7},{7,1},{8,10},{10,12},{12... | collective-permute-start | bytes 393224 | tf_op jit(solution)/shard_map/ppermute | solution.py:127

commit v3 on v2

--- a/solution.py
+++ b/solution.py
@@ -39,6 +39,17 @@
         for s in range(C):
             found.append(lax.dynamic_index_in_dim(row, (ic + s) % C, 0, keepdims=False))
     return jnp.concatenate(found, axis=0)
+
+
+def matched(pieces, blocks, ix, ic):
+    total = None
+    for k in range(X):
+        row = lax.dynamic_index_in_dim(blocks, (ix + X - k) % X, 0, keepdims=False)
+        for s in range(C):
+            block = lax.dynamic_index_in_dim(row, (ic + s) % C, 0, keepdims=False)
+            term = jnp.dot(pieces[k][s], block, preferred_element_type=F32)
+            total = term if total is None else total + term
+    return total
 
 
 def layer(tokens, norm_gain, gate_train, up_train, down_train, routes, route_weight):
@@ -92,6 +103,8 @@
     pieces = gather_tp(arrived)
     rows = jnp.concatenate([a for pair in pieces for a in pair], axis=1)
 
+    down_twice, served = lax.optimization_barrier((down_twice, served))
+    down_cols = exchange(down_twice, ("gr", "zl"))
     served = served.reshape(width, 2 * ff)
     gate_weight = served[None, :, :ff]
     up_weight = served[None, :, ff:]
@@ -105,13 +118,14 @@
         * clipped
         * jax.nn.sigmoid(SLOPE_ALPHA * clipped)
     ).astype(BF)
-    down_twice, hidden = lax.optimization_barrier((down_twice, hidden))
-    down_cols = exchange(down_twice, ("gr", "zl"))
-    pieces = gather_tp(hidden)
-    hidden_all = jnp.concatenate([a for pair in pieces for a in pair], axis=1)
+    near = [hidden, None, None, None]
+    for k in (1, 3, 2):
+        near[k] = lax.ppermute(hidden, "x", ring(X, k))
+    other = [lax.ppermute(a, "c", ring(C, 1)) for a in near]
+    pairs = [(near[k], other[k]) for k in range(X)]
 
     down_blocks = down_cols.reshape(X, C, ff, part)
-    total = jnp.dot(hidden_all, relative(down_blocks, ix, ic), preferred_element_type=F32).astype(BF)
+    total = matched(pairs, down_blocks, ix, ic).astype(BF)
     total, down_blocks = lax.optimization_barrier((total, down_blocks))
     result = exchange(total.reshape(n_exp, CAP, part), FS)
 

time: 196 us -> 195 us (level)
  the two profiles are of different devices: /device:TPU:6 before, /device:TPU:2 now
where the time goes in v3:
time: 195 us; the launch traced here: 193 us
  starting transfers between devices  100 us (51%)
  waiting for transfers between devices  59.7 us (31%)
  local copies, waits for them, and re-layouts  15.1 us (8%)
  matrix products  10.8 us (6%)
  other arithmetic  5.99 us (3%)
    all_to_all x4, starting transfers between devices, exchange(): return lax.all_to_all(a, axis, split_axis=0, concat_axis=0, tiled=True)  39.3 us
    all_to_all x4, waiting for transfers between devices, exchange(): return lax.all_to_all(a, axis, split_axis=0, concat_axis=0, tiled=True)  33.4 us
    ppermute x3, starting transfers between devices, layer(): lax.ppermute(column(j), 'y', ring(Y, j))  12.6 us
    unnamed x29, local copies, waits for them, and re-layouts  11.5 us
    ppermute x3, waiting for transfers between devices, gather_tp(): mine = [own] + [lax.ppermute(own, 'x', ring(X, k)) for k in (1, 3, 2)]  10.5 us
    ppermute x3, starting transfers between devices, layer(): near[k] = lax.ppermute(hidden, 'x', ring(X, k))  10.5 us
    ppermute x3, starting transfers between devices, gather_tp(): mine = [own] + [lax.ppermute(own, 'x', ring(X, k)) for k in (1, 3, 2)]  10.5 us
    ppermute x3, starting transfers between devices, layer(): cols.append(block if k == 0 else lax.ppermute(block, 'x', ring(X, k)))  9.45 us
  transfers between devices with their start and end apart: 25, of which 13 were waited for; matrix products, arithmetic and copies ran while one was open for 14% of the time, Pallas kernels for 0%

profile of v3, /device:TPU:2, one launch (start us, length us, event | category | flops | bytes accessed | tf_op | source)
XLA Modules:
  0.0 193.2 jit_solution(5627157100710134187)
XLA Ops:
  0.7 1.1 fusion.38
  1.8 1.5 fusion.26
  3.4 4.9 %collective-permute-start = (bf16[8,48,256]{2,1,0:T(8,128)(2,1)S(1)}, bf16[8,48,256]{2,1,0:T(8,128)(2,1)S(1)}, u32[]{:S(2)}, u32[]{:S(2)}) collective-permute-start(bf16[8,48,256]{2,1,0:T(8,128)(2,1)S(1)} %pad_maximum_fusion.2), channel_id=1, source_target_pairs={{0,24},{8,0},{16,8},{24,16},{1,25},{9,1},{17,9},{25,17},{2,26},{10... | collective-permute-start | bytes 589832 | tf_op jit(solution)/shard_map/ppermute | solution.py:93
  9.2 1.2 multiply_reduce_fusion
  10.7 2.0 %convolution_convert_fusion = bf16[1024,256]{1,0:T(8,128)(2,1)} fusion(pred[1024,128]{1,0:T(32,128)(4,1)S(1)} %bitcast_compare_fusion, f32[128]{0:T(128)S(1)} %add_rsqrt_fusion, bf16[128,2048]{1,0:T(8,128)(2,1)} %param.7, s32[]{:T(128)S(6)} %select_n.234), kind=kOutput, calls=%fused_computation.8 | convolution fusion | flops 67469312 | bytes 721412 | tf_op jit(solution)/shard_map/dot_general | solution.py:75
  12.7 13.1 %all-to-all-start = ((bf16[32,32,256]{2,1,0:T(8,128)(2,1)}), bf16[32,32,256]{2,1,0:T(8,128)(2,1)S(1)}, u32[]{:S(2)}, u32[]{:S(2)}) async-start(bf16[32,32,256]{2,1,0:T(8,128)(2,1)} %bitcast.29), calls=%async_computation | async-start | bytes 1048576 | tf_op jit(solution)/shard_map/all_to_all | solution.py:25
  25.8 5.2 %collective-permute-start.1 = (bf16[8,48,256]{2,1,0:T(8,128)(2,1)S(1)}, bf16[8,48,256]{2,1,0:T(8,128)(2,1)S(1)}, u32[]{:S(2)}, u32[]{:S(2)}) collective-permute-start(bf16[8,48,256]{2,1,0:T(8,128)(2,1)S(1)} %pad_maximum_fusion.3), channel_id=1, source_target_pairs={{0,16},{8,24},{16,0},{24,8},{1,17},{9,25},{17,1},{25,9},{2,18},{10... | collective-permute-start | bytes 589832 | tf_op jit(solution)/shard_map/ppermute | solution.py:93
  31.1 2.5 %collective-permute-start.2 = (bf16[8,48,256]{2,1,0:T(8,128)(2,1)S(1)}, bf16[8,48,256]{2,1,0:T(8,128)(2,1)S(1)}, u32[]{:S(2)}, u32[]{:S(2)}) collective-permute-start(bf16[8,48,256]{2,1,0:T(8,128)(2,1)S(1)} %pad_maximum_fusion.4), channel_id=1, source_target_pairs={{0,8},{8,16},{16,24},{24,0},{1,9},{9,17},{17,25},{25,1},{2,10},{10... | collective-permute-start | bytes 589832 | tf_op jit(solution)/shard_map/ppermute | solution.py:93
  33.6 4.9 %collective-permute-done.1 = bf16[8,48,256]{2,1,0:T(8,128)(2,1)S(1)} collective-permute-done((bf16[8,48,256]{2,1,0:T(8,128)(2,1)S(1)}, bf16[8,48,256]{2,1,0:T(8,128)(2,1)S(1)}, u32[]{:S(2)}, u32[]{:S(2)}) %collective-permute-start.1) | collective-permute-done | bytes 196640 | tf_op jit(solution)/shard_map/ppermute | solution.py:93
  38.6 4.2 %collective-permute-done.2 = bf16[8,48,256]{2,1,0:T(8,128)(2,1)S(1)} collective-permute-done((bf16[8,48,256]{2,1,0:T(8,128)(2,1)S(1)}, bf16[8,48,256]{2,1,0:T(8,128)(2,1)S(1)}, u32[]{:S(2)}, u32[]{:S(2)}) %collective-permute-start.2) | collective-permute-done | bytes 196640 | tf_op jit(solution)/shard_map/ppermute | solution.py:93
  44.1 11.1 %all-to-all-done = bf16[32,32,256]{2,1,0:T(8,128)(2,1)S(1)} async-done(((bf16[32,32,256]{2,1,0:T(8,128)(2,1)}), bf16[32,32,256]{2,1,0:T(8,128)(2,1)S(1)}, u32[]{:S(2)}, u32[]{:S(2)}) %all-to-all-start) | async-done | bytes 524320 | tf_op jit(solution)/shard_map/all_to_all | solution.py:25
  55.1 7.7 %all-to-all-start.1 = ((bf16[16,128,256]{2,1,0:T(8,128)(2,1)}), bf16[16,128,256]{2,1,0:T(8,128)(2,1)S(1)}, u32[]{:S(2)}, u32[]{:S(2)}) async-start(bf16[16,128,256]{2,1,0:T(8,128)(2,1)} %pad_maximum_fusion), calls=%async_computation.1 | async-start | bytes 2097152 | tf_op jit(solution)/shard_map/all_to_all | solution.py:25
  62.9 3.4 %collective-permute-start.4 = (bf16[1024,256]{1,0:T(8,128)(2,1)S(1)}, bf16[1024,256]{1,0:T(8,128)(2,1)}, u32[]{:S(2)}, u32[]{:S(2)}) collective-permute-start(bf16[1024,256]{1,0:T(8,128)(2,1)S(1)} %bitcast.204), channel_id=1, source_target_pairs={{0,2},{2,4},{4,6},{6,0},{1,3},{3,5},{5,7},{7,1},{8,10},{10,12},{12... | collective-permute-start | bytes 1572872 | tf_op jit(solution)/shard_map/ppermute | solution.py:29
  66.3 3.0 %collective-permute-start.6 = (bf16[1024,256]{1,0:T(8,128)(2,1)S(1)}, bf16[1024,256]{1,0:T(8,128)(2,1)}, u32[]{:S(2)}, u32[]{:S(2)}) collective-permute-start(bf16[1024,256]{1,0:T(8,128)(2,1)S(1)} %bitcast.205), channel_id=1, source_target_pairs={{0,4},{2,6},{4,0},{6,2},{1,5},{3,7},{5,1},{7,3},{8,12},{10,14},{12... | collective-permute-start | bytes 1572872 | tf_op jit(solution)/shard_map/ppermute | solution.py:29
  69.3 4.1 %collective-permute-start.8 = (bf16[1024,256]{1,0:T(8,128)(2,1)S(1)}, bf16[1024,256]{1,0:T(8,128)(2,1)}, u32[]{:S(2)}, u32[]{:S(2)}) collective-permute-start(bf16[1024,256]{1,0:T(8,128)(2,1)S(1)} %bitcast.206), channel_id=1, source_target_pairs={{0,6},{2,0},{4,2},{6,4},{1,7},{3,1},{5,3},{7,5},{8,14},{10,8},{12,... | collective-permute-start | bytes 1572872 | tf_op jit(solution)/shard_map/ppermute | solution.py:29
  73.4 1.9 collective-permute-start.3
  75.4 4.3 %collective-permute-done.4 = bf16[1024,256]{1,0:T(8,128)(2,1)} collective-permute-done((bf16[1024,256]{1,0:T(8,128)(2,1)S(1)}, bf16[1024,256]{1,0:T(8,128)(2,1)}, u32[]{:S(2)}, u32[]{:S(2)}) %collective-permute-start.4) | collective-permute-done | bytes 524320 | tf_op jit(solution)/shard_map/ppermute | solution.py:29
  79.6 1.9 collective-permute-start.5
  82.4 2.1 %collective-permute-done.6 = bf16[1024,256]{1,0:T(8,128)(2,1)} collective-permute-done((bf16[1024,256]{1,0:T(8,128)(2,1)S(1)}, bf16[1024,256]{1,0:T(8,128)(2,1)}, u32[]{:S(2)}, u32[]{:S(2)}) %collective-permute-start.6) | collective-permute-done | bytes 524320 | tf_op jit(solution)/shard_map/ppermute | solution.py:29
  84.6 1.9 collective-permute-start.7
  87.4 4.1 %collective-permute-done.8 = bf16[1024,256]{1,0:T(8,128)(2,1)} collective-permute-done((bf16[1024,256]{1,0:T(8,128)(2,1)S(1)}, bf16[1024,256]{1,0:T(8,128)(2,1)}, u32[]{:S(2)}, u32[]{:S(2)}) %collective-permute-start.8) | collective-permute-done | bytes 524320 | tf_op jit(solution)/shard_map/ppermute | solution.py:29
  91.5 1.9 collective-permute-start.9
  93.4 1.9 constant_dynamic-update-slice_fusion.6
  95.4 1.9 constant_dynamic-update-slice_fusion.5
  98.1 1.9 constant_dynamic-update-slice_fusion.3
  100.9 1.9 constant_dynamic-update-slice_fusion.1
  102.8 6.3 %all-to-all-done.1 = bf16[16,128,256]{2,1,0:T(8,128)(2,1)S(1)} async-done(((bf16[16,128,256]{2,1,0:T(8,128)(2,1)}), bf16[16,128,256]{2,1,0:T(8,128)(2,1)S(1)}, u32[]{:S(2)}, u32[]{:S(2)}) %all-to-all-start.1) | async-done | bytes 1048608 | tf_op jit(solution)/shard_map/all_to_all | solution.py:25
  109.1 9.0 %all-to-all-start.2 = ((bf16[16,64,256]{2,1,0:T(8,128)(2,1)}), bf16[16,64,256]{2,1,0:T(8,128)(2,1)S(1)}, u32[]{:S(2)}, u32[]{:S(2)}) async-start(bf16[16,64,256]{2,1,0:T(8,128)(2,1)} %pad_maximum_fusion.1), calls=%async_computation.2 | async-start | bytes 1048576 | tf_op jit(solution)/shard_map/all_to_all | solution.py:25
  119.2 3.4 %fusion.72 = f32[1024,256]{1,0:T(8,128)S(1)} fusion(bf16[1024,2048]{1,0:T(8,128)(2,1)} %constant_dynamic-update-slice_fusion, bf16[2048,256]{1,0:T(8,128)(2,1)S(1)} %bitcast_dynamic-update-slice_fusion.12), kind=kOutput, calls=%fused_computation.156 | convolution fusion | flops 1073741824 | bytes 6291456 | tf_op jit(solution)/shard_map/dot_general | solution.py:112
  122.9 3.4 %collective-permute-start.11 = (bf16[1024,128]{1,0:T(8,128)(2,1)S(1)}, bf16[1024,128]{1,0:T(8,128)(2,1)S(1)}, u32[]{:S(2)}, u32[]{:S(2)}) collective-permute-start(bf16[1024,128]{1,0:T(8,128)(2,1)S(1)} %fusion.10), channel_id=1, source_target_pairs={{0,2},{2,4},{4,6},{6,0},{1,3},{3,5},{5,7},{7,1},{8,10},{10,12},{12... | collective-permute-start | bytes 786440 | tf_op jit(solution)/shard_map/ppermute | solution.py:123
  126.3 3.0 %collective-permute-start.13 = (bf16[1024,128]{1,0:T(8,128)(2,1)S(1)}, bf16[1024,128]{1,0:T(8,128)(2,1)}, u32[]{:S(2)}, u32[]{:S(2)}) collective-permute-start(bf16[1024,128]{1,0:T(8,128)(2,1)S(1)} %fusion.10), channel_id=1, source_target_pairs={{0,4},{2,6},{4,0},{6,2},{1,5},{3,7},{5,1},{7,3},{8,12},{10,14},{12... | collective-permute-start | bytes 786440 | tf_op jit(solution)/shard_map/ppermute | solution.py:123
  129.3 4.1 %collective-permute-start.15 = (bf16[1024,128]{1,0:T(8,128)(2,1)S(1)}, bf16[1024,128]{1,0:T(8,128)(2,1)S(1)}, u32[]{:S(2)}, u32[]{:S(2)}) collective-permute-start(bf16[1024,128]{1,0:T(8,128)(2,1)S(1)} %fusion.10), channel_id=1, source_target_pairs={{0,6},{2,0},{4,2},{6,4},{1,7},{3,1},{5,3},{7,5},{8,14},{10,8},{12,... | collective-permute-start | bytes 786440 | tf_op jit(solution)/shard_map/ppermute | solution.py:123
  133.4 1.9 collective-permute-start.10
  135.3 2.4 %collective-permute-start.12 = (bf16[1024,128]{1,0:T(8,128)(2,1)S(1)}, bf16[1024,128]{1,0:T(8,128)(2,1)S(1)}, u32[]{:S(2)}, u32[]{:S(2)}) collective-permute-start(bf16[1024,128]{1,0:T(8,128)(2,1)S(1)} %collective-permute-done.11), channel_id=1, source_target_pairs={{0,1},{1,0},{2,3},{3,2},{4,5},{5,4},{6,7},{7,6},{8,9},{9,8},{10,11... | collective-permute-start | bytes 786440 | tf_op jit(solution)/shard_map/ppermute | solution.py:124
  137.7 1.3 collective-permute-done.13
  139.0 1.9 collective-permute-start.14
  140.9 1.3 collective-permute-done.15
  142.2 1.9 collective-permute-start.16
  144.1 2.4 %all-to-all-done.2 = bf16[16,64,256]{2,1,0:T(8,128)(2,1)S(1)} async-done(((bf16[16,64,256]{2,1,0:T(8,128)(2,1)}), bf16[16,64,256]{2,1,0:T(8,128)(2,1)S(1)}, u32[]{:S(2)}, u32[]{:S(2)}) %all-to-all-start.2) | async-done | bytes 524320 | tf_op jit(solution)/shard_map/all_to_all | solution.py:25
  147.4 1.2 fusion.43
  150.6 1.9 collective-permute-start.17
  152.6 9.5 %all-to-all-start.3 = ((bf16[32,32,256]{2,1,0:T(8,128)(2,1)}), bf16[32,32,256]{2,1,0:T(8,128)(2,1)S(1)}, u32[]{:S(2)}, u32[]{:S(2)}) async-start(bf16[32,32,256]{2,1,0:T(8,128)(2,1)} %bitcast.50), calls=%async_computation.3 | async-start | bytes 1048576 | tf_op jit(solution)/shard_map/all_to_all | solution.py:25
  162.3 2.1 %collective-permute-start.18 = (bf16[128,512]{1,0:T(8,128)(2,1)S(1)}, bf16[128,512]{1,0:T(8,128)(2,1)S(1)}, u32[]{:S(2)}, u32[]{:S(2)}) collective-permute-start(bf16[128,512]{1,0:T(8,128)(2,1)S(1)} %get-tuple-element.38), channel_id=1, source_target_pairs={{0,6},{2,0},{4,2},{6,4},{1,7},{3,1},{5,3},{7,5},{8,14},{10,8},{12,... | collective-permute-start | bytes 393224 | tf_op jit(solution)/shard_map/ppermute | solution.py:141
  165.4 3.8 %collective-permute-start.19 = (bf16[128,512]{1,0:T(8,128)(2,1)S(1)}, bf16[128,512]{1,0:T(8,128)(2,1)S(1)}, u32[]{:S(2)}, u32[]{:S(2)}) collective-permute-start(bf16[128,512]{1,0:T(8,128)(2,1)S(1)} %get-tuple-element.39), channel_id=1, source_target_pairs={{0,4},{2,6},{4,0},{6,2},{1,5},{3,7},{5,1},{7,3},{8,12},{10,14},{12... | collective-permute-start | bytes 393224 | tf_op jit(solution)/shard_map/ppermute | solution.py:141
  169.2 3.6 %collective-permute-start.20 = (bf16[128,512]{1,0:T(8,128)(2,1)S(1)}, bf16[128,512]{1,0:T(8,128)(2,1)S(1)}, u32[]{:S(2)}, u32[]{:S(2)}) collective-permute-start(bf16[128,512]{1,0:T(8,128)(2,1)S(1)} %get-tuple-element.36), channel_id=1, source_target_pairs={{0,2},{2,4},{4,6},{6,0},{1,3},{3,5},{5,7},{7,1},{8,10},{10,12},{12... | collective-permute-start | bytes 393224 | tf_op jit(solution)/shard_map/ppermute | solution.py:141
  172.8 1.3 collective-permute-done.19
  174.1 2.8 %collective-permute-done.20 = bf16[128,512]{1,0:T(8,128)(2,1)S(1)} collective-permute-done((bf16[128,512]{1,0:T(8,128)(2,1)S(1)}, bf16[128,512]{1,0:T(8,128)(2,1)S(1)}, u32[]{:S(2)}, u32[]{:S(2)}) %collective-permute-start.20) | collective-permute-done | bytes 131104 | tf_op jit(solution)/shard_map/ppermute | solution.py:141
  178.4 13.6 %all-to-all-done.3 = bf16[32,32,256]{2,1,0:T(8,128)(2,1)S(1)} async-done(((bf16[32,32,256]{2,1,0:T(8,128)(2,1)}), bf16[32,32,256]{2,1,0:T(8,128)(2,1)S(1)}, u32[]{:S(2)}, u32[]{:S(2)}) %all-to-all-start.3) | async-done | bytes 524320 | tf_op jit(solution)/shard_map/all_to_all | solution.py:25
  (74 shorter events, 13.8 us)
Async XLA Ops:
  3.4 30.2 %collective-permute-start = (bf16[8,48,256]{2,1,0:T(8,128)(2,1)S(1)}, bf16[8,48,256]{2,1,0:T(8,128)(2,1)S(1)}, u32[]{:S(2)}, u32[]{:S(2)}) collective-permute-start(bf16[8,48,256]{2,1,0:T(8,128)(2,1)S(1)} %pad_maximum_fusion.2), channel_id=1, source_target_pairs={{0,24},{8,0},{16,8},{24,16},{1,25},{9,1},{17,9},{25,17},{2,26},{10... | collective-permute-start | bytes 589832 | tf_op jit(solution)/shard_map/ppermute | solution.py:93
  12.7 42.5 %all-to-all-start = ((bf16[32,32,256]{2,1,0:T(8,128)(2,1)}), bf16[32,32,256]{2,1,0:T(8,128)(2,1)S(1)}, u32[]{:S(2)}, u32[]{:S(2)}) async-start(bf16[32,32,256]{2,1,0:T(8,128)(2,1)} %bitcast.29), calls=%async_computation | async-start | bytes 1048576 | tf_op jit(solution)/shard_map/all_to_all | solution.py:25
  25.8 12.7 %collective-permute-start.1 = (bf16[8,48,256]{2,1,0:T(8,128)(2,1)S(1)}, bf16[8,48,256]{2,1,0:T(8,128)(2,1)S(1)}, u32[]{:S(2)}, u32[]{:S(2)}) collective-permute-start(bf16[8,48,256]{2,1,0:T(8,128)(2,1)S(1)} %pad_maximum_fusion.3), channel_id=1, source_target_pairs={{0,16},{8,24},{16,0},{24,8},{1,17},{9,25},{17,1},{25,9},{2,18},{10... | collective-permute-start | bytes 589832 | tf_op jit(solution)/shard_map/ppermute | solution.py:93
  31.1 11.7 %collective-permute-start.2 = (bf16[8,48,256]{2,1,0:T(8,128)(2,1)S(1)}, bf16[8,48,256]{2,1,0:T(8,128)(2,1)S(1)}, u32[]{:S(2)}, u32[]{:S(2)}) collective-permute-start(bf16[8,48,256]{2,1,0:T(8,128)(2,1)S(1)} %pad_maximum_fusion.4), channel_id=1, source_target_pairs={{0,8},{8,16},{16,24},{24,0},{1,9},{9,17},{17,25},{25,1},{2,10},{10... | collective-permute-start | bytes 589832 | tf_op jit(solution)/shard_map/ppermute | solution.py:93
  55.1 54.0 %all-to-all-start.1 = ((bf16[16,128,256]{2,1,0:T(8,128)(2,1)}), bf16[16,128,256]{2,1,0:T(8,128)(2,1)S(1)}, u32[]{:S(2)}, u32[]{:S(2)}) async-start(bf16[16,128,256]{2,1,0:T(8,128)(2,1)} %pad_maximum_fusion), calls=%async_computation.1 | async-start | bytes 2097152 | tf_op jit(solution)/shard_map/all_to_all | solution.py:25
  62.9 16.8 %collective-permute-start.4 = (bf16[1024,256]{1,0:T(8,128)(2,1)S(1)}, bf16[1024,256]{1,0:T(8,128)(2,1)}, u32[]{:S(2)}, u32[]{:S(2)}) collective-permute-start(bf16[1024,256]{1,0:T(8,128)(2,1)S(1)} %bitcast.204), channel_id=1, source_target_pairs={{0,2},{2,4},{4,6},{6,0},{1,3},{3,5},{5,7},{7,1},{8,10},{10,12},{12... | collective-permute-start | bytes 1572872 | tf_op jit(solution)/shard_map/ppermute | solution.py:29
  66.3 18.3 %collective-permute-start.6 = (bf16[1024,256]{1,0:T(8,128)(2,1)S(1)}, bf16[1024,256]{1,0:T(8,128)(2,1)}, u32[]{:S(2)}, u32[]{:S(2)}) collective-permute-start(bf16[1024,256]{1,0:T(8,128)(2,1)S(1)} %bitcast.205), channel_id=1, source_target_pairs={{0,4},{2,6},{4,0},{6,2},{1,5},{3,7},{5,1},{7,3},{8,12},{10,14},{12... | collective-permute-start | bytes 1572872 | tf_op jit(solution)/shard_map/ppermute | solution.py:29
  69.3 22.2 %collective-permute-start.8 = (bf16[1024,256]{1,0:T(8,128)(2,1)S(1)}, bf16[1024,256]{1,0:T(8,128)(2,1)}, u32[]{:S(2)}, u32[]{:S(2)}) collective-permute-start(bf16[1024,256]{1,0:T(8,128)(2,1)S(1)} %bitcast.206), channel_id=1, source_target_pairs={{0,6},{2,0},{4,2},{6,4},{1,7},{3,1},{5,3},{7,5},{8,14},{10,8},{12,... | collective-permute-start | bytes 1572872 | tf_op jit(solution)/shard_map/ppermute | solution.py:29
  73.4 20.1 %collective-permute-start.3 = (bf16[1024,256]{1,0:T(8,128)(2,1)S(1)}, bf16[1024,256]{1,0:T(8,128)(2,1)}, u32[]{:S(2)}, u32[]{:S(2)}) collective-permute-start(bf16[1024,256]{1,0:T(8,128)(2,1)S(1)} %bitcast.207), channel_id=1, source_target_pairs={{0,1},{1,0},{2,3},{3,2},{4,5},{5,4},{6,7},{7,6},{8,9},{9,8},{10,11... | collective-permute-start | bytes 1572872 | tf_op jit(solution)/shard_map/ppermute | solution.py:31
  79.6 17.6 %collective-permute-start.5 = (bf16[1024,256]{1,0:T(8,128)(2,1)}, bf16[1024,256]{1,0:T(8,128)(2,1)S(1)}, u32[]{:S(2)}, u32[]{:S(2)}) collective-permute-start(bf16[1024,256]{1,0:T(8,128)(2,1)} %collective-permute-done.4), channel_id=1, source_target_pairs={{0,1},{1,0},{2,3},{3,2},{4,5},{5,4},{6,7},{7,6},{8,9},{9,8},{10,11... | collective-permute-start | bytes 1572872 | tf_op jit(solution)/shard_map/ppermute | solution.py:31
  84.6 15.5 %collective-permute-start.7 = (bf16[1024,256]{1,0:T(8,128)(2,1)}, bf16[1024,256]{1,0:T(8,128)(2,1)S(1)}, u32[]{:S(2)}, u32[]{:S(2)}) collective-permute-start(bf16[1024,256]{1,0:T(8,128)(2,1)} %collective-permute-done.6), channel_id=1, source_target_pairs={{0,1},{1,0},{2,3},{3,2},{4,5},{5,4},{6,7},{7,6},{8,9},{9,8},{10,11... | collective-permute-start | bytes 1572872 | tf_op jit(solution)/shard_map/ppermute | solution.py:31
  91.5 26.6 %collective-permute-start.9 = (bf16[1024,256]{1,0:T(8,128)(2,1)}, bf16[1024,256]{1,0:T(8,128)(2,1)S(1)}, u32[]{:S(2)}, u32[]{:S(2)}) collective-permute-start(bf16[1024,256]{1,0:T(8,128)(2,1)} %collective-permute-done.8), channel_id=1, source_target_pairs={{0,1},{1,0},{2,3},{3,2},{4,5},{5,4},{6,7},{7,6},{8,9},{9,8},{10,11... | collective-permute-start | bytes 1572872 | tf_op jit(solution)/shard_map/ppermute | solution.py:31
  109.1 37.4 %all-to-all-start.2 = ((bf16[16,64,256]{2,1,0:T(8,128)(2,1)}), bf16[16,64,256]{2,1,0:T(8,128)(2,1)S(1)}, u32[]{:S(2)}, u32[]{:S(2)}) async-start(bf16[16,64,256]{2,1,0:T(8,128)(2,1)} %pad_maximum_fusion.1), calls=%async_computation.2 | async-start | bytes 1048576 | tf_op jit(solution)/shard_map/all_to_all | solution.py:25
  122.9 12.4 %collective-permute-start.11 = (bf16[1024,128]{1,0:T(8,128)(2,1)S(1)}, bf16[1024,128]{1,0:T(8,128)(2,1)S(1)}, u32[]{:S(2)}, u32[]{:S(2)}) collective-permute-start(bf16[1024,128]{1,0:T(8,128)(2,1)S(1)} %fusion.10), channel_id=1, source_target_pairs={{0,2},{2,4},{4,6},{6,0},{1,3},{3,5},{5,7},{7,1},{8,10},{10,12},{12... | collective-permute-start | bytes 786440 | tf_op jit(solution)/shard_map/ppermute | solution.py:123
  126.3 12.7 %collective-permute-start.13 = (bf16[1024,128]{1,0:T(8,128)(2,1)S(1)}, bf16[1024,128]{1,0:T(8,128)(2,1)}, u32[]{:S(2)}, u32[]{:S(2)}) collective-permute-start(bf16[1024,128]{1,0:T(8,128)(2,1)S(1)} %fusion.10), channel_id=1, source_target_pairs={{0,4},{2,6},{4,0},{6,2},{1,5},{3,7},{5,1},{7,3},{8,12},{10,14},{12... | collective-permute-start | bytes 786440 | tf_op jit(solution)/shard_map/ppermute | solution.py:123
  129.3 12.9 %collective-permute-start.15 = (bf16[1024,128]{1,0:T(8,128)(2,1)S(1)}, bf16[1024,128]{1,0:T(8,128)(2,1)S(1)}, u32[]{:S(2)}, u32[]{:S(2)}) collective-permute-start(bf16[1024,128]{1,0:T(8,128)(2,1)S(1)} %fusion.10), channel_id=1, source_target_pairs={{0,6},{2,0},{4,2},{6,4},{1,7},{3,1},{5,3},{7,5},{8,14},{10,8},{12,... | collective-permute-start | bytes 786440 | tf_op jit(solution)/shard_map/ppermute | solution.py:123
  133.4 13.4 %collective-permute-start.10 = (bf16[1024,128]{1,0:T(8,128)(2,1)S(1)}, bf16[1024,128]{1,0:T(8,128)(2,1)S(1)}, u32[]{:S(2)}, u32[]{:S(2)}) collective-permute-start(bf16[1024,128]{1,0:T(8,128)(2,1)S(1)} %fusion.10), channel_id=1, source_target_pairs={{0,1},{1,0},{2,3},{3,2},{4,5},{5,4},{6,7},{7,6},{8,9},{9,8},{10,11... | collective-permute-start | bytes 786440 | tf_op jit(solution)/shard_map/ppermute | solution.py:124
  135.3 13.3 %collective-permute-start.12 = (bf16[1024,128]{1,0:T(8,128)(2,1)S(1)}, bf16[1024,128]{1,0:T(8,128)(2,1)S(1)}, u32[]{:S(2)}, u32[]{:S(2)}) collective-permute-start(bf16[1024,128]{1,0:T(8,128)(2,1)S(1)} %collective-permute-done.11), channel_id=1, source_target_pairs={{0,1},{1,0},{2,3},{3,2},{4,5},{5,4},{6,7},{7,6},{8,9},{9,8},{10,11... | collective-permute-start | bytes 786440 | tf_op jit(solution)/shard_map/ppermute | solution.py:124
  139.0 10.2 %collective-permute-start.14 = (bf16[1024,128]{1,0:T(8,128)(2,1)}, bf16[1024,128]{1,0:T(8,128)(2,1)S(1)}, u32[]{:S(2)}, u32[]{:S(2)}) collective-permute-start(bf16[1024,128]{1,0:T(8,128)(2,1)} %collective-permute-done.13), channel_id=1, source_target_pairs={{0,1},{1,0},{2,3},{3,2},{4,5},{5,4},{6,7},{7,6},{8,9},{9,8},{10,11... | collective-permute-start | bytes 786440 | tf_op jit(solution)/shard_map/ppermute | solution.py:124
  142.2 7.3 %collective-permute-start.16 = (bf16[1024,128]{1,0:T(8,128)(2,1)S(1)}, bf16[1024,128]{1,0:T(8,128)(2,1)S(1)}, u32[]{:S(2)}, u32[]{:S(2)}) collective-permute-start(bf16[1024,128]{1,0:T(8,128)(2,1)S(1)} %collective-permute-done.15), channel_id=1, source_target_pairs={{0,1},{1,0},{2,3},{3,2},{4,5},{5,4},{6,7},{7,6},{8,9},{9,8},{10,11... | collective-permute-start | bytes 786440 | tf_op jit(solution)/shard_map/ppermute | solution.py:124
  148.9 3.7 %copy-start = (s32[128,4]{0,1:T(4,128)S(1)}, s32[128,4]{0,1:T(4,128)}, u32[]{:S(2)}) copy-start(s32[128,4]{0,1:T(4,128)} %param.12) | copy-start | bytes 6148
  148.9 3.7 %copy-start.1 = (f32[128,4]{0,1:T(4,128)S(1)}, f32[128,4]{0,1:T(4,128)}, u32[]{:S(2)}) copy-start(f32[128,4]{0,1:T(4,128)} %param.13) | copy-start | bytes 6148
  150.6 11.5 %collective-permute-start.17 = (bf16[4,128,256]{2,1,0:T(8,128)(2,1)S(1)}, bf16[4,128,256]{2,1,0:T(8,128)(2,1)S(1)}, u32[]{:S(2)}, u32[]{:S(2)}) collective-permute-start(bf16[4,128,256]{2,1,0:T(8,128)(2,1)S(1)} %dynamic-slice_bitcast_fusion.1), channel_id=1, source_target_pairs={{0,1},{1,0},{2,3},{3,2},{4,5},{5,4},{6,7},{7,6},{8,9},{9,8},{10,11... | collective-permute-start | bytes 786440 | tf_op jit(solution)/shard_map/ppermute | solution.py:134
  152.6 39.4 %all-to-all-start.3 = ((bf16[32,32,256]{2,1,0:T(8,128)(2,1)}), bf16[32,32,256]{2,1,0:T(8,128)(2,1)S(1)}, u32[]{:S(2)}, u32[]{:S(2)}) async-start(bf16[32,32,256]{2,1,0:T(8,128)(2,1)} %bitcast.50), calls=%async_computation.3 | async-start | bytes 1048576 | tf_op jit(solution)/shard_map/all_to_all | solution.py:25
  162.3 10.5 %collective-permute-start.18 = (bf16[128,512]{1,0:T(8,128)(2,1)S(1)}, bf16[128,512]{1,0:T(8,128)(2,1)S(1)}, u32[]{:S(2)}, u32[]{:S(2)}) collective-permute-start(bf16[128,512]{1,0:T(8,128)(2,1)S(1)} %get-tuple-element.38), channel_id=1, source_target_pairs={{0,6},{2,0},{4,2},{6,4},{1,7},{3,1},{5,3},{7,5},{8,14},{10,8},{12,... | collective-permute-start | bytes 393224 | tf_op jit(solution)/shard_map/ppermute | solution.py:141
  165.4 8.7 %collective-permute-start.19 = (bf16[128,512]{1,0:T(8,128)(2,1)S(1)}, bf16[128,512]{1,0:T(8,128)(2,1)S(1)}, u32[]{:S(2)}, u32[]{:S(2)}) collective-permute-start(bf16[128,512]{1,0:T(8,128)(2,1)S(1)} %get-tuple-element.39), channel_id=1, source_target_pairs={{0,4},{2,6},{4,0},{6,2},{1,5},{3,7},{5,1},{7,3},{8,12},{10,14},{12... | collective-permute-start | bytes 393224 | tf_op jit(solution)/shard_map/ppermute | solution.py:141
  169.2 7.7 %collective-permute-start.20 = (bf16[128,512]{1,0:T(8,128)(2,1)S(1)}, bf16[128,512]{1,0:T(8,128)(2,1)S(1)}, u32[]{:S(2)}, u32[]{:S(2)}) collective-permute-start(bf16[128,512]{1,0:T(8,128)(2,1)S(1)} %get-tuple-element.36), channel_id=1, source_target_pairs={{0,2},{2,4},{4,6},{6,0},{1,3},{3,5},{5,7},{7,1},{8,10},{10,12},{12... | collective-permute-start | bytes 393224 | tf_op jit(solution)/shard_map/ppermute | solution.py:141

commit v4 on v3

--- a/solution.py
+++ b/solution.py
@@ -68,9 +68,9 @@
     at_slot = place[:, None, :] == jnp.arange(CAP, dtype=jnp.int32)[None, :, None]
     pick = at_slot.astype(BF).reshape(n_exp * CAP, n_tok)
 
-    wide = tokens.astype(F32)
+    wide = lax.optimization_barrier(tokens.astype(F32))
     scale = lax.rsqrt(jnp.mean(wide * wide, axis=1, keepdims=True) + NORM_EPSILON)
-    own = lax.dynamic_slice_in_dim(tokens, (ix * C + ic) * part, part, 1).astype(F32)
+    own = lax.dynamic_slice_in_dim(wide, (ix * C + ic) * part, part, 1)
     normed = (own * scale).astype(BF)
     slots = jnp.dot(pick, normed, preferred_element_type=F32).astype(BF)
     arrived = exchange(slots.reshape(n_exp, CAP, part), FS)
@@ -147,9 +147,10 @@
     high = lax.reduce_precision(spread, 8, 7)
     contract = (((0,), (0,)), ((), ()))
     result = result.reshape(n_exp * CAP, part)
-    mixed = lax.dot_general(
-        high.astype(BF), result, contract, preferred_element_type=F32
-    ) + lax.dot_general((spread - high).astype(BF), result, contract, preferred_element_type=F32)
+    coefficients = jnp.concatenate([high.astype(BF), (spread - high).astype(BF)], axis=1)
+    coefficients, total = lax.optimization_barrier((coefficients, total))
+    products = lax.dot_general(coefficients, result, contract, preferred_element_type=F32)
+    mixed = products[:n_tok] + products[n_tok:]
     return (mixed.astype(BF), gate_weight, up_weight, down_weight)
 
 

time: 195 us -> 195 us (level)
    convert_element_type x0 -> x3, other arithmetic: none -> 1.99 us  [the longest x1 1.14 us: layer(): wide = lax.optimization_barrier(tokens.astype(F32))]
    unnamed x29 -> x33, local copies, waits for them, and re-layouts: 11.5 us -> 11.6 us
where the time goes in v4:
time: 195 us; the launch traced here: 193 us
  starting transfers between devices  100 us (51%)
  waiting for transfers between devices  59.7 us (31%)
  local copies, waits for them, and re-layouts  15.2 us (8%)
  matrix products  9.15 us (5%)
  other arithmetic  7.65 us (4%)
    all_to_all x4, starting transfers between devices, exchange(): return lax.all_to_all(a, axis, split_axis=0, concat_axis=0, tiled=True)  39.3 us
    all_to_all x4, waiting for transfers between devices, exchange(): return lax.all_to_all(a, axis, split_axis=0, concat_axis=0, tiled=True)  33.3 us
    ppermute x3, starting transfers between devices, layer(): lax.ppermute(column(j), 'y', ring(Y, j))  12.6 us
    unnamed x33, local copies, waits for them, and re-layouts  11.6 us
    ppermute x3, waiting for transfers between devices, gather_tp(): mine = [own] + [lax.ppermute(own, 'x', ring(X, k)) for k in (1, 3, 2)]  10.6 us
    ppermute x3, starting transfers between devices, layer(): near[k] = lax.ppermute(hidden, 'x', ring(X, k))  10.5 us
    ppermute x3, starting transfers between devices, gather_tp(): mine = [own] + [lax.ppermute(own, 'x', ring(X, k)) for k in (1, 3, 2)]  10.5 us
    ppermute x3, starting transfers between devices, layer(): cols.append(block if k == 0 else lax.ppermute(block, 'x', ring(X, k)))  9.48 us
  transfers between devices with their start and end apart: 25, of which 13 were waited for; matrix products, arithmetic and copies ran while one was open for 14% of the time, Pallas kernels for 0%

profile of v4, /device:TPU:2, one launch (start us, length us, event | category | flops | bytes accessed | tf_op | source)
XLA Modules:
  0.0 193.2 jit_solution(2728948655304537555)
XLA Ops:
  0.7 1.1 fusion.30
  1.8 1.5 fusion.18
  4.0 4.9 %collective-permute-start = (bf16[8,48,256]{2,1,0:T(8,128)(2,1)}, bf16[8,48,256]{2,1,0:T(8,128)(2,1)S(1)}, u32[]{:S(2)}, u32[]{:S(2)}) collective-permute-start(bf16[8,48,256]{2,1,0:T(8,128)(2,1)} %pad_maximum_fusion.3), channel_id=1, source_target_pairs={{0,24},{8,0},{16,8},{24,16},{1,25},{9,1},{17,9},{25,17},{2,26},{10... | collective-permute-start | bytes 589832 | tf_op jit(solution)/shard_map/ppermute | solution.py:93
  9.9 1.1 convert_element_type.97
  11.4 1.2 convolution_convert_fusion
  12.6 13.1 %all-to-all-start = ((bf16[32,32,256]{2,1,0:T(8,128)(2,1)}), bf16[32,32,256]{2,1,0:T(8,128)(2,1)S(1)}, u32[]{:S(2)}, u32[]{:S(2)}) async-start(bf16[32,32,256]{2,1,0:T(8,128)(2,1)} %bitcast.30), calls=%async_computation | async-start | bytes 1048576 | tf_op jit(solution)/shard_map/all_to_all | solution.py:25
  25.7 5.2 %collective-permute-start.1 = (bf16[8,48,256]{2,1,0:T(8,128)(2,1)S(1)}, bf16[8,48,256]{2,1,0:T(8,128)(2,1)S(1)}, u32[]{:S(2)}, u32[]{:S(2)}) collective-permute-start(bf16[8,48,256]{2,1,0:T(8,128)(2,1)S(1)} %pad_maximum_fusion.4), channel_id=1, source_target_pairs={{0,16},{8,24},{16,0},{24,8},{1,17},{9,25},{17,1},{25,9},{2,18},{10... | collective-permute-start | bytes 589832 | tf_op jit(solution)/shard_map/ppermute | solution.py:93
  31.0 2.5 %collective-permute-start.2 = (bf16[8,48,256]{2,1,0:T(8,128)(2,1)S(1)}, bf16[8,48,256]{2,1,0:T(8,128)(2,1)S(1)}, u32[]{:S(2)}, u32[]{:S(2)}) collective-permute-start(bf16[8,48,256]{2,1,0:T(8,128)(2,1)S(1)} %pad_maximum_fusion.5), channel_id=1, source_target_pairs={{0,8},{8,16},{16,24},{24,0},{1,9},{9,17},{17,25},{25,1},{2,10},{10... | collective-permute-start | bytes 589832 | tf_op jit(solution)/shard_map/ppermute | solution.py:93
  33.5 4.9 %collective-permute-done.1 = bf16[8,48,256]{2,1,0:T(8,128)(2,1)S(1)} collective-permute-done((bf16[8,48,256]{2,1,0:T(8,128)(2,1)S(1)}, bf16[8,48,256]{2,1,0:T(8,128)(2,1)S(1)}, u32[]{:S(2)}, u32[]{:S(2)}) %collective-permute-start.1) | collective-permute-done | bytes 196640 | tf_op jit(solution)/shard_map/ppermute | solution.py:93
  38.5 4.2 %collective-permute-done.2 = bf16[8,48,256]{2,1,0:T(8,128)(2,1)S(1)} collective-permute-done((bf16[8,48,256]{2,1,0:T(8,128)(2,1)S(1)}, bf16[8,48,256]{2,1,0:T(8,128)(2,1)S(1)}, u32[]{:S(2)}, u32[]{:S(2)}) %collective-permute-start.2) | collective-permute-done | bytes 196640 | tf_op jit(solution)/shard_map/ppermute | solution.py:93
  44.0 11.1 %all-to-all-done = bf16[32,32,256]{2,1,0:T(8,128)(2,1)S(1)} async-done(((bf16[32,32,256]{2,1,0:T(8,128)(2,1)}), bf16[32,32,256]{2,1,0:T(8,128)(2,1)S(1)}, u32[]{:S(2)}, u32[]{:S(2)}) %all-to-all-start) | async-done | bytes 524320 | tf_op jit(solution)/shard_map/all_to_all | solution.py:25
  55.0 7.7 %all-to-all-start.1 = ((bf16[16,128,256]{2,1,0:T(8,128)(2,1)}), bf16[16,128,256]{2,1,0:T(8,128)(2,1)S(1)}, u32[]{:S(2)}, u32[]{:S(2)}) async-start(bf16[16,128,256]{2,1,0:T(8,128)(2,1)} %pad_maximum_fusion), calls=%async_computation.1 | async-start | bytes 2097152 | tf_op jit(solution)/shard_map/all_to_all | solution.py:25
  62.7 3.4 %collective-permute-start.4 = (bf16[1024,256]{1,0:T(8,128)(2,1)S(1)}, bf16[1024,256]{1,0:T(8,128)(2,1)}, u32[]{:S(2)}, u32[]{:S(2)}) collective-permute-start(bf16[1024,256]{1,0:T(8,128)(2,1)S(1)} %bitcast.207), channel_id=1, source_target_pairs={{0,2},{2,4},{4,6},{6,0},{1,3},{3,5},{5,7},{7,1},{8,10},{10,12},{12... | collective-permute-start | bytes 1572872 | tf_op jit(solution)/shard_map/ppermute | solution.py:29
  66.1 3.0 %collective-permute-start.6 = (bf16[1024,256]{1,0:T(8,128)(2,1)S(1)}, bf16[1024,256]{1,0:T(8,128)(2,1)}, u32[]{:S(2)}, u32[]{:S(2)}) collective-permute-start(bf16[1024,256]{1,0:T(8,128)(2,1)S(1)} %bitcast.208), channel_id=1, source_target_pairs={{0,4},{2,6},{4,0},{6,2},{1,5},{3,7},{5,1},{7,3},{8,12},{10,14},{12... | collective-permute-start | bytes 1572872 | tf_op jit(solution)/shard_map/ppermute | solution.py:29
  69.2 4.1 %collective-permute-start.8 = (bf16[1024,256]{1,0:T(8,128)(2,1)S(1)}, bf16[1024,256]{1,0:T(8,128)(2,1)}, u32[]{:S(2)}, u32[]{:S(2)}) collective-permute-start(bf16[1024,256]{1,0:T(8,128)(2,1)S(1)} %bitcast.209), channel_id=1, source_target_pairs={{0,6},{2,0},{4,2},{6,4},{1,7},{3,1},{5,3},{7,5},{8,14},{10,8},{12,... | collective-permute-start | bytes 1572872 | tf_op jit(solution)/shard_map/ppermute | solution.py:29
  73.2 1.9 collective-permute-start.3
  75.3 4.3 %collective-permute-done.4 = bf16[1024,256]{1,0:T(8,128)(2,1)} collective-permute-done((bf16[1024,256]{1,0:T(8,128)(2,1)S(1)}, bf16[1024,256]{1,0:T(8,128)(2,1)}, u32[]{:S(2)}, u32[]{:S(2)}) %collective-permute-start.4) | collective-permute-done | bytes 524320 | tf_op jit(solution)/shard_map/ppermute | solution.py:29
  79.5 1.9 collective-permute-start.5
  82.3 2.1 %collective-permute-done.6 = bf16[1024,256]{1,0:T(8,128)(2,1)} collective-permute-done((bf16[1024,256]{1,0:T(8,128)(2,1)S(1)}, bf16[1024,256]{1,0:T(8,128)(2,1)}, u32[]{:S(2)}, u32[]{:S(2)}) %collective-permute-start.6) | collective-permute-done | bytes 524320 | tf_op jit(solution)/shard_map/ppermute | solution.py:29
  84.4 1.9 collective-permute-start.7
  87.2 4.2 %collective-permute-done.8 = bf16[1024,256]{1,0:T(8,128)(2,1)} collective-permute-done((bf16[1024,256]{1,0:T(8,128)(2,1)S(1)}, bf16[1024,256]{1,0:T(8,128)(2,1)}, u32[]{:S(2)}, u32[]{:S(2)}) %collective-permute-start.8) | collective-permute-done | bytes 524320 | tf_op jit(solution)/shard_map/ppermute | solution.py:29
  91.4 1.9 collective-permute-start.9
  93.3 1.9 constant_dynamic-update-slice_fusion.6
  95.2 1.9 constant_dynamic-update-slice_fusion.5
  98.0 1.9 %constant_dynamic-update-slice_fusion.3 = bf16[1024,2048]{1,0:T(8,128)(2,1)} fusion(bf16[1024,2048]{1,0:T(8,128)(2,1)} %constant_dynamic-update-slice_fusion.4, bf16[1024,256]{1,0:T(8,128)(2,1)} %collective-permute-done.6), kind=kLoop, calls=%fused_computation.99 | loop fusion | bytes 1048576
  100.8 1.9 constant_dynamic-update-slice_fusion.1
  102.7 6.3 %all-to-all-done.1 = bf16[16,128,256]{2,1,0:T(8,128)(2,1)S(1)} async-done(((bf16[16,128,256]{2,1,0:T(8,128)(2,1)}), bf16[16,128,256]{2,1,0:T(8,128)(2,1)S(1)}, u32[]{:S(2)}, u32[]{:S(2)}) %all-to-all-start.1) | async-done | bytes 1048608 | tf_op jit(solution)/shard_map/all_to_all | solution.py:25
  109.0 9.0 %all-to-all-start.2 = ((bf16[16,64,256]{2,1,0:T(8,128)(2,1)}), bf16[16,64,256]{2,1,0:T(8,128)(2,1)S(1)}, u32[]{:S(2)}, u32[]{:S(2)}) async-start(bf16[16,64,256]{2,1,0:T(8,128)(2,1)} %pad_maximum_fusion.2), calls=%async_computation.2 | async-start | bytes 1048576 | tf_op jit(solution)/shard_map/all_to_all | solution.py:25
  119.1 3.4 %fusion.61 = f32[1024,256]{1,0:T(8,128)S(1)} fusion(bf16[1024,2048]{1,0:T(8,128)(2,1)} %constant_dynamic-update-slice_fusion, bf16[2048,256]{1,0:T(8,128)(2,1)S(1)} %bitcast_dynamic-update-slice_fusion.12), kind=kOutput, calls=%fused_computation.146 | convolution fusion | flops 1073741824 | bytes 6291456 | tf_op jit(solution)/shard_map/dot_general | solution.py:112
  122.8 3.4 %collective-permute-start.11 = (bf16[1024,128]{1,0:T(8,128)(2,1)S(1)}, bf16[1024,128]{1,0:T(8,128)(2,1)S(1)}, u32[]{:S(2)}, u32[]{:S(2)}) collective-permute-start(bf16[1024,128]{1,0:T(8,128)(2,1)S(1)} %fusion.8), channel_id=1, source_target_pairs={{0,2},{2,4},{4,6},{6,0},{1,3},{3,5},{5,7},{7,1},{8,10},{10,12},{12... | collective-permute-start | bytes 786440 | tf_op jit(solution)/shard_map/ppermute | solution.py:123
  126.2 3.0 %collective-permute-start.13 = (bf16[1024,128]{1,0:T(8,128)(2,1)S(1)}, bf16[1024,128]{1,0:T(8,128)(2,1)}, u32[]{:S(2)}, u32[]{:S(2)}) collective-permute-start(bf16[1024,128]{1,0:T(8,128)(2,1)S(1)} %fusion.8), channel_id=1, source_target_pairs={{0,4},{2,6},{4,0},{6,2},{1,5},{3,7},{5,1},{7,3},{8,12},{10,14},{12... | collective-permute-start | bytes 786440 | tf_op jit(solution)/shard_map/ppermute | solution.py:123
  129.2 4.1 %collective-permute-start.15 = (bf16[1024,128]{1,0:T(8,128)(2,1)S(1)}, bf16[1024,128]{1,0:T(8,128)(2,1)S(1)}, u32[]{:S(2)}, u32[]{:S(2)}) collective-permute-start(bf16[1024,128]{1,0:T(8,128)(2,1)S(1)} %fusion.8), channel_id=1, source_target_pairs={{0,6},{2,0},{4,2},{6,4},{1,7},{3,1},{5,3},{7,5},{8,14},{10,8},{12,... | collective-permute-start | bytes 786440 | tf_op jit(solution)/shard_map/ppermute | solution.py:123
  133.3 1.9 collective-permute-start.10
  135.2 2.4 %collective-permute-start.12 = (bf16[1024,128]{1,0:T(8,128)(2,1)S(1)}, bf16[1024,128]{1,0:T(8,128)(2,1)S(1)}, u32[]{:S(2)}, u32[]{:S(2)}) collective-permute-start(bf16[1024,128]{1,0:T(8,128)(2,1)S(1)} %collective-permute-done.11), channel_id=1, source_target_pairs={{0,1},{1,0},{2,3},{3,2},{4,5},{5,4},{6,7},{7,6},{8,9},{9,8},{10,11... | collective-permute-start | bytes 786440 | tf_op jit(solution)/shard_map/ppermute | solution.py:124
  137.6 1.3 collective-permute-done.13
  138.9 1.9 collective-permute-start.14
  140.8 1.3 collective-permute-done.15
  142.1 1.9 collective-permute-start.16
  144.0 2.4 %all-to-all-done.2 = bf16[16,64,256]{2,1,0:T(8,128)(2,1)S(1)} async-done(((bf16[16,64,256]{2,1,0:T(8,128)(2,1)}), bf16[16,64,256]{2,1,0:T(8,128)(2,1)S(1)}, u32[]{:S(2)}, u32[]{:S(2)}) %all-to-all-start.2) | async-done | bytes 524320 | tf_op jit(solution)/shard_map/all_to_all | solution.py:25
  147.2 1.2 fusion.35
  150.6 1.9 collective-permute-start.17
  152.9 9.5 %all-to-all-start.3 = ((bf16[32,32,256]{2,1,0:T(8,128)(2,1)}), bf16[32,32,256]{2,1,0:T(8,128)(2,1)S(1)}, u32[]{:S(2)}, u32[]{:S(2)}) async-start(bf16[32,32,256]{2,1,0:T(8,128)(2,1)} %bitcast.51), calls=%async_computation.3 | async-start | bytes 1048576 | tf_op jit(solution)/shard_map/all_to_all | solution.py:25
  162.5 2.1 %collective-permute-start.18 = (bf16[128,512]{1,0:T(8,128)(2,1)S(1)}, bf16[128,512]{1,0:T(8,128)(2,1)S(1)}, u32[]{:S(2)}, u32[]{:S(2)}) collective-permute-start(bf16[128,512]{1,0:T(8,128)(2,1)S(1)} %get-tuple-element.40), channel_id=1, source_target_pairs={{0,6},{2,0},{4,2},{6,4},{1,7},{3,1},{5,3},{7,5},{8,14},{10,8},{12,... | collective-permute-start | bytes 393224 | tf_op jit(solution)/shard_map/ppermute | solution.py:141
  165.6 3.8 %collective-permute-start.19 = (bf16[128,512]{1,0:T(8,128)(2,1)S(1)}, bf16[128,512]{1,0:T(8,128)(2,1)S(1)}, u32[]{:S(2)}, u32[]{:S(2)}) collective-permute-start(bf16[128,512]{1,0:T(8,128)(2,1)S(1)} %get-tuple-element.41), channel_id=1, source_target_pairs={{0,4},{2,6},{4,0},{6,2},{1,5},{3,7},{5,1},{7,3},{8,12},{10,14},{12... | collective-permute-start | bytes 393224 | tf_op jit(solution)/shard_map/ppermute | solution.py:141
  169.4 3.6 %collective-permute-start.20 = (bf16[128,512]{1,0:T(8,128)(2,1)S(1)}, bf16[128,512]{1,0:T(8,128)(2,1)S(1)}, u32[]{:S(2)}, u32[]{:S(2)}) collective-permute-start(bf16[128,512]{1,0:T(8,128)(2,1)S(1)} %get-tuple-element.38), channel_id=1, source_target_pairs={{0,2},{2,4},{4,6},{6,0},{1,3},{3,5},{5,7},{7,1},{8,10},{10,12},{12... | collective-permute-start | bytes 393224 | tf_op jit(solution)/shard_map/ppermute | solution.py:141
  173.1 1.3 collective-permute-done.19
  174.4 2.8 %collective-permute-done.20 = bf16[128,512]{1,0:T(8,128)(2,1)S(1)} collective-permute-done((bf16[128,512]{1,0:T(8,128)(2,1)S(1)}, bf16[128,512]{1,0:T(8,128)(2,1)S(1)}, u32[]{:S(2)}, u32[]{:S(2)}) %collective-permute-start.20) | collective-permute-done | bytes 131104 | tf_op jit(solution)/shard_map/ppermute | solution.py:141
  178.6 13.6 %all-to-all-done.3 = bf16[32,32,256]{2,1,0:T(8,128)(2,1)S(1)} async-done(((bf16[32,32,256]{2,1,0:T(8,128)(2,1)}), bf16[32,32,256]{2,1,0:T(8,128)(2,1)S(1)}, u32[]{:S(2)}, u32[]{:S(2)}) %all-to-all-start.3) | async-done | bytes 524320 | tf_op jit(solution)/shard_map/all_to_all | solution.py:25
  (81 shorter events, 14.7 us)
Async XLA Ops:
  4.0 29.5 %collective-permute-start = (bf16[8,48,256]{2,1,0:T(8,128)(2,1)}, bf16[8,48,256]{2,1,0:T(8,128)(2,1)S(1)}, u32[]{:S(2)}, u32[]{:S(2)}) collective-permute-start(bf16[8,48,256]{2,1,0:T(8,128)(2,1)} %pad_maximum_fusion.3), channel_id=1, source_target_pairs={{0,24},{8,0},{16,8},{24,16},{1,25},{9,1},{17,9},{25,17},{2,26},{10... | collective-permute-start | bytes 589832 | tf_op jit(solution)/shard_map/ppermute | solution.py:93
  9.9 23.6 %copy-start = (s32[1024]{0:T(1024)}, s32[1024]{0:T(1024)S(1)}, u32[]{:S(2)}) copy-start(s32[1024]{0:T(1024)S(1)} %eq.79) | copy-start | bytes 12292
  12.6 42.5 %all-to-all-start = ((bf16[32,32,256]{2,1,0:T(8,128)(2,1)}), bf16[32,32,256]{2,1,0:T(8,128)(2,1)S(1)}, u32[]{:S(2)}, u32[]{:S(2)}) async-start(bf16[32,32,256]{2,1,0:T(8,128)(2,1)} %bitcast.30), calls=%async_computation | async-start | bytes 1048576 | tf_op jit(solution)/shard_map/all_to_all | solution.py:25
  25.7 12.7 %collective-permute-start.1 = (bf16[8,48,256]{2,1,0:T(8,128)(2,1)S(1)}, bf16[8,48,256]{2,1,0:T(8,128)(2,1)S(1)}, u32[]{:S(2)}, u32[]{:S(2)}) collective-permute-start(bf16[8,48,256]{2,1,0:T(8,128)(2,1)S(1)} %pad_maximum_fusion.4), channel_id=1, source_target_pairs={{0,16},{8,24},{16,0},{24,8},{1,17},{9,25},{17,1},{25,9},{2,18},{10... | collective-permute-start | bytes 589832 | tf_op jit(solution)/shard_map/ppermute | solution.py:93
  31.0 11.7 %collective-permute-start.2 = (bf16[8,48,256]{2,1,0:T(8,128)(2,1)S(1)}, bf16[8,48,256]{2,1,0:T(8,128)(2,1)S(1)}, u32[]{:S(2)}, u32[]{:S(2)}) collective-permute-start(bf16[8,48,256]{2,1,0:T(8,128)(2,1)S(1)} %pad_maximum_fusion.5), channel_id=1, source_target_pairs={{0,8},{8,16},{16,24},{24,0},{1,9},{9,17},{17,25},{25,1},{2,10},{10... | collective-permute-start | bytes 589832 | tf_op jit(solution)/shard_map/ppermute | solution.py:93
  55.0 54.0 %all-to-all-start.1 = ((bf16[16,128,256]{2,1,0:T(8,128)(2,1)}), bf16[16,128,256]{2,1,0:T(8,128)(2,1)S(1)}, u32[]{:S(2)}, u32[]{:S(2)}) async-start(bf16[16,128,256]{2,1,0:T(8,128)(2,1)} %pad_maximum_fusion), calls=%async_computation.1 | async-start | bytes 2097152 | tf_op jit(solution)/shard_map/all_to_all | solution.py:25
  62.7 16.8 %collective-permute-start.4 = (bf16[1024,256]{1,0:T(8,128)(2,1)S(1)}, bf16[1024,256]{1,0:T(8,128)(2,1)}, u32[]{:S(2)}, u32[]{:S(2)}) collective-permute-start(bf16[1024,256]{1,0:T(8,128)(2,1)S(1)} %bitcast.207), channel_id=1, source_target_pairs={{0,2},{2,4},{4,6},{6,0},{1,3},{3,5},{5,7},{7,1},{8,10},{10,12},{12... | collective-permute-start | bytes 1572872 | tf_op jit(solution)/shard_map/ppermute | solution.py:29
  66.1 18.3 %collective-permute-start.6 = (bf16[1024,256]{1,0:T(8,128)(2,1)S(1)}, bf16[1024,256]{1,0:T(8,128)(2,1)}, u32[]{:S(2)}, u32[]{:S(2)}) collective-permute-start(bf16[1024,256]{1,0:T(8,128)(2,1)S(1)} %bitcast.208), channel_id=1, source_target_pairs={{0,4},{2,6},{4,0},{6,2},{1,5},{3,7},{5,1},{7,3},{8,12},{10,14},{12... | collective-permute-start | bytes 1572872 | tf_op jit(solution)/shard_map/ppermute | solution.py:29
  69.2 22.2 %collective-permute-start.8 = (bf16[1024,256]{1,0:T(8,128)(2,1)S(1)}, bf16[1024,256]{1,0:T(8,128)(2,1)}, u32[]{:S(2)}, u32[]{:S(2)}) collective-permute-start(bf16[1024,256]{1,0:T(8,128)(2,1)S(1)} %bitcast.209), channel_id=1, source_target_pairs={{0,6},{2,0},{4,2},{6,4},{1,7},{3,1},{5,3},{7,5},{8,14},{10,8},{12,... | collective-permute-start | bytes 1572872 | tf_op jit(solution)/shard_map/ppermute | solution.py:29
  73.2 20.1 %collective-permute-start.3 = (bf16[1024,256]{1,0:T(8,128)(2,1)S(1)}, bf16[1024,256]{1,0:T(8,128)(2,1)}, u32[]{:S(2)}, u32[]{:S(2)}) collective-permute-start(bf16[1024,256]{1,0:T(8,128)(2,1)S(1)} %bitcast.210), channel_id=1, source_target_pairs={{0,1},{1,0},{2,3},{3,2},{4,5},{5,4},{6,7},{7,6},{8,9},{9,8},{10,11... | collective-permute-start | bytes 1572872 | tf_op jit(solution)/shard_map/ppermute | solution.py:31
  79.5 17.6 %collective-permute-start.5 = (bf16[1024,256]{1,0:T(8,128)(2,1)}, bf16[1024,256]{1,0:T(8,128)(2,1)S(1)}, u32[]{:S(2)}, u32[]{:S(2)}) collective-permute-start(bf16[1024,256]{1,0:T(8,128)(2,1)} %collective-permute-done.4), channel_id=1, source_target_pairs={{0,1},{1,0},{2,3},{3,2},{4,5},{5,4},{6,7},{7,6},{8,9},{9,8},{10,11... | collective-permute-start | bytes 1572872 | tf_op jit(solution)/shard_map/ppermute | solution.py:31
  84.4 15.5 %collective-permute-start.7 = (bf16[1024,256]{1,0:T(8,128)(2,1)}, bf16[1024,256]{1,0:T(8,128)(2,1)S(1)}, u32[]{:S(2)}, u32[]{:S(2)}) collective-permute-start(bf16[1024,256]{1,0:T(8,128)(2,1)} %collective-permute-done.6), channel_id=1, source_target_pairs={{0,1},{1,0},{2,3},{3,2},{4,5},{5,4},{6,7},{7,6},{8,9},{9,8},{10,11... | collective-permute-start | bytes 1572872 | tf_op jit(solution)/shard_map/ppermute | solution.py:31
  91.4 26.6 %collective-permute-start.9 = (bf16[1024,256]{1,0:T(8,128)(2,1)}, bf16[1024,256]{1,0:T(8,128)(2,1)S(1)}, u32[]{:S(2)}, u32[]{:S(2)}) collective-permute-start(bf16[1024,256]{1,0:T(8,128)(2,1)} %collective-permute-done.8), channel_id=1, source_target_pairs={{0,1},{1,0},{2,3},{3,2},{4,5},{5,4},{6,7},{7,6},{8,9},{9,8},{10,11... | collective-permute-start | bytes 1572872 | tf_op jit(solution)/shard_map/ppermute | solution.py:31
  109.0 37.4 %all-to-all-start.2 = ((bf16[16,64,256]{2,1,0:T(8,128)(2,1)}), bf16[16,64,256]{2,1,0:T(8,128)(2,1)S(1)}, u32[]{:S(2)}, u32[]{:S(2)}) async-start(bf16[16,64,256]{2,1,0:T(8,128)(2,1)} %pad_maximum_fusion.2), calls=%async_computation.2 | async-start | bytes 1048576 | tf_op jit(solution)/shard_map/all_to_all | solution.py:25
  122.8 12.4 %collective-permute-start.11 = (bf16[1024,128]{1,0:T(8,128)(2,1)S(1)}, bf16[1024,128]{1,0:T(8,128)(2,1)S(1)}, u32[]{:S(2)}, u32[]{:S(2)}) collective-permute-start(bf16[1024,128]{1,0:T(8,128)(2,1)S(1)} %fusion.8), channel_id=1, source_target_pairs={{0,2},{2,4},{4,6},{6,0},{1,3},{3,5},{5,7},{7,1},{8,10},{10,12},{12... | collective-permute-start | bytes 786440 | tf_op jit(solution)/shard_map/ppermute | solution.py:123
  126.2 12.7 %collective-permute-start.13 = (bf16[1024,128]{1,0:T(8,128)(2,1)S(1)}, bf16[1024,128]{1,0:T(8,128)(2,1)}, u32[]{:S(2)}, u32[]{:S(2)}) collective-permute-start(bf16[1024,128]{1,0:T(8,128)(2,1)S(1)} %fusion.8), channel_id=1, source_target_pairs={{0,4},{2,6},{4,0},{6,2},{1,5},{3,7},{5,1},{7,3},{8,12},{10,14},{12... | collective-permute-start | bytes 786440 | tf_op jit(solution)/shard_map/ppermute | solution.py:123
  129.2 12.9 %collective-permute-start.15 = (bf16[1024,128]{1,0:T(8,128)(2,1)S(1)}, bf16[1024,128]{1,0:T(8,128)(2,1)S(1)}, u32[]{:S(2)}, u32[]{:S(2)}) collective-permute-start(bf16[1024,128]{1,0:T(8,128)(2,1)S(1)} %fusion.8), channel_id=1, source_target_pairs={{0,6},{2,0},{4,2},{6,4},{1,7},{3,1},{5,3},{7,5},{8,14},{10,8},{12,... | collective-permute-start | bytes 786440 | tf_op jit(solution)/shard_map/ppermute | solution.py:123
  133.3 13.4 %collective-permute-start.10 = (bf16[1024,128]{1,0:T(8,128)(2,1)S(1)}, bf16[1024,128]{1,0:T(8,128)(2,1)S(1)}, u32[]{:S(2)}, u32[]{:S(2)}) collective-permute-start(bf16[1024,128]{1,0:T(8,128)(2,1)S(1)} %fusion.8), channel_id=1, source_target_pairs={{0,1},{1,0},{2,3},{3,2},{4,5},{5,4},{6,7},{7,6},{8,9},{9,8},{10,11... | collective-permute-start | bytes 786440 | tf_op jit(solution)/shard_map/ppermute | solution.py:124
  135.2 13.3 %collective-permute-start.12 = (bf16[1024,128]{1,0:T(8,128)(2,1)S(1)}, bf16[1024,128]{1,0:T(8,128)(2,1)S(1)}, u32[]{:S(2)}, u32[]{:S(2)}) collective-permute-start(bf16[1024,128]{1,0:T(8,128)(2,1)S(1)} %collective-permute-done.11), channel_id=1, source_target_pairs={{0,1},{1,0},{2,3},{3,2},{4,5},{5,4},{6,7},{7,6},{8,9},{9,8},{10,11... | collective-permute-start | bytes 786440 | tf_op jit(solution)/shard_map/ppermute | solution.py:124
  138.9 10.2 %collective-permute-start.14 = (bf16[1024,128]{1,0:T(8,128)(2,1)}, bf16[1024,128]{1,0:T(8,128)(2,1)S(1)}, u32[]{:S(2)}, u32[]{:S(2)}) collective-permute-start(bf16[1024,128]{1,0:T(8,128)(2,1)} %collective-permute-done.13), channel_id=1, source_target_pairs={{0,1},{1,0},{2,3},{3,2},{4,5},{5,4},{6,7},{7,6},{8,9},{9,8},{10,11... | collective-permute-start | bytes 786440 | tf_op jit(solution)/shard_map/ppermute | solution.py:124
  142.1 7.3 %collective-permute-start.16 = (bf16[1024,128]{1,0:T(8,128)(2,1)S(1)}, bf16[1024,128]{1,0:T(8,128)(2,1)S(1)}, u32[]{:S(2)}, u32[]{:S(2)}) collective-permute-start(bf16[1024,128]{1,0:T(8,128)(2,1)S(1)} %collective-permute-done.15), channel_id=1, source_target_pairs={{0,1},{1,0},{2,3},{3,2},{4,5},{5,4},{6,7},{7,6},{8,9},{9,8},{10,11... | collective-permute-start | bytes 786440 | tf_op jit(solution)/shard_map/ppermute | solution.py:124
  148.8 3.8 %copy-start.2 = (s32[128,4]{0,1:T(4,128)S(1)}, s32[128,4]{0,1:T(4,128)}, u32[]{:S(2)}) copy-start(s32[128,4]{0,1:T(4,128)} %param.12) | copy-start | bytes 6148
  148.8 3.8 %copy-start.3 = (f32[128,4]{0,1:T(4,128)S(1)}, f32[128,4]{0,1:T(4,128)}, u32[]{:S(2)}) copy-start(f32[128,4]{0,1:T(4,128)} %param.13) | copy-start | bytes 6148
  148.8 3.8 %copy-start.1 = (s32[1024]{0:T(1024)S(1)}, s32[1024]{0:T(1024)}, u32[]{:S(2)}) copy-start(s32[1024]{0:T(1024)} %copy-done) | copy-start | bytes 12292
  150.6 11.8 %collective-permute-start.17 = (bf16[4,128,256]{2,1,0:T(8,128)(2,1)S(1)}, bf16[4,128,256]{2,1,0:T(8,128)(2,1)S(1)}, u32[]{:S(2)}, u32[]{:S(2)}) collective-permute-start(bf16[4,128,256]{2,1,0:T(8,128)(2,1)S(1)} %dynamic-slice_bitcast_fusion.1), channel_id=1, source_target_pairs={{0,1},{1,0},{2,3},{3,2},{4,5},{5,4},{6,7},{7,6},{8,9},{9,8},{10,11... | collective-permute-start | bytes 786440 | tf_op jit(solution)/shard_map/ppermute | solution.py:134
  152.9 39.4 %all-to-all-start.3 = ((bf16[32,32,256]{2,1,0:T(8,128)(2,1)}), bf16[32,32,256]{2,1,0:T(8,128)(2,1)S(1)}, u32[]{:S(2)}, u32[]{:S(2)}) async-start(bf16[32,32,256]{2,1,0:T(8,128)(2,1)} %bitcast.51), calls=%async_computation.3 | async-start | bytes 1048576 | tf_op jit(solution)/shard_map/all_to_all | solution.py:25
  162.5 10.5 %collective-permute-start.18 = (bf16[128,512]{1,0:T(8,128)(2,1)S(1)}, bf16[128,512]{1,0:T(8,128)(2,1)S(1)}, u32[]{:S(2)}, u32[]{:S(2)}) collective-permute-start(bf16[128,512]{1,0:T(8,128)(2,1)S(1)} %get-tuple-element.40), channel_id=1, source_target_pairs={{0,6},{2,0},{4,2},{6,4},{1,7},{3,1},{5,3},{7,5},{8,14},{10,8},{12,... | collective-permute-start | bytes 393224 | tf_op jit(solution)/shard_map/ppermute | solution.py:141
  165.6 8.7 %collective-permute-start.19 = (bf16[128,512]{1,0:T(8,128)(2,1)S(1)}, bf16[128,512]{1,0:T(8,128)(2,1)S(1)}, u32[]{:S(2)}, u32[]{:S(2)}) collective-permute-start(bf16[128,512]{1,0:T(8,128)(2,1)S(1)} %get-tuple-element.41), channel_id=1, source_target_pairs={{0,4},{2,6},{4,0},{6,2},{1,5},{3,7},{5,1},{7,3},{8,12},{10,14},{12... | collective-permute-start | bytes 393224 | tf_op jit(solution)/shard_map/ppermute | solution.py:141
  169.4 7.8 %collective-permute-start.20 = (bf16[128,512]{1,0:T(8,128)(2,1)S(1)}, bf16[128,512]{1,0:T(8,128)(2,1)S(1)}, u32[]{:S(2)}, u32[]{:S(2)}) collective-permute-start(bf16[128,512]{1,0:T(8,128)(2,1)S(1)} %get-tuple-element.38), channel_id=1, source_target_pairs={{0,2},{2,4},{4,6},{6,0},{1,3},{3,5},{5,7},{7,1},{8,10},{10,12},{12... | collective-permute-start | bytes 393224 | tf_op jit(solution)/shard_map/ppermute | solution.py:141

commit v5 on v3

--- a/solution.py
+++ b/solution.py
@@ -68,9 +68,9 @@
     at_slot = place[:, None, :] == jnp.arange(CAP, dtype=jnp.int32)[None, :, None]
     pick = at_slot.astype(BF).reshape(n_exp * CAP, n_tok)
 
-    wide = tokens.astype(F32)
+    wide = lax.optimization_barrier(tokens.astype(F32))
     scale = lax.rsqrt(jnp.mean(wide * wide, axis=1, keepdims=True) + NORM_EPSILON)
-    own = lax.dynamic_slice_in_dim(tokens, (ix * C + ic) * part, part, 1).astype(F32)
+    own = lax.dynamic_slice_in_dim(wide, (ix * C + ic) * part, part, 1)
     normed = (own * scale).astype(BF)
     slots = jnp.dot(pick, normed, preferred_element_type=F32).astype(BF)
     arrived = exchange(slots.reshape(n_exp, CAP, part), FS)
@@ -119,7 +119,7 @@
         * jax.nn.sigmoid(SLOPE_ALPHA * clipped)
     ).astype(BF)
     near = [hidden, None, None, None]
-    for k in (1, 3, 2):
+    for k in (2, 1, 3):
         near[k] = lax.ppermute(hidden, "x", ring(X, k))
     other = [lax.ppermute(a, "c", ring(C, 1)) for a in near]
     pairs = [(near[k], other[k]) for k in range(X)]

time: 195 us -> 194 us (level)
  no operation moved by 1% of the time
where the time goes in v5:
time: 194 us; the launch traced here: 193 us
  starting transfers between devices  100 us (52%)
  waiting for transfers between devices  59.7 us (31%)
  local copies, waits for them, and re-layouts  15.1 us (8%)
  matrix products  9.97 us (5%)
  other arithmetic  6.73 us (3%)
    all_to_all x4, starting transfers between devices, exchange(): return lax.all_to_all(a, axis, split_axis=0, concat_axis=0, tiled=True)  39.3 us
    all_to_all x4, waiting for transfers between devices, exchange(): return lax.all_to_all(a, axis, split_axis=0, concat_axis=0, tiled=True)  33.3 us
    ppermute x3, starting transfers between devices, layer(): lax.ppermute(column(j), 'y', ring(Y, j))  12.6 us
    unnamed x29, local copies, waits for them, and re-layouts  11.5 us
    ppermute x3, waiting for transfers between devices, gather_tp(): mine = [own] + [lax.ppermute(own, 'x', ring(X, k)) for k in (1, 3, 2)]  10.5 us
    ppermute x3, starting transfers between devices, gather_tp(): mine = [own] + [lax.ppermute(own, 'x', ring(X, k)) for k in (1, 3, 2)]  10.5 us
    ppermute x3, starting transfers between devices, layer(): near[k] = lax.ppermute(hidden, 'x', ring(X, k))  10.5 us
    ppermute x3, starting transfers between devices, layer(): cols.append(block if k == 0 else lax.ppermute(block, 'x', ring(X, k)))  9.47 us
  transfers between devices with their start and end apart: 25, of which 13 were waited for; matrix products, arithmetic and copies ran while one was open for 14% of the time, Pallas kernels for 0%

profile of v5, /device:TPU:2, one launch (start us, length us, event | category | flops | bytes accessed | tf_op | source)
XLA Modules:
  0.0 193.1 jit_solution(16361786008257246515)
XLA Ops:
  0.7 1.1 fusion.38
  1.8 1.5 fusion.26
  4.0 4.9 %collective-permute-start = (bf16[8,48,256]{2,1,0:T(8,128)(2,1)}, bf16[8,48,256]{2,1,0:T(8,128)(2,1)S(1)}, u32[]{:S(2)}, u32[]{:S(2)}) collective-permute-start(bf16[8,48,256]{2,1,0:T(8,128)(2,1)} %pad_maximum_fusion.2), channel_id=1, source_target_pairs={{0,24},{8,0},{16,8},{24,16},{1,25},{9,1},{17,9},{25,17},{2,26},{10... | collective-permute-start | bytes 589832 | tf_op jit(solution)/shard_map/ppermute | solution.py:93
  9.9 1.1 convert_element_type.98
  11.4 1.2 convolution_convert_fusion
  12.6 13.1 %all-to-all-start = ((bf16[32,32,256]{2,1,0:T(8,128)(2,1)}), bf16[32,32,256]{2,1,0:T(8,128)(2,1)S(1)}, u32[]{:S(2)}, u32[]{:S(2)}) async-start(bf16[32,32,256]{2,1,0:T(8,128)(2,1)} %bitcast.29), calls=%async_computation | async-start | bytes 1048576 | tf_op jit(solution)/shard_map/all_to_all | solution.py:25
  25.7 5.2 %collective-permute-start.1 = (bf16[8,48,256]{2,1,0:T(8,128)(2,1)S(1)}, bf16[8,48,256]{2,1,0:T(8,128)(2,1)S(1)}, u32[]{:S(2)}, u32[]{:S(2)}) collective-permute-start(bf16[8,48,256]{2,1,0:T(8,128)(2,1)S(1)} %pad_maximum_fusion.3), channel_id=1, source_target_pairs={{0,16},{8,24},{16,0},{24,8},{1,17},{9,25},{17,1},{25,9},{2,18},{10... | collective-permute-start | bytes 589832 | tf_op jit(solution)/shard_map/ppermute | solution.py:93
  31.0 2.5 %collective-permute-start.2 = (bf16[8,48,256]{2,1,0:T(8,128)(2,1)S(1)}, bf16[8,48,256]{2,1,0:T(8,128)(2,1)S(1)}, u32[]{:S(2)}, u32[]{:S(2)}) collective-permute-start(bf16[8,48,256]{2,1,0:T(8,128)(2,1)S(1)} %pad_maximum_fusion.4), channel_id=1, source_target_pairs={{0,8},{8,16},{16,24},{24,0},{1,9},{9,17},{17,25},{25,1},{2,10},{10... | collective-permute-start | bytes 589832 | tf_op jit(solution)/shard_map/ppermute | solution.py:93
  33.5 4.9 %collective-permute-done.1 = bf16[8,48,256]{2,1,0:T(8,128)(2,1)S(1)} collective-permute-done((bf16[8,48,256]{2,1,0:T(8,128)(2,1)S(1)}, bf16[8,48,256]{2,1,0:T(8,128)(2,1)S(1)}, u32[]{:S(2)}, u32[]{:S(2)}) %collective-permute-start.1) | collective-permute-done | bytes 196640 | tf_op jit(solution)/shard_map/ppermute | solution.py:93
  38.5 4.2 %collective-permute-done.2 = bf16[8,48,256]{2,1,0:T(8,128)(2,1)S(1)} collective-permute-done((bf16[8,48,256]{2,1,0:T(8,128)(2,1)S(1)}, bf16[8,48,256]{2,1,0:T(8,128)(2,1)S(1)}, u32[]{:S(2)}, u32[]{:S(2)}) %collective-permute-start.2) | collective-permute-done | bytes 196640 | tf_op jit(solution)/shard_map/ppermute | solution.py:93
  44.0 11.1 %all-to-all-done = bf16[32,32,256]{2,1,0:T(8,128)(2,1)S(1)} async-done(((bf16[32,32,256]{2,1,0:T(8,128)(2,1)}), bf16[32,32,256]{2,1,0:T(8,128)(2,1)S(1)}, u32[]{:S(2)}, u32[]{:S(2)}) %all-to-all-start) | async-done | bytes 524320 | tf_op jit(solution)/shard_map/all_to_all | solution.py:25
  55.0 7.7 %all-to-all-start.1 = ((bf16[16,128,256]{2,1,0:T(8,128)(2,1)}), bf16[16,128,256]{2,1,0:T(8,128)(2,1)S(1)}, u32[]{:S(2)}, u32[]{:S(2)}) async-start(bf16[16,128,256]{2,1,0:T(8,128)(2,1)} %pad_maximum_fusion), calls=%async_computation.1 | async-start | bytes 2097152 | tf_op jit(solution)/shard_map/all_to_all | solution.py:25
  62.7 3.4 %collective-permute-start.4 = (bf16[1024,256]{1,0:T(8,128)(2,1)S(1)}, bf16[1024,256]{1,0:T(8,128)(2,1)}, u32[]{:S(2)}, u32[]{:S(2)}) collective-permute-start(bf16[1024,256]{1,0:T(8,128)(2,1)S(1)} %bitcast.204), channel_id=1, source_target_pairs={{0,2},{2,4},{4,6},{6,0},{1,3},{3,5},{5,7},{7,1},{8,10},{10,12},{12... | collective-permute-start | bytes 1572872 | tf_op jit(solution)/shard_map/ppermute | solution.py:29
  66.1 3.0 %collective-permute-start.6 = (bf16[1024,256]{1,0:T(8,128)(2,1)S(1)}, bf16[1024,256]{1,0:T(8,128)(2,1)}, u32[]{:S(2)}, u32[]{:S(2)}) collective-permute-start(bf16[1024,256]{1,0:T(8,128)(2,1)S(1)} %bitcast.205), channel_id=1, source_target_pairs={{0,4},{2,6},{4,0},{6,2},{1,5},{3,7},{5,1},{7,3},{8,12},{10,14},{12... | collective-permute-start | bytes 1572872 | tf_op jit(solution)/shard_map/ppermute | solution.py:29
  69.2 4.1 %collective-permute-start.8 = (bf16[1024,256]{1,0:T(8,128)(2,1)S(1)}, bf16[1024,256]{1,0:T(8,128)(2,1)}, u32[]{:S(2)}, u32[]{:S(2)}) collective-permute-start(bf16[1024,256]{1,0:T(8,128)(2,1)S(1)} %bitcast.206), channel_id=1, source_target_pairs={{0,6},{2,0},{4,2},{6,4},{1,7},{3,1},{5,3},{7,5},{8,14},{10,8},{12,... | collective-permute-start | bytes 1572872 | tf_op jit(solution)/shard_map/ppermute | solution.py:29
  73.2 1.9 collective-permute-start.3
  75.3 4.3 %collective-permute-done.4 = bf16[1024,256]{1,0:T(8,128)(2,1)} collective-permute-done((bf16[1024,256]{1,0:T(8,128)(2,1)S(1)}, bf16[1024,256]{1,0:T(8,128)(2,1)}, u32[]{:S(2)}, u32[]{:S(2)}) %collective-permute-start.4) | collective-permute-done | bytes 524320 | tf_op jit(solution)/shard_map/ppermute | solution.py:29
  79.5 1.9 collective-permute-start.5
  82.3 2.1 %collective-permute-done.6 = bf16[1024,256]{1,0:T(8,128)(2,1)} collective-permute-done((bf16[1024,256]{1,0:T(8,128)(2,1)S(1)}, bf16[1024,256]{1,0:T(8,128)(2,1)}, u32[]{:S(2)}, u32[]{:S(2)}) %collective-permute-start.6) | collective-permute-done | bytes 524320 | tf_op jit(solution)/shard_map/ppermute | solution.py:29
  84.4 1.9 collective-permute-start.7
  87.3 4.1 %collective-permute-done.8 = bf16[1024,256]{1,0:T(8,128)(2,1)} collective-permute-done((bf16[1024,256]{1,0:T(8,128)(2,1)S(1)}, bf16[1024,256]{1,0:T(8,128)(2,1)}, u32[]{:S(2)}, u32[]{:S(2)}) %collective-permute-start.8) | collective-permute-done | bytes 524320 | tf_op jit(solution)/shard_map/ppermute | solution.py:29
  91.4 1.9 collective-permute-start.9
  93.3 1.9 constant_dynamic-update-slice_fusion.6
  95.2 1.9 constant_dynamic-update-slice_fusion.5
  98.0 1.9 constant_dynamic-update-slice_fusion.3
  100.8 1.9 constant_dynamic-update-slice_fusion.1
  102.7 6.3 %all-to-all-done.1 = bf16[16,128,256]{2,1,0:T(8,128)(2,1)S(1)} async-done(((bf16[16,128,256]{2,1,0:T(8,128)(2,1)}), bf16[16,128,256]{2,1,0:T(8,128)(2,1)S(1)}, u32[]{:S(2)}, u32[]{:S(2)}) %all-to-all-start.1) | async-done | bytes 1048608 | tf_op jit(solution)/shard_map/all_to_all | solution.py:25
  109.0 9.0 %all-to-all-start.2 = ((bf16[16,64,256]{2,1,0:T(8,128)(2,1)}), bf16[16,64,256]{2,1,0:T(8,128)(2,1)S(1)}, u32[]{:S(2)}, u32[]{:S(2)}) async-start(bf16[16,64,256]{2,1,0:T(8,128)(2,1)} %pad_maximum_fusion.1), calls=%async_computation.2 | async-start | bytes 1048576 | tf_op jit(solution)/shard_map/all_to_all | solution.py:25
  119.1 3.4 %fusion.71 = f32[1024,256]{1,0:T(8,128)S(1)} fusion(bf16[1024,2048]{1,0:T(8,128)(2,1)} %constant_dynamic-update-slice_fusion, bf16[2048,256]{1,0:T(8,128)(2,1)S(1)} %bitcast_dynamic-update-slice_fusion.12), kind=kOutput, calls=%fused_computation.155 | convolution fusion | flops 1073741824 | bytes 6291456 | tf_op jit(solution)/shard_map/dot_general | solution.py:112
  122.7 3.4 %collective-permute-start.11 = (bf16[1024,128]{1,0:T(8,128)(2,1)S(1)}, bf16[1024,128]{1,0:T(8,128)(2,1)S(1)}, u32[]{:S(2)}, u32[]{:S(2)}) collective-permute-start(bf16[1024,128]{1,0:T(8,128)(2,1)S(1)} %fusion.10), channel_id=1, source_target_pairs={{0,2},{2,4},{4,6},{6,0},{1,3},{3,5},{5,7},{7,1},{8,10},{10,12},{12... | collective-permute-start | bytes 786440 | tf_op jit(solution)/shard_map/ppermute | solution.py:123
  126.2 3.0 %collective-permute-start.13 = (bf16[1024,128]{1,0:T(8,128)(2,1)S(1)}, bf16[1024,128]{1,0:T(8,128)(2,1)}, u32[]{:S(2)}, u32[]{:S(2)}) collective-permute-start(bf16[1024,128]{1,0:T(8,128)(2,1)S(1)} %fusion.10), channel_id=1, source_target_pairs={{0,4},{2,6},{4,0},{6,2},{1,5},{3,7},{5,1},{7,3},{8,12},{10,14},{12... | collective-permute-start | bytes 786440 | tf_op jit(solution)/shard_map/ppermute | solution.py:123
  129.2 4.1 %collective-permute-start.15 = (bf16[1024,128]{1,0:T(8,128)(2,1)S(1)}, bf16[1024,128]{1,0:T(8,128)(2,1)S(1)}, u32[]{:S(2)}, u32[]{:S(2)}) collective-permute-start(bf16[1024,128]{1,0:T(8,128)(2,1)S(1)} %fusion.10), channel_id=1, source_target_pairs={{0,6},{2,0},{4,2},{6,4},{1,7},{3,1},{5,3},{7,5},{8,14},{10,8},{12,... | collective-permute-start | bytes 786440 | tf_op jit(solution)/shard_map/ppermute | solution.py:123
  133.3 1.9 collective-permute-start.10
  135.2 2.4 %collective-permute-start.12 = (bf16[1024,128]{1,0:T(8,128)(2,1)S(1)}, bf16[1024,128]{1,0:T(8,128)(2,1)S(1)}, u32[]{:S(2)}, u32[]{:S(2)}) collective-permute-start(bf16[1024,128]{1,0:T(8,128)(2,1)S(1)} %collective-permute-done.11), channel_id=1, source_target_pairs={{0,1},{1,0},{2,3},{3,2},{4,5},{5,4},{6,7},{7,6},{8,9},{9,8},{10,11... | collective-permute-start | bytes 786440 | tf_op jit(solution)/shard_map/ppermute | solution.py:124
  137.6 1.3 collective-permute-done.13
  138.9 1.9 collective-permute-start.14
  140.8 1.3 collective-permute-done.15
  142.1 1.9 collective-permute-start.16
  144.0 2.4 %all-to-all-done.2 = bf16[16,64,256]{2,1,0:T(8,128)(2,1)S(1)} async-done(((bf16[16,64,256]{2,1,0:T(8,128)(2,1)}), bf16[16,64,256]{2,1,0:T(8,128)(2,1)S(1)}, u32[]{:S(2)}, u32[]{:S(2)}) %all-to-all-start.2) | async-done | bytes 524320 | tf_op jit(solution)/shard_map/all_to_all | solution.py:25
  147.2 1.2 fusion.43
  150.5 1.9 collective-permute-start.17
  152.5 9.5 %all-to-all-start.3 = ((bf16[32,32,256]{2,1,0:T(8,128)(2,1)}), bf16[32,32,256]{2,1,0:T(8,128)(2,1)S(1)}, u32[]{:S(2)}, u32[]{:S(2)}) async-start(bf16[32,32,256]{2,1,0:T(8,128)(2,1)} %bitcast.50), calls=%async_computation.3 | async-start | bytes 1048576 | tf_op jit(solution)/shard_map/all_to_all | solution.py:25
  162.2 2.1 %collective-permute-start.18 = (bf16[128,512]{1,0:T(8,128)(2,1)S(1)}, bf16[128,512]{1,0:T(8,128)(2,1)S(1)}, u32[]{:S(2)}, u32[]{:S(2)}) collective-permute-start(bf16[128,512]{1,0:T(8,128)(2,1)S(1)} %get-tuple-element.38), channel_id=1, source_target_pairs={{0,6},{2,0},{4,2},{6,4},{1,7},{3,1},{5,3},{7,5},{8,14},{10,8},{12,... | collective-permute-start | bytes 393224 | tf_op jit(solution)/shard_map/ppermute | solution.py:141
  165.3 3.8 %collective-permute-start.19 = (bf16[128,512]{1,0:T(8,128)(2,1)S(1)}, bf16[128,512]{1,0:T(8,128)(2,1)S(1)}, u32[]{:S(2)}, u32[]{:S(2)}) collective-permute-start(bf16[128,512]{1,0:T(8,128)(2,1)S(1)} %get-tuple-element.39), channel_id=1, source_target_pairs={{0,4},{2,6},{4,0},{6,2},{1,5},{3,7},{5,1},{7,3},{8,12},{10,14},{12... | collective-permute-start | bytes 393224 | tf_op jit(solution)/shard_map/ppermute | solution.py:141
  169.1 3.6 %collective-permute-start.20 = (bf16[128,512]{1,0:T(8,128)(2,1)S(1)}, bf16[128,512]{1,0:T(8,128)(2,1)S(1)}, u32[]{:S(2)}, u32[]{:S(2)}) collective-permute-start(bf16[128,512]{1,0:T(8,128)(2,1)S(1)} %get-tuple-element.36), channel_id=1, source_target_pairs={{0,2},{2,4},{4,6},{6,0},{1,3},{3,5},{5,7},{7,1},{8,10},{10,12},{12... | collective-permute-start | bytes 393224 | tf_op jit(solution)/shard_map/ppermute | solution.py:141
  172.7 1.3 collective-permute-done.19
  174.0 2.8 %collective-permute-done.20 = bf16[128,512]{1,0:T(8,128)(2,1)S(1)} collective-permute-done((bf16[128,512]{1,0:T(8,128)(2,1)S(1)}, bf16[128,512]{1,0:T(8,128)(2,1)S(1)}, u32[]{:S(2)}, u32[]{:S(2)}) %collective-permute-start.20) | collective-permute-done | bytes 131104 | tf_op jit(solution)/shard_map/ppermute | solution.py:141
  178.3 13.6 %all-to-all-done.3 = bf16[32,32,256]{2,1,0:T(8,128)(2,1)S(1)} async-done(((bf16[32,32,256]{2,1,0:T(8,128)(2,1)}), bf16[32,32,256]{2,1,0:T(8,128)(2,1)S(1)}, u32[]{:S(2)}, u32[]{:S(2)}) %all-to-all-start.3) | async-done | bytes 524320 | tf_op jit(solution)/shard_map/all_to_all | solution.py:25
  (75 shorter events, 14.6 us)
Async XLA Ops:
  4.0 29.4 %collective-permute-start = (bf16[8,48,256]{2,1,0:T(8,128)(2,1)}, bf16[8,48,256]{2,1,0:T(8,128)(2,1)S(1)}, u32[]{:S(2)}, u32[]{:S(2)}) collective-permute-start(bf16[8,48,256]{2,1,0:T(8,128)(2,1)} %pad_maximum_fusion.2), channel_id=1, source_target_pairs={{0,24},{8,0},{16,8},{24,16},{1,25},{9,1},{17,9},{25,17},{2,26},{10... | collective-permute-start | bytes 589832 | tf_op jit(solution)/shard_map/ppermute | solution.py:93
  12.6 42.5 %all-to-all-start = ((bf16[32,32,256]{2,1,0:T(8,128)(2,1)}), bf16[32,32,256]{2,1,0:T(8,128)(2,1)S(1)}, u32[]{:S(2)}, u32[]{:S(2)}) async-start(bf16[32,32,256]{2,1,0:T(8,128)(2,1)} %bitcast.29), calls=%async_computation | async-start | bytes 1048576 | tf_op jit(solution)/shard_map/all_to_all | solution.py:25
  25.7 12.7 %collective-permute-start.1 = (bf16[8,48,256]{2,1,0:T(8,128)(2,1)S(1)}, bf16[8,48,256]{2,1,0:T(8,128)(2,1)S(1)}, u32[]{:S(2)}, u32[]{:S(2)}) collective-permute-start(bf16[8,48,256]{2,1,0:T(8,128)(2,1)S(1)} %pad_maximum_fusion.3), channel_id=1, source_target_pairs={{0,16},{8,24},{16,0},{24,8},{1,17},{9,25},{17,1},{25,9},{2,18},{10... | collective-permute-start | bytes 589832 | tf_op jit(solution)/shard_map/ppermute | solution.py:93
  31.0 11.7 %collective-permute-start.2 = (bf16[8,48,256]{2,1,0:T(8,128)(2,1)S(1)}, bf16[8,48,256]{2,1,0:T(8,128)(2,1)S(1)}, u32[]{:S(2)}, u32[]{:S(2)}) collective-permute-start(bf16[8,48,256]{2,1,0:T(8,128)(2,1)S(1)} %pad_maximum_fusion.4), channel_id=1, source_target_pairs={{0,8},{8,16},{16,24},{24,0},{1,9},{9,17},{17,25},{25,1},{2,10},{10... | collective-permute-start | bytes 589832 | tf_op jit(solution)/shard_map/ppermute | solution.py:93
  55.0 54.0 %all-to-all-start.1 = ((bf16[16,128,256]{2,1,0:T(8,128)(2,1)}), bf16[16,128,256]{2,1,0:T(8,128)(2,1)S(1)}, u32[]{:S(2)}, u32[]{:S(2)}) async-start(bf16[16,128,256]{2,1,0:T(8,128)(2,1)} %pad_maximum_fusion), calls=%async_computation.1 | async-start | bytes 2097152 | tf_op jit(solution)/shard_map/all_to_all | solution.py:25
  62.7 16.8 %collective-permute-start.4 = (bf16[1024,256]{1,0:T(8,128)(2,1)S(1)}, bf16[1024,256]{1,0:T(8,128)(2,1)}, u32[]{:S(2)}, u32[]{:S(2)}) collective-permute-start(bf16[1024,256]{1,0:T(8,128)(2,1)S(1)} %bitcast.204), channel_id=1, source_target_pairs={{0,2},{2,4},{4,6},{6,0},{1,3},{3,5},{5,7},{7,1},{8,10},{10,12},{12... | collective-permute-start | bytes 1572872 | tf_op jit(solution)/shard_map/ppermute | solution.py:29
  66.1 18.3 %collective-permute-start.6 = (bf16[1024,256]{1,0:T(8,128)(2,1)S(1)}, bf16[1024,256]{1,0:T(8,128)(2,1)}, u32[]{:S(2)}, u32[]{:S(2)}) collective-permute-start(bf16[1024,256]{1,0:T(8,128)(2,1)S(1)} %bitcast.205), channel_id=1, source_target_pairs={{0,4},{2,6},{4,0},{6,2},{1,5},{3,7},{5,1},{7,3},{8,12},{10,14},{12... | collective-permute-start | bytes 1572872 | tf_op jit(solution)/shard_map/ppermute | solution.py:29
  69.2 22.2 %collective-permute-start.8 = (bf16[1024,256]{1,0:T(8,128)(2,1)S(1)}, bf16[1024,256]{1,0:T(8,128)(2,1)}, u32[]{:S(2)}, u32[]{:S(2)}) collective-permute-start(bf16[1024,256]{1,0:T(8,128)(2,1)S(1)} %bitcast.206), channel_id=1, source_target_pairs={{0,6},{2,0},{4,2},{6,4},{1,7},{3,1},{5,3},{7,5},{8,14},{10,8},{12,... | collective-permute-start | bytes 1572872 | tf_op jit(solution)/shard_map/ppermute | solution.py:29
  73.2 20.1 %collective-permute-start.3 = (bf16[1024,256]{1,0:T(8,128)(2,1)S(1)}, bf16[1024,256]{1,0:T(8,128)(2,1)}, u32[]{:S(2)}, u32[]{:S(2)}) collective-permute-start(bf16[1024,256]{1,0:T(8,128)(2,1)S(1)} %bitcast.207), channel_id=1, source_target_pairs={{0,1},{1,0},{2,3},{3,2},{4,5},{5,4},{6,7},{7,6},{8,9},{9,8},{10,11... | collective-permute-start | bytes 1572872 | tf_op jit(solution)/shard_map/ppermute | solution.py:31
  79.5 17.6 %collective-permute-start.5 = (bf16[1024,256]{1,0:T(8,128)(2,1)}, bf16[1024,256]{1,0:T(8,128)(2,1)S(1)}, u32[]{:S(2)}, u32[]{:S(2)}) collective-permute-start(bf16[1024,256]{1,0:T(8,128)(2,1)} %collective-permute-done.4), channel_id=1, source_target_pairs={{0,1},{1,0},{2,3},{3,2},{4,5},{5,4},{6,7},{7,6},{8,9},{9,8},{10,11... | collective-permute-start | bytes 1572872 | tf_op jit(solution)/shard_map/ppermute | solution.py:31
  84.4 15.5 %collective-permute-start.7 = (bf16[1024,256]{1,0:T(8,128)(2,1)}, bf16[1024,256]{1,0:T(8,128)(2,1)S(1)}, u32[]{:S(2)}, u32[]{:S(2)}) collective-permute-start(bf16[1024,256]{1,0:T(8,128)(2,1)} %collective-permute-done.6), channel_id=1, source_target_pairs={{0,1},{1,0},{2,3},{3,2},{4,5},{5,4},{6,7},{7,6},{8,9},{9,8},{10,11... | collective-permute-start | bytes 1572872 | tf_op jit(solution)/shard_map/ppermute | solution.py:31
  91.4 26.6 %collective-permute-start.9 = (bf16[1024,256]{1,0:T(8,128)(2,1)}, bf16[1024,256]{1,0:T(8,128)(2,1)S(1)}, u32[]{:S(2)}, u32[]{:S(2)}) collective-permute-start(bf16[1024,256]{1,0:T(8,128)(2,1)} %collective-permute-done.8), channel_id=1, source_target_pairs={{0,1},{1,0},{2,3},{3,2},{4,5},{5,4},{6,7},{7,6},{8,9},{9,8},{10,11... | collective-permute-start | bytes 1572872 | tf_op jit(solution)/shard_map/ppermute | solution.py:31
  109.0 37.4 %all-to-all-start.2 = ((bf16[16,64,256]{2,1,0:T(8,128)(2,1)}), bf16[16,64,256]{2,1,0:T(8,128)(2,1)S(1)}, u32[]{:S(2)}, u32[]{:S(2)}) async-start(bf16[16,64,256]{2,1,0:T(8,128)(2,1)} %pad_maximum_fusion.1), calls=%async_computation.2 | async-start | bytes 1048576 | tf_op jit(solution)/shard_map/all_to_all | solution.py:25
  122.7 12.4 %collective-permute-start.11 = (bf16[1024,128]{1,0:T(8,128)(2,1)S(1)}, bf16[1024,128]{1,0:T(8,128)(2,1)S(1)}, u32[]{:S(2)}, u32[]{:S(2)}) collective-permute-start(bf16[1024,128]{1,0:T(8,128)(2,1)S(1)} %fusion.10), channel_id=1, source_target_pairs={{0,2},{2,4},{4,6},{6,0},{1,3},{3,5},{5,7},{7,1},{8,10},{10,12},{12... | collective-permute-start | bytes 786440 | tf_op jit(solution)/shard_map/ppermute | solution.py:123
  126.2 12.7 %collective-permute-start.13 = (bf16[1024,128]{1,0:T(8,128)(2,1)S(1)}, bf16[1024,128]{1,0:T(8,128)(2,1)}, u32[]{:S(2)}, u32[]{:S(2)}) collective-permute-start(bf16[1024,128]{1,0:T(8,128)(2,1)S(1)} %fusion.10), channel_id=1, source_target_pairs={{0,4},{2,6},{4,0},{6,2},{1,5},{3,7},{5,1},{7,3},{8,12},{10,14},{12... | collective-permute-start | bytes 786440 | tf_op jit(solution)/shard_map/ppermute | solution.py:123
  129.2 12.9 %collective-permute-start.15 = (bf16[1024,128]{1,0:T(8,128)(2,1)S(1)}, bf16[1024,128]{1,0:T(8,128)(2,1)S(1)}, u32[]{:S(2)}, u32[]{:S(2)}) collective-permute-start(bf16[1024,128]{1,0:T(8,128)(2,1)S(1)} %fusion.10), channel_id=1, source_target_pairs={{0,6},{2,0},{4,2},{6,4},{1,7},{3,1},{5,3},{7,5},{8,14},{10,8},{12,... | collective-permute-start | bytes 786440 | tf_op jit(solution)/shard_map/ppermute | solution.py:123
  133.3 13.4 %collective-permute-start.10 = (bf16[1024,128]{1,0:T(8,128)(2,1)S(1)}, bf16[1024,128]{1,0:T(8,128)(2,1)S(1)}, u32[]{:S(2)}, u32[]{:S(2)}) collective-permute-start(bf16[1024,128]{1,0:T(8,128)(2,1)S(1)} %fusion.10), channel_id=1, source_target_pairs={{0,1},{1,0},{2,3},{3,2},{4,5},{5,4},{6,7},{7,6},{8,9},{9,8},{10,11... | collective-permute-start | bytes 786440 | tf_op jit(solution)/shard_map/ppermute | solution.py:124
  135.2 13.3 %collective-permute-start.12 = (bf16[1024,128]{1,0:T(8,128)(2,1)S(1)}, bf16[1024,128]{1,0:T(8,128)(2,1)S(1)}, u32[]{:S(2)}, u32[]{:S(2)}) collective-permute-start(bf16[1024,128]{1,0:T(8,128)(2,1)S(1)} %collective-permute-done.11), channel_id=1, source_target_pairs={{0,1},{1,0},{2,3},{3,2},{4,5},{5,4},{6,7},{7,6},{8,9},{9,8},{10,11... | collective-permute-start | bytes 786440 | tf_op jit(solution)/shard_map/ppermute | solution.py:124
  138.9 10.2 %collective-permute-start.14 = (bf16[1024,128]{1,0:T(8,128)(2,1)}, bf16[1024,128]{1,0:T(8,128)(2,1)S(1)}, u32[]{:S(2)}, u32[]{:S(2)}) collective-permute-start(bf16[1024,128]{1,0:T(8,128)(2,1)} %collective-permute-done.13), channel_id=1, source_target_pairs={{0,1},{1,0},{2,3},{3,2},{4,5},{5,4},{6,7},{7,6},{8,9},{9,8},{10,11... | collective-permute-start | bytes 786440 | tf_op jit(solution)/shard_map/ppermute | solution.py:124
  142.1 7.3 %collective-permute-start.16 = (bf16[1024,128]{1,0:T(8,128)(2,1)S(1)}, bf16[1024,128]{1,0:T(8,128)(2,1)S(1)}, u32[]{:S(2)}, u32[]{:S(2)}) collective-permute-start(bf16[1024,128]{1,0:T(8,128)(2,1)S(1)} %collective-permute-done.15), channel_id=1, source_target_pairs={{0,1},{1,0},{2,3},{3,2},{4,5},{5,4},{6,7},{7,6},{8,9},{9,8},{10,11... | collective-permute-start | bytes 786440 | tf_op jit(solution)/shard_map/ppermute | solution.py:124
  148.8 3.7 %copy-start = (s32[128,4]{0,1:T(4,128)S(1)}, s32[128,4]{0,1:T(4,128)}, u32[]{:S(2)}) copy-start(s32[128,4]{0,1:T(4,128)} %param.12) | copy-start | bytes 6148
  148.8 3.7 %copy-start.1 = (f32[128,4]{0,1:T(4,128)S(1)}, f32[128,4]{0,1:T(4,128)}, u32[]{:S(2)}) copy-start(f32[128,4]{0,1:T(4,128)} %param.13) | copy-start | bytes 6148
  150.5 11.5 %collective-permute-start.17 = (bf16[4,128,256]{2,1,0:T(8,128)(2,1)S(1)}, bf16[4,128,256]{2,1,0:T(8,128)(2,1)S(1)}, u32[]{:S(2)}, u32[]{:S(2)}) collective-permute-start(bf16[4,128,256]{2,1,0:T(8,128)(2,1)S(1)} %dynamic-slice_bitcast_fusion.1), channel_id=1, source_target_pairs={{0,1},{1,0},{2,3},{3,2},{4,5},{5,4},{6,7},{7,6},{8,9},{9,8},{10,11... | collective-permute-start | bytes 786440 | tf_op jit(solution)/shard_map/ppermute | solution.py:134
  152.5 39.4 %all-to-all-start.3 = ((bf16[32,32,256]{2,1,0:T(8,128)(2,1)}), bf16[32,32,256]{2,1,0:T(8,128)(2,1)S(1)}, u32[]{:S(2)}, u32[]{:S(2)}) async-start(bf16[32,32,256]{2,1,0:T(8,128)(2,1)} %bitcast.50), calls=%async_computation.3 | async-start | bytes 1048576 | tf_op jit(solution)/shard_map/all_to_all | solution.py:25
  162.2 10.5 %collective-permute-start.18 = (bf16[128,512]{1,0:T(8,128)(2,1)S(1)}, bf16[128,512]{1,0:T(8,128)(2,1)S(1)}, u32[]{:S(2)}, u32[]{:S(2)}) collective-permute-start(bf16[128,512]{1,0:T(8,128)(2,1)S(1)} %get-tuple-element.38), channel_id=1, source_target_pairs={{0,6},{2,0},{4,2},{6,4},{1,7},{3,1},{5,3},{7,5},{8,14},{10,8},{12,... | collective-permute-start | bytes 393224 | tf_op jit(solution)/shard_map/ppermute | solution.py:141
  165.3 8.7 %collective-permute-start.19 = (bf16[128,512]{1,0:T(8,128)(2,1)S(1)}, bf16[128,512]{1,0:T(8,128)(2,1)S(1)}, u32[]{:S(2)}, u32[]{:S(2)}) collective-permute-start(bf16[128,512]{1,0:T(8,128)(2,1)S(1)} %get-tuple-element.39), channel_id=1, source_target_pairs={{0,4},{2,6},{4,0},{6,2},{1,5},{3,7},{5,1},{7,3},{8,12},{10,14},{12... | collective-permute-start | bytes 393224 | tf_op jit(solution)/shard_map/ppermute | solution.py:141
  169.1 7.8 %collective-permute-start.20 = (bf16[128,512]{1,0:T(8,128)(2,1)S(1)}, bf16[128,512]{1,0:T(8,128)(2,1)S(1)}, u32[]{:S(2)}, u32[]{:S(2)}) collective-permute-start(bf16[128,512]{1,0:T(8,128)(2,1)S(1)} %get-tuple-element.36), channel_id=1, source_target_pairs={{0,2},{2,4},{4,6},{6,0},{1,3},{3,5},{5,7},{7,1},{8,10},{10,12},{12... | collective-permute-start | bytes 393224 | tf_op jit(solution)/shard_map/ppermute | solution.py:141
